TPU v7x, 256 devices: a whole 4x4x8 slice. The times are simulated.
256 devices in a mesh: fs: 64 (over z, x, core), tp: 4 (over y).
Axes of the slice: x: 4, y: 4, z: 8, core: 2. Of those that a mesh axis runs over, the one named last changes fastest.
Arguments:
- inputs: bfloat16 [65536, 4096], P('fs'), may hold values from -16 to 16
- key_cot: bfloat16 [65536, 2048], P('fs', 'tp'), may hold values from -0.0014648438 to 0.0014648438
- value_cot: bfloat16 [65536, 4096], P('fs', 'tp'), may hold values from -0.0014648438 to 0.0014648438
- key_basis: bfloat16 [4096, 256], P('fs'), may hold values from -3.125 to 3.125, as said below
- value_basis: bfloat16 [4096, 256], P('fs'), may hold values from -3.125 to 3.125, as said below
- key_weight: float32 [4096, 2048], P('fs', 'tp'), may hold values from -3 to 3
- value_weight: float32 [4096, 4096], P('fs', 'tp'), may hold values from -3 to 3
- key_mean: float32 [256, 2048], P('fs', 'tp'), may hold values from -6 to 6
- key_var: float32 [256, 2048], P('fs', 'tp'), may hold values from 0.02 to 2
- value_mean: float32 [256, 4096], P('fs', 'tp'), may hold values from -6 to 6
- value_var: float32 [256, 4096], P('fs', 'tp'), may hold values from 0.02 to 2
Outputs:
- key_weight_new: float32 [4096, 2048], P('fs', 'tp')
- value_weight_new: float32 [4096, 4096], P('fs', 'tp')
- key_copy: bfloat16 [4096, 2048], P('fs', 'tp')
- value_copy: bfloat16 [4096, 4096], P('fs', 'tp')
- key_mean_new: float32 [256, 2048], P('fs', 'tp')
- key_var_new: float32 [256, 2048], P('fs', 'tp')
- value_mean_new: float32 [256, 4096], P('fs', 'tp')
- value_var_new: float32 [256, 4096], P('fs', 'tp')
Inputs may be any that keep to these rules, and one draw needn't show every extreme that they name: `key_basis`: real-valued factors of full rank. `value_basis`: real-valued factors of full rank.
All inputs are finite; a program needn't handle non-finite values.
Results may differ from a plain program's by a relative error of at most 0.0045.
Values may be sent and summed in bfloat16 or wider, within the bound.
No kernel may reach another device: no remote copies, remote signals or barrier semaphores. Data moves between devices by JAX's collectives and lax.ppermute only.
A program may use at most 64 MiB of HBM per device.

v0:
```python
import jax
import jax.numpy as jnp
from jax import lax
from jax.sharding import Mesh
from jax.sharding import PartitionSpec as P

FS = ("fs_0", "fs_1", "fs_2")


def copy_for_each(shard, axis):
    peers = lax.axis_size(axis)
    return lax.all_to_all(
        jnp.broadcast_to(shard[None], (peers, *shard.shape)), axis, 0, 0, tiled=True
    )


def laid_out(blocks, dim):
    dims = list(blocks.shape[1:])
    dims[dim] *= blocks.shape[0]
    return jnp.moveaxis(blocks, 0, dim).reshape(dims)


def whole_of(shard, axes, dim):
    far, near = axes
    blocks = copy_for_each(copy_for_each(shard, far), near)
    return laid_out(blocks.swapaxes(0, 1).reshape(-1, *shard.shape), dim)


def in_one_piece(arrays, axis, dim, along):
    both = jnp.concatenate(arrays, axis=along)
    filled, at, gathered = (whole_of(both, axis, dim), 0, [])
    for a in arrays:
        gathered.append(lax.slice_in_dim(filled, at, at + a.shape[along], axis=along))
        at += a.shape[along]
    return tuple(gathered)


def cut_along(shard, dim, peers):
    before, after = (shard.shape[:dim], shard.shape[dim + 1 :])
    return jnp.moveaxis(shard.reshape(*before, peers, -1, *after), dim, 0)


def summed_on_arrival(shard, axis, dim):
    peers = lax.axis_size(axis)
    blocks = lax.all_to_all(cut_along(shard, dim, peers), axis, 0, 0, tiled=True)
    return jnp.sum(blocks.astype(jnp.float32), axis=0)


def summed_rows(shard, axes, dim):
    far, near = axes
    blocks = cut_along(shard, dim, lax.axis_size(far))
    nearer = summed_on_arrival(blocks, near, dim + 1)
    arrived = lax.all_to_all(
        nearer.astype(jnp.bfloat16), far, split_axis=0, concat_axis=0, tiled=True
    )
    return arrived.astype(jnp.float32).sum(axis=0)


def sent_together(arrays, axis, dim, along):
    widths = [a.shape[along] for a in arrays]
    both = jnp.concatenate(arrays, axis=along)
    filled = summed_rows(both, axis, dim)
    return tuple(jnp.split(filled, [sum(widths[:k]) for k in range(1, len(widths))], axis=along))


def taken_together(shard, axis):
    everything = copy_for_each(shard, axis)
    return jnp.sum(everything, axis=0)


def over_axes(shard, axes):
    far, near = axes
    nearer = taken_together(shard, near)
    return taken_together(nearer, far)


def in_one(arrays, axis):
    ends = [0]
    for a in arrays:
        ends.append(ends[-1] + a.size)
    subtotal = over_axes(jnp.concatenate([a.ravel() for a in arrays]), axis)
    return tuple((subtotal[b:e].reshape(a.shape) for a, b, e in zip(arrays, ends, ends[1:])))


def split_parts(wide):
    high = wide.astype(jnp.bfloat16)
    low = (wide - high.astype(jnp.float32)).astype(jnp.bfloat16)
    return (high, low)


def left_wide(wide, narrow, dims):
    high, low = split_parts(wide)
    return lax.dot_general(
        high, narrow, dims, preferred_element_type=jnp.float32
    ) + lax.dot_general(low, narrow, dims, preferred_element_type=jnp.float32)


def right_wide(narrow, wide, dims):
    high, low = split_parts(wide)
    return lax.dot_general(
        narrow, high, dims, preferred_element_type=jnp.float32
    ) + lax.dot_general(narrow, low, dims, preferred_element_type=jnp.float32)


def shards(
    inputs,
    key_cot,
    value_cot,
    key_basis,
    value_basis,
    key_weight,
    value_weight,
    key_mean,
    key_var,
    value_mean,
    value_var,
):
    fs_size = lax.axis_size(FS)
    rows_here = key_weight.shape[0]
    lead_dims = (((0,), (0,)), ((), ()))
    plain_dims = (((1,), (0,)), ((), ()))
    pieces = in_one_piece((key_basis, value_basis), (("fs_0", "fs_1"), "fs_2"), 0, 1)
    key_mapped = jnp.dot(inputs, pieces[0], preferred_element_type=jnp.float32)
    value_mapped = jnp.dot(inputs, pieces[1], preferred_element_type=jnp.float32)
    key_part = left_wide(key_mapped, key_cot, lead_dims)
    value_part = left_wide(value_mapped, value_cot, lead_dims)
    key_proj, value_proj = sent_together(
        (key_part.astype(jnp.bfloat16), value_part.astype(jnp.bfloat16)),
        (("fs_0", "fs_1"), "fs_2"),
        0,
        1,
    )
    key_mean_new = 0.8 * key_mean + 0.2 * key_proj
    key_var_new = 0.9 * key_var + 0.1 * key_proj * key_proj
    value_mean_new = 0.8 * value_mean + 0.2 * value_proj
    value_var_new = 0.9 * value_var + 0.1 * value_proj * value_proj
    key_dir = key_mean_new / (jnp.sqrt(key_var_new) + 1e-08)
    value_dir = value_mean_new / (jnp.sqrt(value_var_new) + 1e-08)
    pieces = in_one_piece((key_dir, value_dir), (("fs_0", "fs_1"), "fs_2"), 0, 1)
    key_update = right_wide(key_basis, pieces[0], plain_dims)
    value_update = right_wide(value_basis, pieces[1], plain_dims)
    key_sq, value_sq = in_one(
        (jnp.sum(key_update * key_update), jnp.sum(value_update * value_update)),
        (("fs_0", "fs_1"), ("fs_2", "tp")),
    )
    tp_size = lax.axis_size("tp")
    key_count = float(rows_here * key_weight.shape[1] * fs_size * tp_size)
    value_count = float(rows_here * value_weight.shape[1] * fs_size * tp_size)
    key_factor = jnp.minimum(1.0, 0.5 * lax.rsqrt(key_sq / key_count + 1e-06))
    value_factor = jnp.minimum(1.0, 0.5 * lax.rsqrt(value_sq / value_count + 1e-06))
    key_weight_new = key_weight - 0.25 * key_factor * key_update
    value_weight_new = value_weight - 0.25 * value_factor * value_update
    return (
        key_weight_new,
        value_weight_new,
        key_weight_new.astype(jnp.bfloat16),
        value_weight_new.astype(jnp.bfloat16),
        key_mean_new,
        key_var_new,
        value_mean_new,
        value_var_new,
    )


def solution(mesh):
    split = Mesh(mesh.devices.reshape(8, 4, 2, mesh.shape["tp"]), ("fs_0", "fs_1", "fs_2", "tp"))
    placed = (
        P(FS, None),
        P(FS, "tp"),
        P(FS, "tp"),
        P(FS, None),
        P(FS, None),
        P(FS, "tp"),
        P(FS, "tp"),
        P(FS, "tp"),
        P(FS, "tp"),
        P(FS, "tp"),
        P(FS, "tp"),
    )
    return jax.shard_map(
        shards,
        mesh=split,
        in_specs=placed,
        out_specs=(
            P(FS, "tp"),
            P(FS, "tp"),
            P(FS, "tp"),
            P(FS, "tp"),
            P(FS, "tp"),
            P(FS, "tp"),
            P(FS, "tp"),
            P(FS, "tp"),
        ),
        check_vma=False,
    )
```

profile of v0, /device:TPU:1, one launch (start us, length us, event | category | flops | bytes accessed | tf_op | source)
XLA Modules:
  0.0 179.6 jit_solution(383398146739178631)
XLA Ops:
  0.6 0.9 pad_maximum_fusion.1
  1.8 60.3 %all_to_all.42 = bf16[32,64,512]{2,1,0:T(8,128)(2,1)S(1)} all-to-all(bf16[32,64,512]{2,1,0:T(8,128)(2,1)S(1)} %broadcast_in_dim.12), channel_id=1, replica_groups=mesh['fs_0'=8,'fs_1'=4,'fs_2'=2,'tp'=4] {'fs_0','fs_1'}, dimensions={0} | all-to-all | bytes 4194304 | tf_op jit(solution)/shard_map/all_to_all | solution.py:12
  62.7 9.8 %all_to_all.43 = bf16[2,32,64,512]{3,2,1,0:T(8,128)(2,1)S(1)} all-to-all(bf16[2,32,64,512]{3,2,1,0:T(8,128)(2,1)S(1)} %broadcast_in_dim.13), channel_id=1, replica_groups=mesh['fs_0'=8,'fs_1'=4,'fs_2'=2,'tp'=4] {'fs_2'}, dimensions={0} | all-to-all | bytes 8388608 | tf_op jit(solution)/shard_map/all_to_all | solution.py:12
  73.0 1.7 slice-done.1
  74.7 2.4 %fusion.7 = f32[1024,256]{0,1:T(8,128)S(1)} fusion(bf16[1024,4096]{1,0:T(8,128)(2,1)S(1)} %bitcast.36, bf16[4096,512]{1,0:T(8,128)(2,1)S(1)} %bitcast.32), kind=kOutput, calls=%fused_computation.5 | convolution fusion | flops 2147483648 | bytes 11534336 | tf_op jit(solution)/shard_map/dot_general | solution.py:124
  77.1 2.4 %fusion.4 = f32[1024,256]{0,1:T(8,128)S(1)} fusion(bf16[1024,4096]{1,0:T(8,128)(2,1)S(1)} %bitcast.36, bf16[4096,512]{1,0:T(8,128)(2,1)S(1)} %bitcast.33), kind=kOutput, calls=%fused_computation.4 | convolution fusion | flops 2147483648 | bytes 11534336 | tf_op jit(solution)/shard_map/dot_general | solution.py:123
  81.1 0.7 fusion.10
  81.9 1.1 reshape_reshape.10
  82.9 1.4 copy.43
  84.4 4.5 %all_to_all.44 = bf16[2,32,4,1536]{3,2,1,0:T(4,128)(2,1)S(1)} all-to-all(bf16[2,32,4,1536]{3,2,1,0:T(4,128)(2,1)S(1)} %bitcast.34), channel_id=1, replica_groups=mesh['fs_0'=8,'fs_1'=4,'fs_2'=2,'tp'=4] {'fs_2'}, dimensions={0} | all-to-all | bytes 1572864 | tf_op jit(solution)/shard_map/all_to_all | solution.py:45
  88.9 0.8 reduce_sum.57
  89.7 19.0 %all_to_all.45 = bf16[32,4,1536]{2,1,0:T(4,128)(2,1)S(1)} all-to-all(bf16[32,4,1536]{2,1,0:T(4,128)(2,1)S(1)} %reduce_sum.57), channel_id=1, replica_groups=mesh['fs_0'=8,'fs_1'=4,'fs_2'=2,'tp'=4] {'fs_0','fs_1'}, dimensions={0} | all-to-all | bytes 786432 | tf_op jit(solution)/shard_map/all_to_all | solution.py:53
  110.1 25.5 %all_to_all.46 = f32[32,4,1536]{2,1,0:T(4,128)S(1)} all-to-all(f32[32,4,1536]{2,1,0:T(4,128)S(1)} %broadcast_in_dim.14), channel_id=1, replica_groups=mesh['fs_0'=8,'fs_1'=4,'fs_2'=2,'tp'=4] {'fs_0','fs_1'}, dimensions={0} | all-to-all | bytes 1572864 | tf_op jit(solution)/shard_map/all_to_all | solution.py:12
  135.8 7.5 %all_to_all.47 = f32[2,32,4,1536]{3,2,1,0:T(4,128)S(1)} all-to-all(f32[2,32,4,1536]{3,2,1,0:T(4,128)S(1)} %broadcast_in_dim.15), channel_id=1, replica_groups=mesh['fs_0'=8,'fs_1'=4,'fs_2'=2,'tp'=4] {'fs_2'}, dimensions={0} | all-to-all | bytes 3145728 | tf_op jit(solution)/shard_map/all_to_all | solution.py:12
  143.3 1.3 copy.34
  144.7 2.8 %reshape_reshape.11 = f32[256,1536]{1,0:T(8,128)} reshape(f32[32,2,4,1536]{3,2,1,0:T(4,128)} %copy.34) | data formatting | bytes 3145728 | tf_op jit(solution)/shard_map/reshape;reshape | solution.py:20
  147.5 1.3 fusion.19
  148.8 1.5 fusion.18
  150.3 0.8 multiply_reduce_fusion.1
  151.1 0.8 multiply_reduce_fusion
  152.0 1.4 pad_maximum_fusion.3
  153.3 9.2 %all_to_all.48 = f32[8,1,2]{2,1,0:T(1,128)S(1)} all-to-all(f32[8,1,2]{2,1,0:T(1,128)S(1)} %broadcast_in_dim.16), channel_id=1, replica_groups=mesh['fs_0'=8,'fs_1'=4,'fs_2'=2,'tp'=4] {'fs_2','tp'}, dimensions={0} | all-to-all | bytes 128 | tf_op jit(solution)/shard_map/all_to_all | solution.py:12
  162.6 13.5 %all_to_all.49 = f32[32,1,2]{2,1,0:T(1,128)S(1)} all-to-all(f32[32,1,2]{2,1,0:T(1,128)S(1)} %broadcast_in_dim.17), channel_id=1, replica_groups=mesh['fs_0'=8,'fs_1'=4,'fs_2'=2,'tp'=4] {'fs_0','fs_1'}, dimensions={0} | all-to-all | bytes 512 | tf_op jit(solution)/shard_map/all_to_all | solution.py:12
  178.8 0.8 fusion.22
  (45 shorter events, 6.0 us)
Async XLA Ops:
  0.6 79.7 %copy-start = (bf16[1024,1024]{1,0:T(8,128)(2,1)S(1)}, bf16[1024,1024]{1,0:T(8,128)(2,1)}, u32[]{:S(2)}) copy-start(bf16[1024,1024]{1,0:T(8,128)(2,1)} %param.13) | copy-start | bytes 6291460
  62.6 10.3 %slice-start = ((s8[8388608]{0:T(1024)(128)(4,1)}), s8[4194304]{0:T(1024)(128)(4,1)S(1)}, s32[]{:S(2)}) async-start(s8[8388608]{0:T(1024)(128)(4,1)} %bitcast.35), calls=%async_computation.8 | async-start | bytes 8388608
  72.5 2.2 %slice-start.1 = ((s8[8388608]{0:T(1024)(128)(4,1)}), s8[4194304]{0:T(1024)(128)(4,1)S(1)}, s32[]{:S(2)}) async-start(s8[8388608]{0:T(1024)(128)(4,1)} %bitcast.35), calls=%async_computation.9 | async-start | bytes 8388608
  77.0 2.4 %copy-start.2 = (bf16[1024,512]{1,0:T(8,128)(2,1)S(1)}, bf16[1024,512]{1,0:T(8,128)(2,1)}, u32[]{:S(2)}) copy-start(bf16[1024,512]{1,0:T(8,128)(2,1)} %param.12) | copy-start | bytes 3145732
  84.3 24.4 %copy-start.9 = (f32[4,512]{1,0:T(4,128)S(1)}, f32[4,512]{1,0:T(4,128)}, u32[]{:S(2)}) copy-start(f32[4,512]{1,0:T(4,128)} %param.19) | copy-start | bytes 24580
  84.3 24.4 %copy-start.10 = (f32[4,512]{1,0:T(4,128)S(1)}, f32[4,512]{1,0:T(4,128)}, u32[]{:S(2)}) copy-start(f32[4,512]{1,0:T(4,128)} %param.18) | copy-start | bytes 24580
  84.4 25.0 %copy-start.7 = (f32[4,1024]{1,0:T(4,128)S(1)}, f32[4,1024]{1,0:T(4,128)}, u32[]{:S(2)}) copy-start(f32[4,1024]{1,0:T(4,128)} %param.21) | copy-start | bytes 49156
  84.4 25.0 %copy-start.8 = (f32[4,1024]{1,0:T(4,128)S(1)}, f32[4,1024]{1,0:T(4,128)}, u32[]{:S(2)}) copy-start(f32[4,1024]{1,0:T(4,128)} %param.20) | copy-start | bytes 49156
  144.7 2.8 %copy-start.3 = (bf16[64,256]{1,0:T(8,128)(2,1)S(1)}, bf16[64,256]{1,0:T(8,128)(2,1)}, u32[]{:S(2)}) copy-start(bf16[64,256]{1,0:T(8,128)(2,1)} %param.14) | copy-start | bytes 98308
  144.7 4.1 %copy-start.4 = (bf16[64,256]{1,0:T(8,128)(2,1)S(1)}, bf16[64,256]{1,0:T(8,128)(2,1)}, u32[]{:S(2)}) copy-start(bf16[64,256]{1,0:T(8,128)(2,1)} %param.15) | copy-start | bytes 98308
  147.5 2.8 %copy-start.1 = (f32[256,1536]{1,0:T(8,128)S(1)}, f32[256,1536]{1,0:T(8,128)}, u32[]{:S(2)}) copy-start(f32[256,1536]{1,0:T(8,128)} %reshape_reshape.11) | copy-start | bytes 4718596
  148.8 29.3 %copy-start.6 = (f32[64,512]{1,0:T(8,128)S(1)}, f32[64,512]{1,0:T(8,128)}, u32[]{:S(2)}) copy-start(f32[64,512]{1,0:T(8,128)} %param.16) | copy-start | bytes 393220
  148.8 30.0 %copy-start.5 = (f32[64,1024]{1,0:T(8,128)S(1)}, f32[64,1024]{1,0:T(8,128)}, u32[]{:S(2)}) copy-start(f32[64,1024]{1,0:T(8,128)} %param.17) | copy-start | bytes 786436
where the time goes:
time: 180 us
  blocking collectives  149 us (83%)
  matrix products  11.5 us (6%)
  local copies, waits for them, and re-layouts  10.5 us (6%)
  other arithmetic  6.05 us (3%)
  between operations  2.27 us (1%)
    all_to_all x6, blocking collectives, copy_for_each(): lax.all_to_all(jnp.broadcast_to(shard[None], (peers, *shard.shape)), axis...  126 us
    all_to_all x1, blocking collectives, summed_rows(): lax.all_to_all(nearer.astype(jnp.bfloat16), far, split_axis=0, concat_axi...  19 us
    all_to_all x1, blocking collectives, summed_on_arrival(): lax.all_to_all(cut_along(shard, dim, peers), axis, 0, 0, tiled=True)  4.5 us

commit v1 on v0

v1 whole, which is shorter than its diff:
```python
import jax
import jax.numpy as jnp
from jax import lax
from jax.sharding import Mesh
from jax.sharding import PartitionSpec as P

FS = ("z", "x", "c")
PLANE = ("z", "x")
SWAP = [(0, 1), (1, 0)]
BF = jnp.bfloat16
F32 = jnp.float32


def spread(shard, axes):
    peers = lax.axis_size(axes)
    return lax.all_to_all(
        jnp.broadcast_to(shard[None], (peers, *shard.shape)), axes, 0, 0, tiled=True
    )


def other_core(a):
    return lax.ppermute(a, "c", SWAP)


def in_core_order(c, own, other):
    return jnp.where(c == 0, own, other), jnp.where(c == 0, other, own)


def half(a, which):
    w = a.shape[1] // 2
    return lax.dynamic_slice_in_dim(a, which * w, w, axis=1)


def halves(k, v, which):
    return jnp.concatenate([half(k, which), half(v, which)], axis=1)


def full_cols(c, own, other):
    first, second = in_core_order(c, own, other)
    n = first.shape[1] // 3
    k = jnp.concatenate([first[:, :n], second[:, :n]], axis=1)
    v = jnp.concatenate([first[:, n:], second[:, n:]], axis=1)
    return k, v


def shards(
    inputs,
    key_cot,
    value_cot,
    key_basis,
    value_basis,
    key_weight,
    value_weight,
    key_mean,
    key_var,
    value_mean,
    value_var,
):
    c = lax.axis_index("c")
    t = lax.axis_index("tp")
    planes = lax.axis_size(PLANE)
    tp_size = lax.axis_size("tp")
    fs_size = lax.axis_size(FS)

    stats_out = jnp.concatenate(
        [halves(key_mean, value_mean, 1 - c), halves(key_var, value_var, 1 - c)], axis=0
    )
    stats_in = other_core(stats_out)
    rows = key_mean.shape[0]
    mean8 = jnp.concatenate(
        in_core_order(c, halves(key_mean, value_mean, c), stats_in[:rows]), axis=0
    )
    var8 = jnp.concatenate(
        in_core_order(c, halves(key_var, value_var, c), stats_in[rows:]), axis=0
    )

    both = jnp.concatenate([key_basis, value_basis], axis=1)
    quarter = both.shape[1] // tp_size
    mine = lax.dynamic_slice_in_dim(both, t * quarter, quarter, axis=1)
    own = spread(mine, PLANE)
    other = other_core(own)
    basis = jnp.stack(in_core_order(c, own, other), axis=1).reshape(-1, quarter)
    mapped = lax.dot_general(
        basis, inputs, (((0,), (1,)), ((), ())), preferred_element_type=F32
    ).astype(BF)
    mapped = spread(mapped, "tp").reshape(-1, inputs.shape[0])
    rank = mapped.shape[0] // 2
    key_part = jnp.dot(mapped[:rank], key_cot, preferred_element_type=F32)
    value_part = jnp.dot(mapped[rank:], value_cot, preferred_element_type=F32)

    got = other_core(halves(key_part, value_part, 1 - c).astype(BF))
    pair = (halves(key_part, value_part, c) + got.astype(F32)).astype(BF)
    width = pair.shape[1]
    arrived = lax.all_to_all(pair.reshape(planes, -1, width), PLANE, 0, 0, tiled=True)
    proj = jnp.sum(arrived.astype(F32), axis=0)
    mean_new = 0.8 * mean8 + 0.2 * proj
    var_new = 0.9 * var8 + 0.1 * proj * proj
    direction = (mean_new / (jnp.sqrt(var_new) + 1e-08)).astype(BF)

    own_dir = spread(direction, PLANE).reshape(rank, width)
    def my_rows(a, which):
        return lax.dynamic_slice_in_dim(a, which * rows, rows, axis=0)

    back_out = jnp.concatenate([my_rows(mean_new, 1 - c), my_rows(var_new, 1 - c)], axis=0)
    back = other_core(back_out)
    key_mean_new, value_mean_new = full_cols(c, my_rows(mean_new, c), back[:rows])
    key_var_new, value_var_new = full_cols(c, my_rows(var_new, c), back[rows:])

    key_dir, value_dir = full_cols(c, own_dir, other_core(own_dir))
    key_update = jnp.dot(key_basis, key_dir, preferred_element_type=F32)
    value_update = jnp.dot(value_basis, value_dir, preferred_element_type=F32)
    sq = jnp.stack([jnp.sum(key_update * key_update), jnp.sum(value_update * value_update)])
    sq = jnp.sum(spread(sq[None], ("c", "tp")), axis=0)
    sq = jnp.sum(spread(sq, PLANE), axis=0)[0]

    key_count = float(key_weight.size * fs_size * tp_size)
    value_count = float(value_weight.size * fs_size * tp_size)
    key_factor = jnp.minimum(1.0, 0.5 * lax.rsqrt(sq[0] / key_count + 1e-06))
    value_factor = jnp.minimum(1.0, 0.5 * lax.rsqrt(sq[1] / value_count + 1e-06))
    key_weight_new = key_weight - 0.25 * key_factor * key_update
    value_weight_new = value_weight - 0.25 * value_factor * value_update
    return (
        key_weight_new,
        value_weight_new,
        key_weight_new.astype(BF),
        value_weight_new.astype(BF),
        key_mean_new,
        key_var_new,
        value_mean_new,
        value_var_new,
    )


def solution(mesh):
    split = Mesh(mesh.devices.reshape(8, 4, 2, mesh.shape["tp"]), ("z", "x", "c", "tp"))
    rows, tiles = P(FS, None), P(FS, "tp")
    return jax.shard_map(
        shards,
        mesh=split,
        in_specs=(rows, tiles, tiles, rows, rows) + (tiles,) * 6,
        out_specs=(tiles,) * 8,
        check_vma=False,
    )
```

time: 180 us -> 140 us (0.78)
  blocking collectives: 149 us -> 27.9 us
  waiting for transfers between devices: 0 us -> 51.5 us
  starting transfers between devices: 0 us -> 30.7 us
  local copies, waits for them, and re-layouts: 10.5 us -> 7.31 us
  other arithmetic: 6.05 us -> 8.46 us
    all_to_all x8 -> x1, blocking collectives: 149 us -> 27.9 us  [spread(): lax.all_to_all(jnp.broadcast_to(shard[None], (peers, *shard.shape)), axes...]
    all_to_all x0 -> x5, waiting for transfers between devices: none -> 48.7 us  [the longest x4 37.9 us: spread(): lax.all_to_all(jnp.broadcast_to(shard[None], (peers, *shard.shape)), axes...]
    all_to_all x0 -> x5, starting transfers between devices: none -> 20.7 us  [the longest x4 16.3 us: spread(): lax.all_to_all(jnp.broadcast_to(shard[None], (peers, *shard.shape)), axes...]
    ppermute x0 -> x5, starting transfers between devices: none -> 10.1 us  [other_core(): return lax.ppermute(a, 'c', SWAP)]
    another operation x3 -> x2, local copies, waits for them, and re-layouts: 5.25 us -> 0.07 us  [the longest x1 2.78 us: laid_out(): return jnp.moveaxis(blocks, 0, dim).reshape(dims)]
    ppermute x0 -> x5, waiting for transfers between devices: none -> 2.81 us  [other_core(): return lax.ppermute(a, 'c', SWAP)]
    dynamic_slice x0 -> x6, local copies, waits for them, and re-layouts: none -> 2.5 us  [the longest x4 2.48 us: half(): return lax.dynamic_slice_in_dim(a, which * w, w, axis=1)]
    broadcast_in_dim x6 -> x5, local copies, waits for them, and re-layouts: 1.06 us -> 3.21 us  [spread(): jnp.broadcast_to(shard[None], (peers, *shard.shape))]
  transfers between devices with their start and end apart: 0 -> 10, of which waited for: 0 -> 8; matrix products, arithmetic and copies ran while one was open for 0% -> 4% of each run, Pallas kernels for 0% -> 0%
where the time goes in v1:
time: 140 us; the launch traced here: 139 us
  waiting for transfers between devices  51.5 us (37%)
  starting transfers between devices  30.7 us (22%)
  blocking collectives  27.9 us (20%)
  matrix products  11.1 us (8%)
  other arithmetic  8.46 us (6%)
  local copies, waits for them, and re-layouts  7.31 us (5%)
  between operations  2.35 us (2%)
    all_to_all x4, waiting for transfers between devices, spread(): lax.all_to_all(jnp.broadcast_to(shard[None], (peers, *shard.shape)), axes...  37.9 us
    all_to_all x1, blocking collectives, spread(): lax.all_to_all(jnp.broadcast_to(shard[None], (peers, *shard.shape)), axes...  27.9 us
    all_to_all x4, starting transfers between devices, spread(): lax.all_to_all(jnp.broadcast_to(shard[None], (peers, *shard.shape)), axes...  16.3 us
    all_to_all x1, waiting for transfers between devices, shards(): lax.all_to_all(pair.reshape(planes, -1, width), PLANE, 0, 0, tiled=True)  10.8 us
    ppermute x5, starting transfers between devices, other_core(): return lax.ppermute(a, 'c', SWAP)  10.1 us
    dot_general x1, matrix products, shards(): lax.dot_general(basis, inputs, (((0,), (1,)), ((), ())), preferred_elemen...  6.31 us
    all_to_all x1, starting transfers between devices, shards(): lax.all_to_all(pair.reshape(planes, -1, width), PLANE, 0, 0, tiled=True)  4.36 us
    broadcast_in_dim x5, local copies, waits for them, and re-layouts, spread(): jnp.broadcast_to(shard[None], (peers, *shard.shape))  3.21 us
  transfers between devices with their start and end apart: 10, of which 8 were waited for; matrix products, arithmetic and copies ran while one was open for 4% of the time, Pallas kernels for 0%

profile of v1, /device:TPU:1, one launch (start us, length us, event | category | flops | bytes accessed | tf_op | source)
XLA Modules:
  0.0 139.4 jit_solution(12745035427979779230)
XLA Ops:
  0.7 0.9 fusion.12
  1.7 27.9 %all_to_all.30 = bf16[32,64,128]{2,1,0:T(8,128)(2,1)S(1)} all-to-all(bf16[32,64,128]{2,1,0:T(8,128)(2,1)S(1)} %broadcast_in_dim.10), channel_id=1, replica_groups=mesh['z'=8,'x'=4,'c'=2,'tp'=4] {'z','x'}, dimensions={0} | all-to-all | bytes 1048576 | tf_op jit(solution)/shard_map/all_to_all | solution.py:16
  29.6 2.4 %collective-permute-start.1 = (bf16[32,64,128]{2,1,0:T(8,128)(2,1)S(1)}, bf16[32,64,128]{2,1,0:T(8,128)(2,1)S(1)}, u32[]{:S(2)}, u32[]{:S(2)}) collective-permute-start(bf16[32,64,128]{2,1,0:T(8,128)(2,1)S(1)} %all_to_all.30), channel_id=1, source_target_pairs={{0,4},{4,0},{1,5},{5,1},{2,6},{6,2},{3,7},{7,3},{8,12},{12,8},{9,1... | collective-permute-start | bytes 1572872 | tf_op jit(solution)/shard_map/ppermute | solution.py:22
  32.0 1.5 %collective-permute-done.1 = bf16[32,64,128]{2,1,0:T(8,128)(2,1)S(1)} collective-permute-done((bf16[32,64,128]{2,1,0:T(8,128)(2,1)S(1)}, bf16[32,64,128]{2,1,0:T(8,128)(2,1)S(1)}, u32[]{:S(2)}, u32[]{:S(2)}) %collective-permute-start.1) | collective-permute-done | bytes 524320 | tf_op jit(solution)/shard_map/ppermute | solution.py:22
  33.7 6.3 %convolution_convert_fusion = bf16[128,1024]{1,0:T(8,128)(2,1)S(1)} fusion(bf16[4096,128]{1,0:T(8,128)(2,1)S(1)} %bitcast.33, bf16[1024,4096]{1,0:T(8,128)(2,1)} %param.11), kind=kOutput, calls=%fused_computation | convolution fusion | flops 1073872896 | bytes 9699328 | tf_op jit(solution)/shard_map/dot_general | solution.py:83
  40.1 1.1 broadcast_in_dim.11
  41.2 4.2 %all-to-all-start.1 = ((bf16[4,128,1024]{2,1,0:T(8,128)(2,1)}), bf16[4,128,1024]{2,1,0:T(8,128)(2,1)S(1)}, u32[]{:S(2)}, u32[]{:S(2)}) async-start(bf16[4,128,1024]{2,1,0:T(8,128)(2,1)} %broadcast_in_dim.11), calls=%async_computation.1 | async-start | bytes 2097152 | tf_op jit(solution)/shard_map/all_to_all | solution.py:16
  45.4 14.5 %all-to-all-done.1 = bf16[4,128,1024]{2,1,0:T(8,128)(2,1)S(1)} async-done(((bf16[4,128,1024]{2,1,0:T(8,128)(2,1)}), bf16[4,128,1024]{2,1,0:T(8,128)(2,1)S(1)}, u32[]{:S(2)}, u32[]{:S(2)}) %all-to-all-start.1) | async-done | bytes 1048608 | tf_op jit(solution)/shard_map/all_to_all | solution.py:16
  60.0 1.7 %fusion.21 = f32[256,512]{1,0:T(8,128)S(1)} fusion(bf16[256,1024]{1,0:T(8,128)(2,1)S(1)} %bitcast.35, bf16[1024,512]{1,0:T(8,128)(2,1)} %param.12), kind=kOutput, calls=%fused_computation.69 | convolution fusion | flops 268435456 | bytes 2097152 | tf_op jit(solution)/shard_map/dot_general | solution.py:88
  63.2 1.6 %collective-permute-start.2 = (bf16[256,768]{1,0:T(8,128)(2,1)S(1)}, bf16[256,768]{1,0:T(8,128)(2,1)}, u32[]{:S(2)}, u32[]{:S(2)}) collective-permute-start(bf16[256,768]{1,0:T(8,128)(2,1)S(1)} %pad_maximum_fusion.1), channel_id=1, source_target_pairs={{0,4},{4,0},{1,5},{5,1},{2,6},{6,2},{3,7},{7,3},{8,12},{12,8},{9,1... | collective-permute-start | bytes 1179656 | tf_op jit(solution)/shard_map/ppermute | solution.py:22
  64.8 1.0 constant_dynamic-slice_fusion.5
  66.3 1.8 %fusion.5 = bf16[32,8,768]{2,1,0:T(8,128)(2,1)} fusion(bf16[256,768]{1,0:T(8,128)(2,1)} %collective-permute-done.2, f32[256,512]{1,0:T(8,128)S(1)} %constant_dynamic-slice_fusion.4, f32[256,256]{1,0:T(8,128)S(1)} %constant_dynamic-slice_fusion.5), kind=kLoop, calls=%fused_computation.12 | loop fusion | flops 786432 | bytes 1572864 | tf_op jit(solution)/shard_map/reshape | solution.py:94
  68.2 4.4 %all-to-all-start.2 = ((bf16[32,8,768]{2,1,0:T(8,128)(2,1)}), bf16[32,8,768]{2,1,0:T(8,128)(2,1)S(1)}, u32[]{:S(2)}, u32[]{:S(2)}) async-start(bf16[32,8,768]{2,1,0:T(8,128)(2,1)} %fusion.5), calls=%async_computation.2 | async-start | bytes 786432 | tf_op jit(solution)/shard_map/all_to_all | solution.py:94
  75.6 10.8 %all-to-all-done.2 = bf16[32,8,768]{2,1,0:T(8,128)(2,1)S(1)} async-done(((bf16[32,8,768]{2,1,0:T(8,128)(2,1)}), bf16[32,8,768]{2,1,0:T(8,128)(2,1)S(1)}, u32[]{:S(2)}, u32[]{:S(2)}) %all-to-all-start.2) | async-done | bytes 393248 | tf_op jit(solution)/shard_map/all_to_all | solution.py:94
  87.3 5.0 %all-to-all-start.3 = ((bf16[32,8,768]{2,1,0:T(8,128)(2,1)}), bf16[32,8,768]{2,1,0:T(8,128)(2,1)S(1)}, u32[]{:S(2)}, u32[]{:S(2)}) async-start(bf16[32,8,768]{2,1,0:T(8,128)(2,1)} %broadcast_in_dim.12), calls=%async_computation.3 | async-start | bytes 786432 | tf_op jit(solution)/shard_map/all_to_all | solution.py:16
  92.3 1.8 %collective-permute-start.4 = (f32[8,768]{1,0:T(8,128)S(1)}, f32[8,768]{1,0:T(8,128)S(1)}, u32[]{:S(2)}, u32[]{:S(2)}) collective-permute-start(f32[8,768]{1,0:T(8,128)S(1)} %pad_maximum_fusion.2), channel_id=1, source_target_pairs={{0,4},{4,0},{1,5},{5,1},{2,6},{6,2},{3,7},{7,3},{8,12},{12,8},{9,1... | collective-permute-start | bytes 73736 | tf_op jit(solution)/shard_map/ppermute | solution.py:22
  94.1 11.0 %all-to-all-done.3 = bf16[32,8,768]{2,1,0:T(8,128)(2,1)S(1)} async-done(((bf16[32,8,768]{2,1,0:T(8,128)(2,1)}), bf16[32,8,768]{2,1,0:T(8,128)(2,1)S(1)}, u32[]{:S(2)}, u32[]{:S(2)}) %all-to-all-start.3) | async-done | bytes 393248 | tf_op jit(solution)/shard_map/all_to_all | solution.py:16
  105.1 3.5 %collective-permute-start.3 = (bf16[256,768]{1,0:T(8,128)(2,1)S(1)}, bf16[256,768]{1,0:T(8,128)(2,1)S(1)}, u32[]{:S(2)}, u32[]{:S(2)}) collective-permute-start(bf16[256,768]{1,0:T(8,128)(2,1)S(1)} %bitcast.36), channel_id=1, source_target_pairs={{0,4},{4,0},{1,5},{5,1},{2,6},{6,2},{3,7},{7,3},{8,12},{12,8},{9,1... | collective-permute-start | bytes 1179656 | tf_op jit(solution)/shard_map/ppermute | solution.py:22
  110.7 1.6 %multiply_reduce_fusion = (f32[]{:T(128)}, f32[1024,64]{0,1:T(8,128)S(1)}) fusion(bf16[64,256]{1,0:T(8,128)(2,1)} %param.15, bf16[256,512]{1,0:T(8,128)(2,1)S(1)} %slice.97, bf16[256,512]{1,0:T(8,128)(2,1)S(1)} %slice.96), kind=kOutput, calls=%fused_computation.21 | convolution fusion | flops 34734080 | bytes 819204 | tf_op jit(solution)/shard_map/dot_general | solution.py:111
  113.1 1.4 pad_maximum_fusion.9
  115.1 3.3 %all-to-all-start.4 = ((f32[8,1,2]{2,1,0:T(1,128)}), f32[8,1,2]{2,1,0:T(1,128)S(1)}, u32[]{:S(2)}, u32[]{:S(2)}) async-start(f32[8,1,2]{2,1,0:T(1,128)} %broadcast_in_dim.13), calls=%async_computation.4 | async-start | bytes 8192 | tf_op jit(solution)/shard_map/all_to_all | solution.py:16
  118.3 4.5 %all-to-all-done.4 = f32[8,1,2]{2,1,0:T(1,128)S(1)} async-done(((f32[8,1,2]{2,1,0:T(1,128)}), f32[8,1,2]{2,1,0:T(1,128)S(1)}, u32[]{:S(2)}, u32[]{:S(2)}) %all-to-all-start.4) | async-done | bytes 96 | tf_op jit(solution)/shard_map/all_to_all | solution.py:16
  123.5 3.9 %all-to-all-start.5 = ((f32[32,1,2]{2,1,0:T(1,128)}), f32[32,1,2]{2,1,0:T(1,128)S(1)}, u32[]{:S(2)}, u32[]{:S(2)}) async-start(f32[32,1,2]{2,1,0:T(1,128)} %broadcast_in_dim.14), calls=%async_computation.5 | async-start | bytes 32768 | tf_op jit(solution)/shard_map/all_to_all | solution.py:16
  127.9 7.9 %all-to-all-done.5 = f32[32,1,2]{2,1,0:T(1,128)S(1)} async-done(((f32[32,1,2]{2,1,0:T(1,128)}), f32[32,1,2]{2,1,0:T(1,128)S(1)}, u32[]{:S(2)}, u32[]{:S(2)}) %all-to-all-start.5) | async-done | bytes 288 | tf_op jit(solution)/shard_map/all_to_all | solution.py:16
  (62 shorter events, 13.1 us)
Async XLA Ops:
  0.6 61.8 %copy-start = (bf16[1024,1024]{1,0:T(8,128)(2,1)S(1)}, bf16[1024,1024]{1,0:T(8,128)(2,1)}, u32[]{:S(2)}) copy-start(bf16[1024,1024]{1,0:T(8,128)(2,1)} %param.13) | copy-start | bytes 6291460
  29.6 4.0 %collective-permute-start.1 = (bf16[32,64,128]{2,1,0:T(8,128)(2,1)S(1)}, bf16[32,64,128]{2,1,0:T(8,128)(2,1)S(1)}, u32[]{:S(2)}, u32[]{:S(2)}) collective-permute-start(bf16[32,64,128]{2,1,0:T(8,128)(2,1)S(1)} %all_to_all.30), channel_id=1, source_target_pairs={{0,4},{4,0},{1,5},{5,1},{2,6},{6,2},{3,7},{7,3},{8,12},{12,8},{9,1... | collective-permute-start | bytes 1572872 | tf_op jit(solution)/shard_map/ppermute | solution.py:22
  40.1 33.2 %copy-start.5 = (f32[4,1024]{1,0:T(4,128)S(1)}, f32[4,1024]{1,0:T(4,128)}, u32[]{:S(2)}) copy-start(f32[4,1024]{1,0:T(4,128)} %param.21) | copy-start | bytes 49156
  41.2 18.7 %all-to-all-start.1 = ((bf16[4,128,1024]{2,1,0:T(8,128)(2,1)}), bf16[4,128,1024]{2,1,0:T(8,128)(2,1)S(1)}, u32[]{:S(2)}, u32[]{:S(2)}) async-start(bf16[4,128,1024]{2,1,0:T(8,128)(2,1)} %broadcast_in_dim.11), calls=%async_computation.1 | async-start | bytes 2097152 | tf_op jit(solution)/shard_map/all_to_all | solution.py:16
  61.6 0.8 copy-start.1
  63.2 3.1 %collective-permute-start.2 = (bf16[256,768]{1,0:T(8,128)(2,1)S(1)}, bf16[256,768]{1,0:T(8,128)(2,1)}, u32[]{:S(2)}, u32[]{:S(2)}) collective-permute-start(bf16[256,768]{1,0:T(8,128)(2,1)S(1)} %pad_maximum_fusion.1), channel_id=1, source_target_pairs={{0,4},{4,0},{1,5},{5,1},{2,6},{6,2},{3,7},{7,3},{8,12},{12,8},{9,1... | collective-permute-start | bytes 1179656 | tf_op jit(solution)/shard_map/ppermute | solution.py:22
  65.9 46.4 %copy-start.4 = (bf16[64,256]{1,0:T(8,128)(2,1)S(1)}, bf16[64,256]{1,0:T(8,128)(2,1)}, u32[]{:S(2)}) copy-start(bf16[64,256]{1,0:T(8,128)(2,1)} %param.14) | copy-start | bytes 98308
  65.9 72.0 %copy-start.3 = (f32[64,512]{1,0:T(8,128)S(1)}, f32[64,512]{1,0:T(8,128)}, u32[]{:S(2)}) copy-start(f32[64,512]{1,0:T(8,128)} %param.16) | copy-start | bytes 393220
  65.9 72.7 %copy-start.2 = (f32[64,1024]{1,0:T(8,128)S(1)}, f32[64,1024]{1,0:T(8,128)}, u32[]{:S(2)}) copy-start(f32[64,1024]{1,0:T(8,128)} %param.17) | copy-start | bytes 786436
  68.2 18.2 %all-to-all-start.2 = ((bf16[32,8,768]{2,1,0:T(8,128)(2,1)}), bf16[32,8,768]{2,1,0:T(8,128)(2,1)S(1)}, u32[]{:S(2)}, u32[]{:S(2)}) async-start(bf16[32,8,768]{2,1,0:T(8,128)(2,1)} %fusion.5), calls=%async_computation.2 | async-start | bytes 786432 | tf_op jit(solution)/shard_map/all_to_all | solution.py:94
  74.0 1.6 %collective-permute-start = (f32[8,768]{1,0:T(8,128)S(1)}, f32[8,768]{1,0:T(8,128)S(1)}, u32[]{:S(2)}, u32[]{:S(2)}) collective-permute-start(f32[8,768]{1,0:T(8,128)S(1)} %maximum_maximum_fusion), channel_id=1, source_target_pairs={{0,4},{4,0},{1,5},{5,1},{2,6},{6,2},{3,7},{7,3},{8,12},{12,8},{9,1... | collective-permute-start | bytes 73736 | tf_op jit(solution)/shard_map/ppermute | solution.py:22
  87.3 17.8 %all-to-all-start.3 = ((bf16[32,8,768]{2,1,0:T(8,128)(2,1)}), bf16[32,8,768]{2,1,0:T(8,128)(2,1)S(1)}, u32[]{:S(2)}, u32[]{:S(2)}) async-start(bf16[32,8,768]{2,1,0:T(8,128)(2,1)} %broadcast_in_dim.12), calls=%async_computation.3 | async-start | bytes 786432 | tf_op jit(solution)/shard_map/all_to_all | solution.py:16
  92.3 16.3 %collective-permute-start.4 = (f32[8,768]{1,0:T(8,128)S(1)}, f32[8,768]{1,0:T(8,128)S(1)}, u32[]{:S(2)}, u32[]{:S(2)}) collective-permute-start(f32[8,768]{1,0:T(8,128)S(1)} %pad_maximum_fusion.2), channel_id=1, source_target_pairs={{0,4},{4,0},{1,5},{5,1},{2,6},{6,2},{3,7},{7,3},{8,12},{12,8},{9,1... | collective-permute-start | bytes 73736 | tf_op jit(solution)/shard_map/ppermute | solution.py:22
  105.1 5.5 %collective-permute-start.3 = (bf16[256,768]{1,0:T(8,128)(2,1)S(1)}, bf16[256,768]{1,0:T(8,128)(2,1)S(1)}, u32[]{:S(2)}, u32[]{:S(2)}) collective-permute-start(bf16[256,768]{1,0:T(8,128)(2,1)S(1)} %bitcast.36), channel_id=1, source_target_pairs={{0,4},{4,0},{1,5},{5,1},{2,6},{6,2},{3,7},{7,3},{8,12},{12,8},{9,1... | collective-permute-start | bytes 1179656 | tf_op jit(solution)/shard_map/ppermute | solution.py:22
  115.1 7.7 %all-to-all-start.4 = ((f32[8,1,2]{2,1,0:T(1,128)}), f32[8,1,2]{2,1,0:T(1,128)S(1)}, u32[]{:S(2)}, u32[]{:S(2)}) async-start(f32[8,1,2]{2,1,0:T(1,128)} %broadcast_in_dim.13), calls=%async_computation.4 | async-start | bytes 8192 | tf_op jit(solution)/shard_map/all_to_all | solution.py:16
  123.5 12.4 %all-to-all-start.5 = ((f32[32,1,2]{2,1,0:T(1,128)}), f32[32,1,2]{2,1,0:T(1,128)S(1)}, u32[]{:S(2)}, u32[]{:S(2)}) async-start(f32[32,1,2]{2,1,0:T(1,128)} %broadcast_in_dim.14), calls=%async_computation.5 | async-start | bytes 32768 | tf_op jit(solution)/shard_map/all_to_all | solution.py:16

commit v2 on v1

v2 whole, which is shorter than its diff:
```python
import functools

import jax
import jax.numpy as jnp
from jax import lax
from jax.experimental import pallas as pl
from jax.experimental.pallas import tpu as pltpu
from jax.sharding import Mesh
from jax.sharding import PartitionSpec as P


FS = ("z", "x", "c")
PLANE = ("z", "x")
SWAP = [(0, 1), (1, 0)]
BF = jnp.bfloat16
F32 = jnp.float32
VMEM = pl.BlockSpec(memory_space=pltpu.VMEM)


def spread(shard, axes):
    peers = lax.axis_size(axes)
    return lax.all_to_all(
        jnp.broadcast_to(shard[None], (peers, *shard.shape)), axes, 0, 0, tiled=True
    )


def other_core(a):
    return lax.ppermute(a, "c", SWAP)


def shape(dims, dtype=F32):
    return jax.ShapeDtypeStruct(dims, dtype)


def local(body, outs, flops=0, mib=16):
    def call(*arrays):
        return pl.pallas_call(
            body,
            out_shape=outs,
            in_specs=[VMEM] * len(arrays),
            out_specs=(VMEM,) * len(outs) if isinstance(outs, tuple) else VMEM,
            compiler_params=pltpu.CompilerParams(vmem_limit_bytes=mib << 20),
            cost_estimate=pl.CostEstimate(
                flops=max(flops, 1 << 20), bytes_accessed=1 << 20, transcendentals=0
            ),
        )(*arrays)

    return call


BLOCKS = 8


def mapped_body(x_ref, own_ref, other_ref, out_ref, held, basis, sems):
    block = held.shape[1]

    def load(i):
        return pltpu.make_async_copy(
            x_ref.at[pl.ds(i * block, block)], held.at[i], sems.at[i]
        )

    for i in range(BLOCKS):
        load(i).start()
    first = lax.axis_index("c") == 0
    own, other = own_ref[...], other_ref[...]
    basis[:, 0] = jnp.where(first, own, other)
    basis[:, 1] = jnp.where(first, other, own)
    whole = basis[...].reshape(x_ref.shape[1], -1)
    for i in range(BLOCKS):
        load(i).wait()
        m = jnp.dot(held[i], whole, preferred_element_type=F32).T.astype(BF)
        for k in range(out_ref.shape[0]):
            out_ref[k, :, i * block : (i + 1) * block] = m


def mapped_kernel(inputs, own, other, tp_size):
    tok, depth = inputs.shape
    planes, rows, quarter = own.shape
    return pl.pallas_call(
        mapped_body,
        out_shape=shape((tp_size, quarter, tok), BF),
        in_specs=[pl.BlockSpec(memory_space=pltpu.HBM), VMEM, VMEM],
        out_specs=VMEM,
        scratch_shapes=[
            pltpu.VMEM((BLOCKS, tok // BLOCKS, depth), BF),
            pltpu.VMEM((planes, 2, rows, quarter), BF),
            pltpu.SemaphoreType.DMA((BLOCKS,)),
        ],
        name="mapped",
        compiler_params=pltpu.CompilerParams(vmem_limit_bytes=48 << 20),
        cost_estimate=pl.CostEstimate(
            flops=4 * tok * depth * quarter, bytes_accessed=2 * tok * depth, transcendentals=0
        ),
    )(inputs, own, other)


def part_body(mine, m_ref, k_ref, v_ref, out_ref):
    c = lax.axis_index("c")
    side = c if mine else 1 - c
    rank = m_ref.shape[0] // 2
    kw, vw = k_ref.shape[1] // 2, v_ref.shape[1] // 2
    kc = k_ref[:, pl.ds(pl.multiple_of(side * kw, 128), kw)]
    vc = v_ref[:, pl.ds(pl.multiple_of(side * vw, 128), vw)]
    out_ref[:, :kw] = jnp.dot(m_ref[:rank], kc, preferred_element_type=F32).astype(out_ref.dtype)
    out_ref[:, kw:] = jnp.dot(m_ref[rank:], vc, preferred_element_type=F32).astype(out_ref.dtype)


def stats_body(km, kv, vm, vv, kb, vb, mine, theirs, rows_kb, rows_vb):
    c = lax.axis_index("c")
    rows = km.shape[0]
    kw, vw = km.shape[1] // 2, vm.shape[1] // 2
    for out, side in ((mine, c), (theirs, 1 - c)):
        ks, vs = (pl.ds(pl.multiple_of(side * w, 128), w) for w in (kw, vw))
        out[:rows, :kw] = km[:, ks]
        out[:rows, kw:] = vm[:, vs]
        out[rows:, :kw] = kv[:, ks]
        out[rows:, kw:] = vv[:, vs]
    rows_kb[...] = kb[...]
    rows_vb[...] = vb[...]


def moments_body(arrived, mine, theirs, dirs, own_new, back):
    first = lax.axis_index("c") == 0
    rows = mine.shape[0] // 2
    proj = jnp.sum(arrived[...].astype(F32), axis=0)

    def both(at):
        own, other = mine[at : at + rows], theirs[at : at + rows]
        low = jnp.where(first, own, other)
        high = jnp.where(first, other, own)
        return jnp.concatenate([low, high], axis=0)

    mean_new = 0.8 * both(0) + 0.2 * proj
    var_new = 0.9 * both(rows) + 0.1 * proj * proj
    d = (mean_new / (jnp.sqrt(var_new) + 1e-08)).astype(BF)
    dirs[...] = jnp.broadcast_to(d[None], dirs.shape)
    for at, new in ((0, mean_new), (rows, var_new)):
        low, high = new[:rows], new[rows:]
        own_new[at : at + rows] = jnp.where(first, low, high)
        back[at : at + rows] = jnp.where(first, high, low)


def placed_body(own, back, km, kv, vm, vv):
    c = lax.axis_index("c")
    rows = km.shape[0]
    kw, vw = km.shape[1] // 2, vm.shape[1] // 2
    for src, side in ((own, c), (back, 1 - c)):
        ks, vs = (pl.ds(pl.multiple_of(side * w, 128), w) for w in (kw, vw))
        km[:, ks] = src[:rows, :kw]
        vm[:, vs] = src[:rows, kw:]
        kv[:, ks] = src[rows:, :kw]
        vv[:, vs] = src[rows:, kw:]


def gram_body(own, other, own_y, other_y, out):
    first = lax.axis_index("tp") % 2 == 0
    mine = jnp.concatenate([own[...], other[...]], axis=0)
    theirs = jnp.concatenate([own_y[...], other_y[...]], axis=0)
    low = jnp.where(first, mine, theirs)
    high = jnp.where(first, theirs, mine)
    cols = jnp.concatenate([low, high], axis=1)
    out[...] = lax.dot_general(
        cols, cols, (((0,), (0,)), ((), ())), preferred_element_type=F32
    )


def update_body(own, other, kb, vb, gram, gram_y, key_up, value_up, sums):
    c, t = lax.axis_index("c"), lax.axis_index("tp")
    kw, vw = key_up.shape[1] // 2, value_up.shape[1] // 2
    is_key = t < 2
    key_gram = jnp.where(is_key, gram[...], gram_y[...])
    value_gram = jnp.where(is_key, gram_y[...], gram[...])

    def pieces(g):
        a = g.astype(BF)
        r = g - a.astype(F32)
        b = r.astype(BF)
        return a, b, (r - b.astype(F32)).astype(BF)

    def square(ps, d):
        gd = sum(jnp.dot(p, d, preferred_element_type=F32) for p in ps)
        return jnp.sum(gd * d.astype(F32), axis=0, keepdims=True)

    kp, vp = pieces(key_gram), pieces(value_gram)
    ksq = jnp.zeros((1, kw), F32)
    vsq = jnp.zeros((1, vw), F32)
    for src, side in ((own, c), (other, 1 - c)):
        dk, dv = src[:, :kw], src[:, kw:]
        ks, vs = (pl.ds(pl.multiple_of(side * w, 128), w) for w in (kw, vw))
        key_up[:, ks] = jnp.dot(kb[...], dk, preferred_element_type=F32)
        value_up[:, vs] = jnp.dot(vb[...], dv, preferred_element_type=F32)
        ksq += square(kp, dk)
        vsq += square(vp, dv)
    lane = lax.broadcasted_iota(jnp.int32, sums.shape, 1)
    sums[...] = jnp.where(lane == 0, jnp.sum(ksq), jnp.where(lane == 1, jnp.sum(vsq), 0.0))


def finish_body(counts, s0, s1, s2, s3, ku, vu, kw, vw, kn, vn, kc, vc):
    total = (s0[...] + s1[...]) + (s2[...] + s3[...])
    for lane, u, w, n, b in ((0, ku, kw, kn, kc), (1, vu, vw, vn, vc)):
        mean = total[:, lane : lane + 1] / counts[lane]
        factor = jnp.minimum(1.0, 0.5 * lax.rsqrt(mean + 1e-06))
        new = w[...] - 0.25 * factor * u[...]
        n[...] = new
        b[...] = new.astype(BF)


def step(
    inputs,
    key_cot,
    value_cot,
    key_basis,
    value_basis,
    key_weight,
    value_weight,
    key_mean,
    key_var,
    value_mean,
    value_var,
):
    t = lax.axis_index("tp")
    planes = lax.axis_size(PLANE)
    tp_size = lax.axis_size("tp")
    devices = lax.axis_size(FS) * tp_size
    moments = (key_mean, key_var, value_mean, value_var)
    rank = key_basis.shape[1]
    width = (key_cot.shape[1] + value_cot.shape[1]) // 2
    two_rows = 2 * key_mean.shape[0]

    both = jnp.concatenate([key_basis, value_basis], axis=1)
    quarter = both.shape[1] // tp_size
    own = spread(lax.dynamic_slice_in_dim(both, t * quarter, quarter, axis=1), PLANE)
    other = other_core(own)
    mapped = mapped_kernel(inputs, own, other, tp_size)
    mapped = lax.all_to_all(mapped, "tp", 0, 0, tiled=True)
    mapped, own, other = lax.optimization_barrier((mapped, own, other))
    mapped = mapped.reshape(-1, inputs.shape[0])

    flops = mapped.size * 2 * width // 2
    theirs = local(
        functools.partial(part_body, False), shape((rank, width), BF), flops
    )(mapped, key_cot, value_cot)
    got = other_core(theirs)
    ours = local(functools.partial(part_body, True), shape((rank, width)), flops)(
        mapped, key_cot, value_cot
    )
    pair = (ours + got.astype(F32)).astype(BF)

    beside = [(i, i ^ 1) for i in range(tp_size)]
    across = [(i, tp_size - 1 - i) for i in range(tp_size)]
    own_y = lax.ppermute(own, "tp", beside)
    other_y = lax.ppermute(other, "tp", beside)

    stat = shape((two_rows, width))
    mine, theirs, key_rows, value_rows = local(
        stats_body, (stat, stat, shape(key_basis.shape, BF), shape(value_basis.shape, BF))
    )(*moments, key_basis, value_basis)
    stats = other_core(theirs)
    arrived = lax.all_to_all(pair.reshape(planes, -1, width), PLANE, 0, 0, tiled=True)
    dirs, own_new, back = local(
        moments_body, (shape(arrived.shape, BF), stat, stat)
    )(arrived, mine, stats)
    own_dir = lax.all_to_all(dirs, PLANE, 0, 0, tiled=True).reshape(rank, width)

    flat = [a.reshape(-1, quarter) for a in (own, other, own_y, other_y)]
    gram = local(gram_body, shape((rank, rank)), 4 * flat[0].size * rank)(*flat)
    gram_y = lax.ppermute(gram, "tp", across)
    new_moments = local(placed_body, tuple(shape(a.shape) for a in moments))(
        own_new, other_core(back)
    )

    key_up, value_up, sums = local(
        update_body,
        (shape(key_weight.shape), shape(value_weight.shape), shape((1, 128))),
        8 * rank * rank * width,
    )(own_dir, other_core(own_dir), key_rows, value_rows, gram, gram_y)
    sums = [sums] + [
        lax.ppermute(sums, "tp", [(i, (i + k) % tp_size) for i in range(tp_size)])
        for k in range(1, tp_size)
    ]
    counts = (float(key_weight.size * devices), float(value_weight.size * devices))
    key_new, value_new, key_copy, value_copy = local(
        functools.partial(finish_body, counts),
        (
            shape(key_weight.shape),
            shape(value_weight.shape),
            shape(key_weight.shape, BF),
            shape(value_weight.shape, BF),
        ),
    )(*sums, key_up, value_up, key_weight, value_weight)
    key_mean_new, key_var_new, value_mean_new, value_var_new = new_moments
    return (
        key_new,
        value_new,
        key_copy,
        value_copy,
        key_mean_new,
        key_var_new,
        value_mean_new,
        value_var_new,
    )


def solution(mesh):
    split = Mesh(mesh.devices.reshape(8, 4, 2, mesh.shape["tp"]), ("z", "x", "c", "tp"))
    rows, tiles = P(FS, None), P(FS, "tp")
    return jax.shard_map(
        step,
        mesh=split,
        in_specs=(rows, tiles, tiles, rows, rows) + (tiles,) * 6,
        out_specs=(tiles,) * 8,
        check_vma=False,
    )
```

time: 140 us -> 128 us (0.914)
  the two profiles are of different devices: /device:TPU:1 before, /device:TPU:2 now
where the time goes in v2:
time: 128 us
  blocking collectives  48 us (38%)
  waiting for transfers between devices  47.5 us (37%)
  starting transfers between devices  18 us (14%)
  Pallas kernels  10.7 us (8%)
  other arithmetic  1.71 us (1%)
    all_to_all x1, blocking collectives, spread(): lax.all_to_all(jnp.broadcast_to(shard[None], (peers, *shard.shape)), axes...  28.2 us
    all_to_all x1, blocking collectives, step(): mapped = lax.all_to_all(mapped, 'tp', 0, 0, tiled=True)  19.8 us
    all_to_all x1, waiting for transfers between devices, step(): lax.all_to_all(pair.reshape(planes, -1, width), PLANE, 0, 0, tiled=True)  12.9 us
    all_to_all x1, waiting for transfers between devices, step(): own_dir = lax.all_to_all(dirs, PLANE, 0, 0, tiled=True).reshape(rank, width)  11.2 us
    ppermute x1, waiting for transfers between devices, step(): other_y = lax.ppermute(other, 'tp', beside)  8.81 us
    ppermute x1, waiting for transfers between devices, step(): gram_y = lax.ppermute(gram, 'tp', across)  6.41 us
    all_to_all x1, starting transfers between devices, step(): lax.all_to_all(pair.reshape(planes, -1, width), PLANE, 0, 0, tiled=True)  5.59 us
    all_to_all x1, starting transfers between devices, step(): own_dir = lax.all_to_all(dirs, PLANE, 0, 0, tiled=True).reshape(rank, width)  5.57 us
  transfers between devices with their start and end apart: 13, of which 11 were waited for; matrix products, arithmetic and copies ran while one was open for 0% of the time, Pallas kernels for 2%

profile of v2, /device:TPU:2, one launch (start us, length us, event | category | flops | bytes accessed | tf_op | source)
XLA Modules:
  0.0 127.9 jit_solution(4601624035786113550)
XLA Ops:
  0.7 0.9 fusion.1
  1.7 28.2 %all_to_all.20.own_ref = bf16[32,64,128]{2,1,0:T(8,128)(2,1)S(1)} all-to-all(bf16[32,64,128]{2,1,0:T(8,128)(2,1)S(1)} %broadcast_in_dim.2), channel_id=1, replica_groups=mesh['z'=8,'x'=4,'c'=2,'tp'=4] {'z','x'}, dimensions={0} | all-to-all | bytes 1048576 | tf_op jit(solution)/shard_map/all_to_all | solution.py:22
  29.9 1.9 %collective-permute-done.other_ref = bf16[32,64,128]{2,1,0:T(8,128)(2,1)S(1)} collective-permute-done((bf16[32,64,128]{2,1,0:T(8,128)(2,1)S(1)}, bf16[32,64,128]{2,1,0:T(8,128)(2,1)S(1)}, u32[]{:S(2)}, u32[]{:S(2)}) %collective-permute-start) | collective-permute-done | bytes 524320 | tf_op jit(solution)/shard_map/ppermute | solution.py:28
  31.8 5.3 %mapped.1 = bf16[4,128,1024]{2,1,0:T(8,128)(2,1)S(1)} custom-call(bf16[1024,4096]{1,0:T(8,128)(2,1)} %x_ref.1, bf16[32,64,128]{2,1,0:T(8,128)(2,1)S(1)} %all_to_all.20.own_ref, bf16[32,64,128]{2,1,0:T(8,128)(2,1)S(1)} %collective-permute-done.other_ref), custom_call_target="tpu_custom_call" | custom-call | flops 2147483648 | bytes 8388608 | tf_op jit(solution)/shard_map/mapped/pallas_call | solution.py:79
  37.2 19.8 %all_to_all.21 = bf16[4,128,1024]{2,1,0:T(8,128)(2,1)S(1)} all-to-all(bf16[4,128,1024]{2,1,0:T(8,128)(2,1)S(1)} %mapped.1), channel_id=1, replica_groups=mesh['z'=8,'x'=4,'c'=2,'tp'=4] {'tp'}, dimensions={0} | all-to-all | bytes 2097152 | tf_op jit(solution)/shard_map/all_to_all | solution.py:235
  58.3 1.1 collective-permute-done.1
  59.4 0.8 fusion
  60.2 5.6 %all-to-all-start.2 = ((bf16[32,8,768]{2,1,0:T(8,128)(2,1)}), bf16[32,8,768]{2,1,0:T(8,128)(2,1)S(1)}, u32[]{:S(2)}, u32[]{:S(2)}) async-start(bf16[32,8,768]{2,1,0:T(8,128)(2,1)} %fusion), calls=%async_computation.2 | async-start | bytes 786432 | tf_op jit(solution)/shard_map/all_to_all | solution.py:259
  66.0 1.2 collective-permute-done.2.theirs
  67.2 12.9 %all-to-all-done.2.arrived = bf16[32,8,768]{2,1,0:T(8,128)(2,1)S(1)} async-done(((bf16[32,8,768]{2,1,0:T(8,128)(2,1)}), bf16[32,8,768]{2,1,0:T(8,128)(2,1)S(1)}, u32[]{:S(2)}, u32[]{:S(2)}) %all-to-all-start.2) | async-done | bytes 393248 | tf_op jit(solution)/shard_map/all_to_all | solution.py:259
  80.1 0.9 shard_map.173
  81.0 5.6 %all-to-all-start.3 = ((bf16[32,8,768]{2,1,0:T(8,128)(2,1)}), bf16[32,8,768]{2,1,0:T(8,128)(2,1)S(1)}, u32[]{:S(2)}, u32[]{:S(2)}) async-start(bf16[32,8,768]{2,1,0:T(8,128)(2,1)} %get-tuple-element.32), calls=%async_computation.3 | async-start | bytes 786432 | tf_op jit(solution)/shard_map/all_to_all | solution.py:263
  87.2 1.5 %collective-permute-start.5 = (bf16[32,64,128]{2,1,0:T(8,128)(2,1)S(1)}, bf16[32,64,128]{2,1,0:T(8,128)(2,1)S(1)}, u32[]{:S(2)}, u32[]{:S(2)}) collective-permute-start(bf16[32,64,128]{2,1,0:T(8,128)(2,1)S(1)} %collective-permute-done.other_ref), channel_id=1, source_target_pairs={{0,1},{1,0},{2,3},{3,2},{4,5},{5,4},{6,7},{7,6},{8,9},{9,8},{10,11... | collective-permute-start | bytes 1572872 | tf_op jit(solution)/shard_map/ppermute | solution.py:252
  88.7 11.2 %all-to-all-done.3 = bf16[32,8,768]{2,1,0:T(8,128)(2,1)S(1)} async-done(((bf16[32,8,768]{2,1,0:T(8,128)(2,1)}), bf16[32,8,768]{2,1,0:T(8,128)(2,1)S(1)}, u32[]{:S(2)}, u32[]{:S(2)}) %all-to-all-start.3) | async-done | bytes 393248 | tf_op jit(solution)/shard_map/all_to_all | solution.py:263
  99.9 1.6 %collective-permute-done.4 = bf16[32,64,128]{2,1,0:T(8,128)(2,1)S(1)} collective-permute-done((bf16[32,64,128]{2,1,0:T(8,128)(2,1)S(1)}, bf16[32,64,128]{2,1,0:T(8,128)(2,1)S(1)}, u32[]{:S(2)}, u32[]{:S(2)}) %collective-permute-start.4) | collective-permute-done | bytes 524320 | tf_op jit(solution)/shard_map/ppermute | solution.py:251
  101.5 8.8 %collective-permute-done.5 = bf16[32,64,128]{2,1,0:T(8,128)(2,1)S(1)} collective-permute-done((bf16[32,64,128]{2,1,0:T(8,128)(2,1)S(1)}, bf16[32,64,128]{2,1,0:T(8,128)(2,1)S(1)}, u32[]{:S(2)}, u32[]{:S(2)}) %collective-permute-start.5) | collective-permute-done | bytes 524320 | tf_op jit(solution)/shard_map/ppermute | solution.py:252
  111.0 1.3 collective-permute-start.6
  112.3 6.4 %collective-permute-done.6.gram_y = f32[256,256]{1,0:T(8,128)S(1)} collective-permute-done((f32[256,256]{1,0:T(8,128)S(1)}, f32[256,256]{1,0:T(8,128)S(1)}, u32[]{:S(2)}, u32[]{:S(2)}) %collective-permute-start.6) | collective-permute-done | bytes 262176 | tf_op jit(solution)/shard_map/ppermute | solution.py:267
  118.7 1.1 shard_map.175
  119.9 2.6 %collective-permute-start.8 = (f32[1,128]{1,0:T(1,128)S(1)}, f32[1,128]{1,0:T(1,128)S(1)}, u32[]{:S(2)}, u32[]{:S(2)}) collective-permute-start(f32[1,128]{1,0:T(1,128)S(1)} %get-tuple-element.37.s0), channel_id=1, source_target_pairs={{0,2},{1,3},{2,0},{3,1},{4,6},{5,7},{6,4},{7,5},{8,10},{9,11},{10,... | collective-permute-start | bytes 1544 | tf_op jit(solution)/shard_map/ppermute | solution.py:278
  123.7 0.9 collective-permute-done.7.s1
  125.0 1.0 collective-permute-done.9.s3
  126.1 0.9 copy-done.5
  127.0 0.9 shard_map.176
  (36 shorter events, 4.7 us)
Async XLA Ops:
  0.6 56.3 %copy-start = (bf16[1024,1024]{1,0:T(8,128)(2,1)S(1)}, bf16[1024,1024]{1,0:T(8,128)(2,1)}, u32[]{:S(2)}) copy-start(bf16[1024,1024]{1,0:T(8,128)(2,1)} %v_ref.3) | copy-start | bytes 6291460
  0.6 56.3 %copy-start.1 = (bf16[1024,512]{1,0:T(8,128)(2,1)S(1)}, bf16[1024,512]{1,0:T(8,128)(2,1)}, u32[]{:S(2)}) copy-start(bf16[1024,512]{1,0:T(8,128)(2,1)} %k_ref.3) | copy-start | bytes 3145732
  29.9 1.9 %collective-permute-start = (bf16[32,64,128]{2,1,0:T(8,128)(2,1)S(1)}, bf16[32,64,128]{2,1,0:T(8,128)(2,1)S(1)}, u32[]{:S(2)}, u32[]{:S(2)}) collective-permute-start(bf16[32,64,128]{2,1,0:T(8,128)(2,1)S(1)} %all_to_all.20.own_ref), channel_id=1, source_target_pairs={{0,4},{4,0},{1,5},{5,1},{2,6},{6,2},{3,7},{7,3},{8,12},{12,8},{9,1... | collective-permute-start | bytes 1572872 | tf_op jit(solution)/shard_map/ppermute | solution.py:28
  37.1 28.7 %copy-start.3 = (bf16[64,256]{1,0:T(8,128)(2,1)S(1)}, bf16[64,256]{1,0:T(8,128)(2,1)}, u32[]{:S(2)}) copy-start(bf16[64,256]{1,0:T(8,128)(2,1)} %kb.1) | copy-start | bytes 98308
  37.1 28.7 %copy-start.4 = (bf16[64,256]{1,0:T(8,128)(2,1)S(1)}, bf16[64,256]{1,0:T(8,128)(2,1)}, u32[]{:S(2)}) copy-start(bf16[64,256]{1,0:T(8,128)(2,1)} %vb.1) | copy-start | bytes 98308
  37.2 28.7 %copy-start.6 = (f32[4,1024]{1,0:T(4,128)S(1)}, f32[4,1024]{1,0:T(4,128)}, u32[]{:S(2)}) copy-start(f32[4,1024]{1,0:T(4,128)} %vm.1) | copy-start | bytes 49156
  37.2 28.7 %copy-start.7 = (f32[4,1024]{1,0:T(4,128)S(1)}, f32[4,1024]{1,0:T(4,128)}, u32[]{:S(2)}) copy-start(f32[4,1024]{1,0:T(4,128)} %vv.1) | copy-start | bytes 49156
  37.2 28.7 %copy-start.8 = (f32[4,512]{1,0:T(4,128)S(1)}, f32[4,512]{1,0:T(4,128)}, u32[]{:S(2)}) copy-start(f32[4,512]{1,0:T(4,128)} %km.1) | copy-start | bytes 24580
  37.2 28.7 %copy-start.9 = (f32[4,512]{1,0:T(4,128)S(1)}, f32[4,512]{1,0:T(4,128)}, u32[]{:S(2)}) copy-start(f32[4,512]{1,0:T(4,128)} %kv.1) | copy-start | bytes 24580
  57.0 69.1 %copy-start.2 = (f32[64,1024]{1,0:T(8,128)S(1)}, f32[64,1024]{1,0:T(8,128)}, u32[]{:S(2)}) copy-start(f32[64,1024]{1,0:T(8,128)} %vw.1) | copy-start | bytes 786436
  57.6 1.8 %collective-permute-start.1 = (bf16[256,768]{1,0:T(8,128)(2,1)S(1)}, bf16[256,768]{1,0:T(8,128)(2,1)S(1)}, u32[]{:S(2)}, u32[]{:S(2)}) collective-permute-start(bf16[256,768]{1,0:T(8,128)(2,1)S(1)} %shard_map.171), channel_id=1, source_target_pairs={{0,4},{4,0},{1,5},{5,1},{2,6},{6,2},{3,7},{7,3},{8,12},{12,8},{9,1... | collective-permute-start | bytes 1179656 | tf_op jit(solution)/shard_map/ppermute | solution.py:28
  60.2 19.9 %all-to-all-start.2 = ((bf16[32,8,768]{2,1,0:T(8,128)(2,1)}), bf16[32,8,768]{2,1,0:T(8,128)(2,1)S(1)}, u32[]{:S(2)}, u32[]{:S(2)}) async-start(bf16[32,8,768]{2,1,0:T(8,128)(2,1)} %fusion), calls=%async_computation.2 | async-start | bytes 786432 | tf_op jit(solution)/shard_map/all_to_all | solution.py:259
  65.9 1.3 %collective-permute-start.2 = (f32[8,768]{1,0:T(8,128)S(1)}, f32[8,768]{1,0:T(8,128)S(1)}, u32[]{:S(2)}, u32[]{:S(2)}) collective-permute-start(f32[8,768]{1,0:T(8,128)S(1)} %get-tuple-element.31), channel_id=1, source_target_pairs={{0,4},{4,0},{1,5},{5,1},{2,6},{6,2},{3,7},{7,3},{8,12},{12,8},{9,1... | collective-permute-start | bytes 73736 | tf_op jit(solution)/shard_map/ppermute | solution.py:28
  81.0 18.9 %all-to-all-start.3 = ((bf16[32,8,768]{2,1,0:T(8,128)(2,1)}), bf16[32,8,768]{2,1,0:T(8,128)(2,1)S(1)}, u32[]{:S(2)}, u32[]{:S(2)}) async-start(bf16[32,8,768]{2,1,0:T(8,128)(2,1)} %get-tuple-element.32), calls=%async_computation.3 | async-start | bytes 786432 | tf_op jit(solution)/shard_map/all_to_all | solution.py:263
  86.6 14.9 %collective-permute-start.4 = (bf16[32,64,128]{2,1,0:T(8,128)(2,1)S(1)}, bf16[32,64,128]{2,1,0:T(8,128)(2,1)S(1)}, u32[]{:S(2)}, u32[]{:S(2)}) collective-permute-start(bf16[32,64,128]{2,1,0:T(8,128)(2,1)S(1)} %all_to_all.20.own_ref), channel_id=1, source_target_pairs={{0,1},{1,0},{2,3},{3,2},{4,5},{5,4},{6,7},{7,6},{8,9},{9,8},{10,11... | collective-permute-start | bytes 1572872 | tf_op jit(solution)/shard_map/ppermute | solution.py:251
  87.2 23.0 %collective-permute-start.5 = (bf16[32,64,128]{2,1,0:T(8,128)(2,1)S(1)}, bf16[32,64,128]{2,1,0:T(8,128)(2,1)S(1)}, u32[]{:S(2)}, u32[]{:S(2)}) collective-permute-start(bf16[32,64,128]{2,1,0:T(8,128)(2,1)S(1)} %collective-permute-done.other_ref), channel_id=1, source_target_pairs={{0,1},{1,0},{2,3},{3,2},{4,5},{5,4},{6,7},{7,6},{8,9},{9,8},{10,11... | collective-permute-start | bytes 1572872 | tf_op jit(solution)/shard_map/ppermute | solution.py:252
  99.9 18.8 %collective-permute-start.3 = (bf16[256,768]{1,0:T(8,128)(2,1)S(1)}, bf16[256,768]{1,0:T(8,128)(2,1)S(1)}, u32[]{:S(2)}, u32[]{:S(2)}) collective-permute-start(bf16[256,768]{1,0:T(8,128)(2,1)S(1)} %bitcast.14), channel_id=1, source_target_pairs={{0,4},{4,0},{1,5},{5,1},{2,6},{6,2},{3,7},{7,3},{8,12},{12,8},{9,1... | collective-permute-start | bytes 1179656 | tf_op jit(solution)/shard_map/ppermute | solution.py:28
  111.0 7.7 %collective-permute-start.6 = (f32[256,256]{1,0:T(8,128)S(1)}, f32[256,256]{1,0:T(8,128)S(1)}, u32[]{:S(2)}, u32[]{:S(2)}) collective-permute-start(f32[256,256]{1,0:T(8,128)S(1)} %shard_map.174.gram), channel_id=1, source_target_pairs={{0,3},{1,2},{2,1},{3,0},{4,7},{5,6},{6,5},{7,4},{8,11},{9,10},{10,... | collective-permute-start | bytes 786440 | tf_op jit(solution)/shard_map/ppermute | solution.py:267
  112.3 10.8 %collective-permute-start.10 = (f32[8,768]{1,0:T(8,128)S(1)}, f32[8,768]{1,0:T(8,128)S(1)}, u32[]{:S(2)}, u32[]{:S(2)}) collective-permute-start(f32[8,768]{1,0:T(8,128)S(1)} %get-tuple-element.45), channel_id=1, source_target_pairs={{0,4},{4,0},{1,5},{5,1},{2,6},{6,2},{3,7},{7,3},{8,12},{12,8},{9,1... | collective-permute-start | bytes 73736 | tf_op jit(solution)/shard_map/ppermute | solution.py:28
  119.8 4.9 %collective-permute-start.7 = (f32[1,128]{1,0:T(1,128)S(1)}, f32[1,128]{1,0:T(1,128)S(1)}, u32[]{:S(2)}, u32[]{:S(2)}) collective-permute-start(f32[1,128]{1,0:T(1,128)S(1)} %get-tuple-element.37.s0), channel_id=1, source_target_pairs={{0,1},{1,2},{2,3},{3,0},{4,5},{5,6},{6,7},{7,4},{8,9},{9,10},{10,1... | collective-permute-start | bytes 1544 | tf_op jit(solution)/shard_map/ppermute | solution.py:278
  119.9 5.2 %collective-permute-start.8 = (f32[1,128]{1,0:T(1,128)S(1)}, f32[1,128]{1,0:T(1,128)S(1)}, u32[]{:S(2)}, u32[]{:S(2)}) collective-permute-start(f32[1,128]{1,0:T(1,128)S(1)} %get-tuple-element.37.s0), channel_id=1, source_target_pairs={{0,2},{1,3},{2,0},{3,1},{4,6},{5,7},{6,4},{7,5},{8,10},{9,11},{10,... | collective-permute-start | bytes 1544 | tf_op jit(solution)/shard_map/ppermute | solution.py:278
  122.5 3.6 %collective-permute-start.9 = (f32[1,128]{1,0:T(1,128)S(1)}, f32[1,128]{1,0:T(1,128)S(1)}, u32[]{:S(2)}, u32[]{:S(2)}) collective-permute-start(f32[1,128]{1,0:T(1,128)S(1)} %get-tuple-element.37.s0), channel_id=1, source_target_pairs={{0,3},{1,0},{2,1},{3,2},{4,7},{5,4},{6,5},{7,6},{8,11},{9,8},{10,9... | collective-permute-start | bytes 1544 | tf_op jit(solution)/shard_map/ppermute | solution.py:278
  126.1 0.9 copy-start.5

commit v3 on v2

--- a/solution.py
+++ b/solution.py
@@ -48,55 +48,61 @@
     return call
 
 
-BLOCKS = 8
-
-
-def mapped_body(x_ref, own_ref, other_ref, out_ref, held, basis, sems):
-    block = held.shape[1]
+PIECES = 4
+
+
+def mapped_body(start, fresh, *refs):
+    if fresh:
+        x_ref, own_ref, other_ref, out_ref, basis, held, sems = refs
+    else:
+        x_ref, basis, out_ref, held, sems = refs
+    tok, piece = held.shape[1:]
 
     def load(i):
         return pltpu.make_async_copy(
-            x_ref.at[pl.ds(i * block, block)], held.at[i], sems.at[i]
+            x_ref.at[pl.ds(start, tok), pl.ds(i * piece, piece)], held.at[i], sems.at[i]
         )
 
-    for i in range(BLOCKS):
+    for i in range(PIECES):
         load(i).start()
-    first = lax.axis_index("c") == 0
-    own, other = own_ref[...], other_ref[...]
-    basis[:, 0] = jnp.where(first, own, other)
-    basis[:, 1] = jnp.where(first, other, own)
-    whole = basis[...].reshape(x_ref.shape[1], -1)
-    for i in range(BLOCKS):
+    if fresh:
+        first = lax.axis_index("c") == 0
+        planes, rows, quarter = own_ref.shape
+        own, other = own_ref[...], other_ref[...]
+        low = jnp.where(first, own, other)
+        high = jnp.where(first, other, own)
+        basis[...] = jnp.stack([low, high], axis=1).reshape(2 * planes * rows, quarter)
+    total = jnp.zeros((tok, out_ref.shape[0]), F32)
+    for i in range(PIECES):
         load(i).wait()
-        m = jnp.dot(held[i], whole, preferred_element_type=F32).T.astype(BF)
-        for k in range(out_ref.shape[0]):
-            out_ref[k, :, i * block : (i + 1) * block] = m
-
-
-def mapped_kernel(inputs, own, other, tp_size):
-    tok, depth = inputs.shape
-    planes, rows, quarter = own.shape
+        total += jnp.dot(
+            held[i], basis[i * piece : (i + 1) * piece], preferred_element_type=F32
+        )
+    out_ref[...] = total.T.astype(BF)
+
+
+def mapped_kernel(inputs, start, tok, quarter, *factor):
+    depth = inputs.shape[1]
+    fresh = len(factor) == 2
+    out = shape((quarter, tok), BF)
     return pl.pallas_call(
-        mapped_body,
-        out_shape=shape((tp_size, quarter, tok), BF),
-        in_specs=[pl.BlockSpec(memory_space=pltpu.HBM), VMEM, VMEM],
-        out_specs=VMEM,
+        functools.partial(mapped_body, start, fresh),
+        out_shape=(out, shape((depth, quarter), BF)) if fresh else out,
+        in_specs=[pl.BlockSpec(memory_space=pltpu.HBM)] + [VMEM] * len(factor),
+        out_specs=(VMEM, VMEM) if fresh else VMEM,
         scratch_shapes=[
-            pltpu.VMEM((BLOCKS, tok // BLOCKS, depth), BF),
-            pltpu.VMEM((planes, 2, rows, quarter), BF),
-            pltpu.SemaphoreType.DMA((BLOCKS,)),
+            pltpu.VMEM((PIECES, tok, depth // PIECES), BF),
+            pltpu.SemaphoreType.DMA((PIECES,)),
         ],
         name="mapped",
         compiler_params=pltpu.CompilerParams(vmem_limit_bytes=48 << 20),
         cost_estimate=pl.CostEstimate(
             flops=4 * tok * depth * quarter, bytes_accessed=2 * tok * depth, transcendentals=0
         ),
-    )(inputs, own, other)
-
-
-def part_body(mine, m_ref, k_ref, v_ref, out_ref):
-    c = lax.axis_index("c")
-    side = c if mine else 1 - c
+    )(inputs, *factor)
+
+
+def part_half(side, m_ref, k_ref, v_ref, out_ref):
     rank = m_ref.shape[0] // 2
     kw, vw = k_ref.shape[1] // 2, v_ref.shape[1] // 2
     kc = k_ref[:, pl.ds(pl.multiple_of(side * kw, 128), kw)]
@@ -105,7 +111,24 @@
     out_ref[:, kw:] = jnp.dot(m_ref[rank:], vc, preferred_element_type=F32).astype(out_ref.dtype)
 
 
-def stats_body(km, kv, vm, vv, kb, vb, mine, theirs, rows_kb, rows_vb):
+def part_theirs_body(*refs):
+    blocks, (k_ref, v_ref, m_ref, out_ref) = refs[:-4], refs[-4:]
+    t = lax.axis_index("tp")
+    quarter, tok = blocks[0].shape
+    peers = len(blocks) // 2
+    for away in range(peers):
+        rows = pl.ds(pl.multiple_of(lax.rem(t + away, peers) * quarter, quarter), quarter)
+        m_ref[rows, :tok] = blocks[2 * away][...]
+        m_ref[rows, tok:] = blocks[2 * away + 1][...]
+    part_half(1 - lax.axis_index("c"), m_ref, k_ref, v_ref, out_ref)
+
+
+def part_ours_body(m_ref, k_ref, v_ref, out_ref):
+    part_half(lax.axis_index("c"), m_ref, k_ref, v_ref, out_ref)
+
+
+def stats_body(km, kv, vm, vv, *refs):
+    held, (mine, theirs), staged = refs[:4], refs[4:6], refs[6:]
     c = lax.axis_index("c")
     rows = km.shape[0]
     kw, vw = km.shape[1] // 2, vm.shape[1] // 2
@@ -115,8 +138,8 @@
         out[:rows, kw:] = vm[:, vs]
         out[rows:, :kw] = kv[:, ks]
         out[rows:, kw:] = vv[:, vs]
-    rows_kb[...] = kb[...]
-    rows_vb[...] = vb[...]
+    for src, dst in zip(held, staged):
+        dst[...] = src[...]
 
 
 def moments_body(arrived, mine, theirs, dirs, own_new, back):
@@ -152,12 +175,10 @@
         vv[:, vs] = src[rows:, kw:]
 
 
-def gram_body(own, other, own_y, other_y, out):
+def gram_body(mine, beside, out):
     first = lax.axis_index("tp") % 2 == 0
-    mine = jnp.concatenate([own[...], other[...]], axis=0)
-    theirs = jnp.concatenate([own_y[...], other_y[...]], axis=0)
-    low = jnp.where(first, mine, theirs)
-    high = jnp.where(first, theirs, mine)
+    low = jnp.where(first, mine[...], beside[...])
+    high = jnp.where(first, beside[...], mine[...])
     cols = jnp.concatenate([low, high], axis=1)
     out[...] = lax.dot_general(
         cols, cols, (((0,), (0,)), ((), ())), preferred_element_type=F32
@@ -231,30 +252,38 @@
     quarter = both.shape[1] // tp_size
     own = spread(lax.dynamic_slice_in_dim(both, t * quarter, quarter, axis=1), PLANE)
     other = other_core(own)
-    mapped = mapped_kernel(inputs, own, other, tp_size)
-    mapped = lax.all_to_all(mapped, "tp", 0, 0, tiled=True)
-    mapped, own, other = lax.optimization_barrier((mapped, own, other))
-    mapped = mapped.reshape(-1, inputs.shape[0])
-
-    flops = mapped.size * 2 * width // 2
-    theirs = local(
-        functools.partial(part_body, False), shape((rank, width), BF), flops
-    )(mapped, key_cot, value_cot)
+    tok = inputs.shape[0] // 2
+    first, basis = mapped_kernel(inputs, 0, tok, quarter, own, other_core(own))
+    last = mapped_kernel(inputs, tok, tok, quarter, basis)
+
+    up = [(i, (i + 1) % tp_size) for i in range(tp_size)]
+    down = [(i, (i - 1) % tp_size) for i in range(tp_size)]
+    first_up = lax.ppermute(first, "tp", up)
+    first_down = lax.ppermute(first, "tp", down)
+    last_up = lax.ppermute(last, "tp", up)
+    last_down = lax.ppermute(last, "tp", down)
+    far_first = lax.ppermute(first_up, "tp", up)
+    far_last = lax.ppermute(last_down, "tp", down)
+    blocks = (first, last, first_down, last_down, far_first, far_last, first_up, last_up)
+
+    flops = 2 * rank * inputs.shape[0] * width
+    mapped, theirs = local(
+        part_theirs_body, (shape((2 * rank, inputs.shape[0]), BF), shape((rank, width), BF)), flops
+    )(*blocks, key_cot, value_cot)
     got = other_core(theirs)
-    ours = local(functools.partial(part_body, True), shape((rank, width)), flops)(
-        mapped, key_cot, value_cot
-    )
+    ours = local(part_ours_body, shape((rank, width)), flops)(mapped, key_cot, value_cot)
     pair = (ours + got.astype(F32)).astype(BF)
 
     beside = [(i, i ^ 1) for i in range(tp_size)]
     across = [(i, tp_size - 1 - i) for i in range(tp_size)]
-    own_y = lax.ppermute(own, "tp", beside)
-    other_y = lax.ppermute(other, "tp", beside)
+    basis, _ = lax.optimization_barrier((basis, mapped))
+    basis_y = lax.ppermute(basis, "tp", beside)
 
     stat = shape((two_rows, width))
-    mine, theirs, key_rows, value_rows = local(
-        stats_body, (stat, stat, shape(key_basis.shape, BF), shape(value_basis.shape, BF))
-    )(*moments, key_basis, value_basis)
+    held = (key_basis, value_basis, key_weight, value_weight)
+    mine, theirs, key_rows, value_rows, key_old, value_old = local(
+        stats_body, (stat, stat) + tuple(shape(a.shape, a.dtype) for a in held)
+    )(*moments, *held)
     stats = other_core(theirs)
     arrived = lax.all_to_all(pair.reshape(planes, -1, width), PLANE, 0, 0, tiled=True)
     dirs, own_new, back = local(
@@ -262,8 +291,7 @@
     )(arrived, mine, stats)
     own_dir = lax.all_to_all(dirs, PLANE, 0, 0, tiled=True).reshape(rank, width)
 
-    flat = [a.reshape(-1, quarter) for a in (own, other, own_y, other_y)]
-    gram = local(gram_body, shape((rank, rank)), 4 * flat[0].size * rank)(*flat)
+    gram = local(gram_body, shape((rank, rank)), 4 * basis.size * rank)(basis, basis_y)
     gram_y = lax.ppermute(gram, "tp", across)
     new_moments = local(placed_body, tuple(shape(a.shape) for a in moments))(
         own_new, other_core(back)
@@ -287,7 +315,7 @@
             shape(key_weight.shape, BF),
             shape(value_weight.shape, BF),
         ),
-    )(*sums, key_up, value_up, key_weight, value_weight)
+    )(*sums, key_up, value_up, key_old, value_old)
     key_mean_new, key_var_new, value_mean_new, value_var_new = new_moments
     return (
         key_new,

time: 128 us -> 119 us (0.930)
  the two profiles are of different devices: /device:TPU:2 before, /device:TPU:1 now
where the time goes in v3:
time: 119 us; the launch traced here: 118 us
  blocking collectives  45.6 us (38%)
  waiting for transfers between devices  30.1 us (25%)
  starting transfers between devices  26.4 us (22%)
  Pallas kernels  13.1 us (11%)
  other arithmetic  1.55 us (1%)
    all_to_all x1, blocking collectives, spread(): lax.all_to_all(jnp.broadcast_to(shard[None], (peers, *shard.shape)), axes...  27.9 us
    all_to_all x1, blocking collectives, step(): own_dir = lax.all_to_all(dirs, PLANE, 0, 0, tiled=True).reshape(rank, width)  17.6 us
    all_to_all x1, waiting for transfers between devices, step(): lax.all_to_all(pair.reshape(planes, -1, width), PLANE, 0, 0, tiled=True)  12.1 us
    ppermute x5, starting transfers between devices, other_core(): return lax.ppermute(a, 'c', SWAP)  10.4 us
    ppermute x1, waiting for transfers between devices, step(): gram_y = lax.ppermute(gram, 'tp', across)  8.96 us
    pallas_call x2, Pallas kernels, mapped_kernel(): pl.pallas_call(functools.partial(mapped_body, start, fresh), out_shape=(o...  8.39 us
    pallas_call x8, Pallas kernels, call(): pl.pallas_call(body, out_shape=outs, in_specs=[VMEM] * len(arrays), out_s...  4.72 us
    all_to_all x1, starting transfers between devices, step(): lax.all_to_all(pair.reshape(planes, -1, width), PLANE, 0, 0, tiled=True)  4.35 us
  transfers between devices with their start and end apart: 17, of which 10 were waited for; matrix products, arithmetic and copies ran while one was open for 0% of the time, Pallas kernels for 3%

profile of v3, /device:TPU:1, one launch (start us, length us, event | category | flops | bytes accessed | tf_op | source)
XLA Modules:
  0.0 117.7 jit_solution(14341318228173508165)
XLA Ops:
  1.5 27.9 %all_to_all.15.refs_1_ = bf16[32,64,128]{2,1,0:T(8,128)(2,1)S(1)} all-to-all(bf16[32,64,128]{2,1,0:T(8,128)(2,1)S(1)} %broadcast_in_dim.2), channel_id=1, replica_groups=mesh['z'=8,'x'=4,'c'=2,'tp'=4] {'z','x'}, dimensions={0} | all-to-all | bytes 1048576 | tf_op jit(solution)/shard_map/all_to_all | solution.py:22
  29.4 2.4 %collective-permute-start = (bf16[32,64,128]{2,1,0:T(8,128)(2,1)S(1)}, bf16[32,64,128]{2,1,0:T(8,128)(2,1)S(1)}, u32[]{:S(2)}, u32[]{:S(2)}) collective-permute-start(bf16[32,64,128]{2,1,0:T(8,128)(2,1)S(1)} %all_to_all.15.refs_1_), channel_id=1, source_target_pairs={{0,4},{4,0},{1,5},{5,1},{2,6},{6,2},{3,7},{7,3},{8,12},{12,8},{9,1... | collective-permute-start | bytes 1572872 | tf_op jit(solution)/shard_map/ppermute | solution.py:28
  31.9 1.5 %collective-permute-done.refs_2_ = bf16[32,64,128]{2,1,0:T(8,128)(2,1)S(1)} collective-permute-done((bf16[32,64,128]{2,1,0:T(8,128)(2,1)S(1)}, bf16[32,64,128]{2,1,0:T(8,128)(2,1)S(1)}, u32[]{:S(2)}, u32[]{:S(2)}) %collective-permute-start) | collective-permute-done | bytes 524320 | tf_op jit(solution)/shard_map/ppermute | solution.py:28
  33.4 4.1 %mapped.2 = (bf16[128,512]{1,0:T(8,128)(2,1)S(1)}, bf16[4096,128]{1,0:T(8,128)(2,1)S(1)}) custom-call(bf16[1024,4096]{1,0:T(8,128)(2,1)} %refs_0_.4, bf16[32,64,128]{2,1,0:T(8,128)(2,1)S(1)} %all_to_all.15.refs_1_, bf16[32,64,128]{2,1,0:T(8,128)(2,1)S(1)} %collective-permute-done.refs_2_), custom_call_target="tpu_custom_call" | custom-call | flops 1073741824 | bytes 4194304 | tf_op jit(solution)/shard_map/mapped/pallas_call | solution.py:88
  37.7 4.2 %mapped.3.refs_1_ = bf16[128,512]{1,0:T(8,128)(2,1)S(1)} custom-call(bf16[1024,4096]{1,0:T(8,128)(2,1)} %refs_0_.4, bf16[4096,128]{1,0:T(8,128)(2,1)S(1)} %get-tuple-element.42.refs_1_.mine), custom_call_target="tpu_custom_call" | custom-call | flops 1073741824 | bytes 4194304 | tf_op jit(solution)/shard_map/mapped/pallas_call | solution.py:88
  41.9 2.8 %collective-permute-start.2 = (bf16[128,512]{1,0:T(8,128)(2,1)S(1)}, bf16[128,512]{1,0:T(8,128)(2,1)S(1)}, u32[]{:S(2)}, u32[]{:S(2)}) collective-permute-start(bf16[128,512]{1,0:T(8,128)(2,1)S(1)} %mapped.3.refs_1_), channel_id=1, source_target_pairs={{0,3},{1,0},{2,1},{3,2},{4,7},{5,4},{6,5},{7,6},{8,11},{9,8},{10,9... | collective-permute-start | bytes 393224 | tf_op jit(solution)/shard_map/ppermute | solution.py:264
  44.7 2.7 %collective-permute-start.1 = (bf16[128,512]{1,0:T(8,128)(2,1)S(1)}, bf16[128,512]{1,0:T(8,128)(2,1)S(1)}, u32[]{:S(2)}, u32[]{:S(2)}) collective-permute-start(bf16[128,512]{1,0:T(8,128)(2,1)S(1)} %get-tuple-element.33.refs_0_), channel_id=1, source_target_pairs={{0,3},{1,0},{2,1},{3,2},{4,7},{5,4},{6,5},{7,6},{8,11},{9,8},{10,9... | collective-permute-start | bytes 393224 | tf_op jit(solution)/shard_map/ppermute | solution.py:262
  47.4 3.2 %collective-permute-start.5 = (bf16[128,512]{1,0:T(8,128)(2,1)S(1)}, bf16[128,512]{1,0:T(8,128)(2,1)S(1)}, u32[]{:S(2)}, u32[]{:S(2)}) collective-permute-start(bf16[128,512]{1,0:T(8,128)(2,1)S(1)} %collective-permute-done.2.refs_3_), channel_id=1, source_target_pairs={{0,3},{1,0},{2,1},{3,2},{4,7},{5,4},{6,5},{7,6},{8,11},{9,8},{10,9... | collective-permute-start | bytes 393224 | tf_op jit(solution)/shard_map/ppermute | solution.py:266
  50.6 2.5 %collective-permute-done.6.refs_7_ = bf16[128,512]{1,0:T(8,128)(2,1)S(1)} collective-permute-done((bf16[128,512]{1,0:T(8,128)(2,1)S(1)}, bf16[128,512]{1,0:T(8,128)(2,1)S(1)}, u32[]{:S(2)}, u32[]{:S(2)}) %collective-permute-start.6) | collective-permute-done | bytes 131104 | tf_op jit(solution)/shard_map/ppermute | solution.py:263
  53.1 2.5 %collective-permute-done.4.refs_4_ = bf16[128,512]{1,0:T(8,128)(2,1)S(1)} collective-permute-done((bf16[128,512]{1,0:T(8,128)(2,1)S(1)}, bf16[128,512]{1,0:T(8,128)(2,1)S(1)}, u32[]{:S(2)}, u32[]{:S(2)}) %collective-permute-start.4) | collective-permute-done | bytes 131104 | tf_op jit(solution)/shard_map/ppermute | solution.py:265
  56.3 3.6 %collective-permute-start.7 = (bf16[256,768]{1,0:T(8,128)(2,1)S(1)}, bf16[256,768]{1,0:T(8,128)(2,1)S(1)}, u32[]{:S(2)}, u32[]{:S(2)}) collective-permute-start(bf16[256,768]{1,0:T(8,128)(2,1)S(1)} %get-tuple-element.36), channel_id=1, source_target_pairs={{0,4},{4,0},{1,5},{5,1},{2,6},{6,2},{3,7},{7,3},{8,12},{12,8},{9,1... | collective-permute-start | bytes 1179656 | tf_op jit(solution)/shard_map/ppermute | solution.py:28
  60.4 0.8 collective-permute-done.7
  61.2 0.8 fusion
  62.0 4.4 %all-to-all-start.1 = ((bf16[32,8,768]{2,1,0:T(8,128)(2,1)}), bf16[32,8,768]{2,1,0:T(8,128)(2,1)S(1)}, u32[]{:S(2)}, u32[]{:S(2)}) async-start(bf16[32,8,768]{2,1,0:T(8,128)(2,1)} %fusion), calls=%async_computation.1 | async-start | bytes 786432 | tf_op jit(solution)/shard_map/all_to_all | solution.py:288
  67.3 0.8 collective-permute-done.8.theirs
  68.2 12.1 %all-to-all-done.1.arrived = bf16[32,8,768]{2,1,0:T(8,128)(2,1)S(1)} async-done(((bf16[32,8,768]{2,1,0:T(8,128)(2,1)}), bf16[32,8,768]{2,1,0:T(8,128)(2,1)S(1)}, u32[]{:S(2)}, u32[]{:S(2)}) %all-to-all-start.1) | async-done | bytes 393248 | tf_op jit(solution)/shard_map/all_to_all | solution.py:288
  80.4 17.6 %all_to_all.16 = bf16[32,8,768]{2,1,0:T(8,128)(2,1)S(1)} all-to-all(bf16[32,8,768]{2,1,0:T(8,128)(2,1)S(1)} %get-tuple-element.39), channel_id=1, replica_groups=mesh['z'=8,'x'=4,'c'=2,'tp'=4] {'z','x'}, dimensions={0} | all-to-all | bytes 786432 | tf_op jit(solution)/shard_map/all_to_all | solution.py:292
  98.0 3.5 %collective-permute-start.9 = (bf16[256,768]{1,0:T(8,128)(2,1)S(1)}, bf16[256,768]{1,0:T(8,128)(2,1)S(1)}, u32[]{:S(2)}, u32[]{:S(2)}) collective-permute-start(bf16[256,768]{1,0:T(8,128)(2,1)S(1)} %bitcast.3), channel_id=1, source_target_pairs={{0,4},{4,0},{1,5},{5,1},{2,6},{6,2},{3,7},{7,3},{8,12},{12,8},{9,1... | collective-permute-start | bytes 1179656 | tf_op jit(solution)/shard_map/ppermute | solution.py:28
  101.5 0.8 shard_map.174.gram
  102.5 9.0 %collective-permute-done.11.gram_y = f32[256,256]{1,0:T(8,128)S(1)} collective-permute-done((f32[256,256]{1,0:T(8,128)S(1)}, f32[256,256]{1,0:T(8,128)S(1)}, u32[]{:S(2)}, u32[]{:S(2)}) %collective-permute-start.11) | collective-permute-done | bytes 262176 | tf_op jit(solution)/shard_map/ppermute | solution.py:295
  111.5 1.1 shard_map.175
  112.6 1.5 %collective-permute-start.13 = (f32[1,128]{1,0:T(1,128)S(1)}, f32[1,128]{1,0:T(1,128)S(1)}, u32[]{:S(2)}, u32[]{:S(2)}) collective-permute-start(f32[1,128]{1,0:T(1,128)S(1)} %get-tuple-element.43.s0), channel_id=1, source_target_pairs={{0,2},{1,3},{2,0},{3,1},{4,6},{5,7},{6,4},{7,5},{8,10},{9,11},{10,... | collective-permute-start | bytes 1544 | tf_op jit(solution)/shard_map/ppermute | solution.py:306
  114.1 1.2 %collective-permute-start.14 = (f32[1,128]{1,0:T(1,128)S(1)}, f32[1,128]{1,0:T(1,128)S(1)}, u32[]{:S(2)}, u32[]{:S(2)}) collective-permute-start(f32[1,128]{1,0:T(1,128)S(1)} %get-tuple-element.43.s0), channel_id=1, source_target_pairs={{0,3},{1,0},{2,1},{3,2},{4,7},{5,4},{6,5},{7,6},{8,11},{9,8},{10,9... | collective-permute-start | bytes 1544 | tf_op jit(solution)/shard_map/ppermute | solution.py:306
  116.8 0.9 shard_map.176
  (45 shorter events, 4.9 us)
Async XLA Ops:
  29.4 4.0 %collective-permute-start = (bf16[32,64,128]{2,1,0:T(8,128)(2,1)S(1)}, bf16[32,64,128]{2,1,0:T(8,128)(2,1)S(1)}, u32[]{:S(2)}, u32[]{:S(2)}) collective-permute-start(bf16[32,64,128]{2,1,0:T(8,128)(2,1)S(1)} %all_to_all.15.refs_1_), channel_id=1, source_target_pairs={{0,4},{4,0},{1,5},{5,1},{2,6},{6,2},{3,7},{7,3},{8,12},{12,8},{9,1... | collective-permute-start | bytes 1572872 | tf_op jit(solution)/shard_map/ppermute | solution.py:28
  37.6 28.9 %copy-start.2 = (f32[64,1024]{1,0:T(8,128)S(1)}, f32[64,1024]{1,0:T(8,128)}, u32[]{:S(2)}) copy-start(f32[64,1024]{1,0:T(8,128)} %refs_3_.1) | copy-start | bytes 786436
  37.6 28.9 %copy-start.3 = (bf16[64,256]{1,0:T(8,128)(2,1)S(1)}, bf16[64,256]{1,0:T(8,128)(2,1)}, u32[]{:S(2)}) copy-start(bf16[64,256]{1,0:T(8,128)(2,1)} %refs_0_.5) | copy-start | bytes 98308
  37.6 28.9 %copy-start.4 = (bf16[64,256]{1,0:T(8,128)(2,1)S(1)}, bf16[64,256]{1,0:T(8,128)(2,1)}, u32[]{:S(2)}) copy-start(bf16[64,256]{1,0:T(8,128)(2,1)} %refs_1_.1) | copy-start | bytes 98308
  37.6 28.9 %copy-start.5 = (f32[64,512]{1,0:T(8,128)S(1)}, f32[64,512]{1,0:T(8,128)}, u32[]{:S(2)}) copy-start(f32[64,512]{1,0:T(8,128)} %refs_2_.1) | copy-start | bytes 393220
  37.6 28.9 %copy-start.6 = (f32[4,1024]{1,0:T(4,128)S(1)}, f32[4,1024]{1,0:T(4,128)}, u32[]{:S(2)}) copy-start(f32[4,1024]{1,0:T(4,128)} %vm.1) | copy-start | bytes 49156
  37.6 28.9 %copy-start.7 = (f32[4,1024]{1,0:T(4,128)S(1)}, f32[4,1024]{1,0:T(4,128)}, u32[]{:S(2)}) copy-start(f32[4,1024]{1,0:T(4,128)} %vv.1) | copy-start | bytes 49156
  37.6 28.9 %copy-start.8 = (f32[4,512]{1,0:T(4,128)S(1)}, f32[4,512]{1,0:T(4,128)}, u32[]{:S(2)}) copy-start(f32[4,512]{1,0:T(4,128)} %km.1) | copy-start | bytes 24580
  41.9 5.5 %collective-permute-start.2 = (bf16[128,512]{1,0:T(8,128)(2,1)S(1)}, bf16[128,512]{1,0:T(8,128)(2,1)S(1)}, u32[]{:S(2)}, u32[]{:S(2)}) collective-permute-start(bf16[128,512]{1,0:T(8,128)(2,1)S(1)} %mapped.3.refs_1_), channel_id=1, source_target_pairs={{0,3},{1,0},{2,1},{3,2},{4,7},{5,4},{6,5},{7,6},{8,11},{9,8},{10,9... | collective-permute-start | bytes 393224 | tf_op jit(solution)/shard_map/ppermute | solution.py:264
  44.7 5.9 %collective-permute-start.3 = (bf16[128,512]{1,0:T(8,128)(2,1)S(1)}, bf16[128,512]{1,0:T(8,128)(2,1)S(1)}, u32[]{:S(2)}, u32[]{:S(2)}) collective-permute-start(bf16[128,512]{1,0:T(8,128)(2,1)S(1)} %get-tuple-element.33.refs_0_), channel_id=1, source_target_pairs={{0,1},{1,2},{2,3},{3,0},{4,5},{5,6},{6,7},{7,4},{8,9},{9,10},{10,1... | collective-permute-start | bytes 393224 | tf_op jit(solution)/shard_map/ppermute | solution.py:261
  44.7 8.4 %collective-permute-start.6 = (bf16[128,512]{1,0:T(8,128)(2,1)S(1)}, bf16[128,512]{1,0:T(8,128)(2,1)S(1)}, u32[]{:S(2)}, u32[]{:S(2)}) collective-permute-start(bf16[128,512]{1,0:T(8,128)(2,1)S(1)} %mapped.3.refs_1_), channel_id=1, source_target_pairs={{0,1},{1,2},{2,3},{3,0},{4,5},{5,6},{6,7},{7,4},{8,9},{9,10},{10,1... | collective-permute-start | bytes 393224 | tf_op jit(solution)/shard_map/ppermute | solution.py:263
  44.7 8.4 %collective-permute-start.1 = (bf16[128,512]{1,0:T(8,128)(2,1)S(1)}, bf16[128,512]{1,0:T(8,128)(2,1)S(1)}, u32[]{:S(2)}, u32[]{:S(2)}) collective-permute-start(bf16[128,512]{1,0:T(8,128)(2,1)S(1)} %get-tuple-element.33.refs_0_), channel_id=1, source_target_pairs={{0,3},{1,0},{2,1},{3,2},{4,7},{5,4},{6,5},{7,6},{8,11},{9,8},{10,9... | collective-permute-start | bytes 393224 | tf_op jit(solution)/shard_map/ppermute | solution.py:262
  47.4 5.7 %collective-permute-start.5 = (bf16[128,512]{1,0:T(8,128)(2,1)S(1)}, bf16[128,512]{1,0:T(8,128)(2,1)S(1)}, u32[]{:S(2)}, u32[]{:S(2)}) collective-permute-start(bf16[128,512]{1,0:T(8,128)(2,1)S(1)} %collective-permute-done.2.refs_3_), channel_id=1, source_target_pairs={{0,3},{1,0},{2,1},{3,2},{4,7},{5,4},{6,5},{7,6},{8,11},{9,8},{10,9... | collective-permute-start | bytes 393224 | tf_op jit(solution)/shard_map/ppermute | solution.py:266
  50.6 5.0 %collective-permute-start.4 = (bf16[128,512]{1,0:T(8,128)(2,1)S(1)}, bf16[128,512]{1,0:T(8,128)(2,1)S(1)}, u32[]{:S(2)}, u32[]{:S(2)}) collective-permute-start(bf16[128,512]{1,0:T(8,128)(2,1)S(1)} %collective-permute-done.3.refs_6_), channel_id=1, source_target_pairs={{0,1},{1,2},{2,3},{3,0},{4,5},{5,6},{6,7},{7,4},{8,9},{9,10},{10,1... | collective-permute-start | bytes 393224 | tf_op jit(solution)/shard_map/ppermute | solution.py:265
  56.3 4.9 %collective-permute-start.7 = (bf16[256,768]{1,0:T(8,128)(2,1)S(1)}, bf16[256,768]{1,0:T(8,128)(2,1)S(1)}, u32[]{:S(2)}, u32[]{:S(2)}) collective-permute-start(bf16[256,768]{1,0:T(8,128)(2,1)S(1)} %get-tuple-element.36), channel_id=1, source_target_pairs={{0,4},{4,0},{1,5},{5,1},{2,6},{6,2},{3,7},{7,3},{8,12},{12,8},{9,1... | collective-permute-start | bytes 1179656 | tf_op jit(solution)/shard_map/ppermute | solution.py:28
  62.0 18.2 %all-to-all-start.1 = ((bf16[32,8,768]{2,1,0:T(8,128)(2,1)}), bf16[32,8,768]{2,1,0:T(8,128)(2,1)S(1)}, u32[]{:S(2)}, u32[]{:S(2)}) async-start(bf16[32,8,768]{2,1,0:T(8,128)(2,1)} %fusion), calls=%async_computation.1 | async-start | bytes 786432 | tf_op jit(solution)/shard_map/all_to_all | solution.py:288
  66.4 35.2 %collective-permute-start.10 = (bf16[4096,128]{1,0:T(8,128)(2,1)S(1)}, bf16[4096,128]{1,0:T(8,128)(2,1)S(1)}, u32[]{:S(2)}, u32[]{:S(2)}) collective-permute-start(bf16[4096,128]{1,0:T(8,128)(2,1)S(1)} %get-tuple-element.42.refs_1_.mine), channel_id=1, source_target_pairs={{0,1},{1,0},{2,3},{3,2},{4,5},{5,4},{6,7},{7,6},{8,9},{9,8},{10,11... | collective-permute-start | bytes 3145736 | tf_op jit(solution)/shard_map/ppermute | solution.py:280
  66.6 1.6 %collective-permute-start.8 = (f32[8,768]{1,0:T(8,128)S(1)}, f32[8,768]{1,0:T(8,128)S(1)}, u32[]{:S(2)}, u32[]{:S(2)}) collective-permute-start(f32[8,768]{1,0:T(8,128)S(1)} %get-tuple-element.38), channel_id=1, source_target_pairs={{0,4},{4,0},{1,5},{5,1},{2,6},{6,2},{3,7},{7,3},{8,12},{12,8},{9,1... | collective-permute-start | bytes 73736 | tf_op jit(solution)/shard_map/ppermute | solution.py:28
  98.0 13.5 %collective-permute-start.9 = (bf16[256,768]{1,0:T(8,128)(2,1)S(1)}, bf16[256,768]{1,0:T(8,128)(2,1)S(1)}, u32[]{:S(2)}, u32[]{:S(2)}) collective-permute-start(bf16[256,768]{1,0:T(8,128)(2,1)S(1)} %bitcast.3), channel_id=1, source_target_pairs={{0,4},{4,0},{1,5},{5,1},{2,6},{6,2},{3,7},{7,3},{8,12},{12,8},{9,1... | collective-permute-start | bytes 1179656 | tf_op jit(solution)/shard_map/ppermute | solution.py:28
  102.3 9.2 %collective-permute-start.11 = (f32[256,256]{1,0:T(8,128)S(1)}, f32[256,256]{1,0:T(8,128)S(1)}, u32[]{:S(2)}, u32[]{:S(2)}) collective-permute-start(f32[256,256]{1,0:T(8,128)S(1)} %shard_map.174.gram), channel_id=1, source_target_pairs={{0,3},{1,2},{2,1},{3,0},{4,7},{5,6},{6,5},{7,4},{8,11},{9,10},{10,... | collective-permute-start | bytes 786440 | tf_op jit(solution)/shard_map/ppermute | solution.py:295
  102.4 12.9 %collective-permute-start.15 = (f32[8,768]{1,0:T(8,128)S(1)}, f32[8,768]{1,0:T(8,128)S(1)}, u32[]{:S(2)}, u32[]{:S(2)}) collective-permute-start(f32[8,768]{1,0:T(8,128)S(1)} %get-tuple-element.53), channel_id=1, source_target_pairs={{0,4},{4,0},{1,5},{5,1},{2,6},{6,2},{3,7},{7,3},{8,12},{12,8},{9,1... | collective-permute-start | bytes 73736 | tf_op jit(solution)/shard_map/ppermute | solution.py:28
  112.5 3.7 %collective-permute-start.12 = (f32[1,128]{1,0:T(1,128)S(1)}, f32[1,128]{1,0:T(1,128)S(1)}, u32[]{:S(2)}, u32[]{:S(2)}) collective-permute-start(f32[1,128]{1,0:T(1,128)S(1)} %get-tuple-element.43.s0), channel_id=1, source_target_pairs={{0,1},{1,2},{2,3},{3,0},{4,5},{5,6},{6,7},{7,4},{8,9},{9,10},{10,1... | collective-permute-start | bytes 1544 | tf_op jit(solution)/shard_map/ppermute | solution.py:306
  112.6 4.0 %collective-permute-start.13 = (f32[1,128]{1,0:T(1,128)S(1)}, f32[1,128]{1,0:T(1,128)S(1)}, u32[]{:S(2)}, u32[]{:S(2)}) collective-permute-start(f32[1,128]{1,0:T(1,128)S(1)} %get-tuple-element.43.s0), channel_id=1, source_target_pairs={{0,2},{1,3},{2,0},{3,1},{4,6},{5,7},{6,4},{7,5},{8,10},{9,11},{10,... | collective-permute-start | bytes 1544 | tf_op jit(solution)/shard_map/ppermute | solution.py:306
  114.1 2.7 %collective-permute-start.14 = (f32[1,128]{1,0:T(1,128)S(1)}, f32[1,128]{1,0:T(1,128)S(1)}, u32[]{:S(2)}, u32[]{:S(2)}) collective-permute-start(f32[1,128]{1,0:T(1,128)S(1)} %get-tuple-element.43.s0), channel_id=1, source_target_pairs={{0,3},{1,0},{2,1},{3,2},{4,7},{5,4},{6,5},{7,6},{8,11},{9,8},{10,9... | collective-permute-start | bytes 1544 | tf_op jit(solution)/shard_map/ppermute | solution.py:306
  (3 other events, 81.3 us)

commit v4 on v3

--- a/solution.py
+++ b/solution.py
@@ -48,58 +48,32 @@
     return call
 
 
-PIECES = 4
-
-
-def mapped_body(start, fresh, *refs):
+def mapped_body(fresh, *refs):
     if fresh:
-        x_ref, own_ref, other_ref, out_ref, basis, held, sems = refs
+        x_ref, own_ref, other_ref, out_ref, basis = refs
+        c, x = lax.axis_index("c"), lax.axis_index("x")
+        peers = own_ref.shape[0]
+        for away in range(peers):
+            at = lax.rem(x + away, peers)
+            basis[:, at, c] = own_ref[away]
+            basis[:, at, 1 - c] = other_ref[away]
     else:
-        x_ref, basis, out_ref, held, sems = refs
-    tok, piece = held.shape[1:]
-
-    def load(i):
-        return pltpu.make_async_copy(
-            x_ref.at[pl.ds(start, tok), pl.ds(i * piece, piece)], held.at[i], sems.at[i]
-        )
-
-    for i in range(PIECES):
-        load(i).start()
-    if fresh:
-        first = lax.axis_index("c") == 0
-        planes, rows, quarter = own_ref.shape
-        own, other = own_ref[...], other_ref[...]
-        low = jnp.where(first, own, other)
-        high = jnp.where(first, other, own)
-        basis[...] = jnp.stack([low, high], axis=1).reshape(2 * planes * rows, quarter)
-    total = jnp.zeros((tok, out_ref.shape[0]), F32)
-    for i in range(PIECES):
-        load(i).wait()
-        total += jnp.dot(
-            held[i], basis[i * piece : (i + 1) * piece], preferred_element_type=F32
-        )
-    out_ref[...] = total.T.astype(BF)
-
-
-def mapped_kernel(inputs, start, tok, quarter, *factor):
-    depth = inputs.shape[1]
+        x_ref, basis, out_ref = refs
+    whole = basis[...].reshape(x_ref.shape[1], -1)
+    out_ref[...] = jnp.dot(x_ref[...], whole, preferred_element_type=F32).T.astype(BF)
+
+
+def mapped_kernel(x, *factor):
+    tok, depth = x.shape
+    quarter = factor[0].shape[-1]
     fresh = len(factor) == 2
     out = shape((quarter, tok), BF)
-    return pl.pallas_call(
-        functools.partial(mapped_body, start, fresh),
-        out_shape=(out, shape((depth, quarter), BF)) if fresh else out,
-        in_specs=[pl.BlockSpec(memory_space=pltpu.HBM)] + [VMEM] * len(factor),
-        out_specs=(VMEM, VMEM) if fresh else VMEM,
-        scratch_shapes=[
-            pltpu.VMEM((PIECES, tok, depth // PIECES), BF),
-            pltpu.SemaphoreType.DMA((PIECES,)),
-        ],
-        name="mapped",
-        compiler_params=pltpu.CompilerParams(vmem_limit_bytes=48 << 20),
-        cost_estimate=pl.CostEstimate(
-            flops=4 * tok * depth * quarter, bytes_accessed=2 * tok * depth, transcendentals=0
-        ),
-    )(inputs, *factor)
+    peers, far, rows = factor[0].shape[:3]
+    return local(
+        functools.partial(mapped_body, fresh),
+        (out, shape((far, peers, 2, rows, quarter), BF)) if fresh else out,
+        4 * tok * depth * quarter,
+    )(x, *factor)
 
 
 def part_half(side, m_ref, k_ref, v_ref, out_ref):
@@ -250,11 +224,19 @@
 
     both = jnp.concatenate([key_basis, value_basis], axis=1)
     quarter = both.shape[1] // tp_size
-    own = spread(lax.dynamic_slice_in_dim(both, t * quarter, quarter, axis=1), PLANE)
-    other = other_core(own)
     tok = inputs.shape[0] // 2
-    first, basis = mapped_kernel(inputs, 0, tok, quarter, own, other_core(own))
-    last = mapped_kernel(inputs, tok, tok, quarter, basis)
+    shard = lax.dynamic_slice_in_dim(both, t * quarter, quarter, axis=1)
+    near = spread(shard, "z")
+    x_size = lax.axis_size("x")
+    own = [near]
+    for away in range(1, x_size):
+        own.append(
+            lax.ppermute(near, "x", [((i + away) % x_size, i) for i in range(x_size)])
+        )
+    own = jnp.stack(own)
+    x_first, x_last = inputs[:tok], inputs[tok:]
+    first, basis = mapped_kernel(x_first, own, other_core(own))
+    last = mapped_kernel(x_last, basis)
 
     up = [(i, (i + 1) % tp_size) for i in range(tp_size)]
     down = [(i, (i - 1) % tp_size) for i in range(tp_size)]
@@ -276,7 +258,6 @@
 
     beside = [(i, i ^ 1) for i in range(tp_size)]
     across = [(i, tp_size - 1 - i) for i in range(tp_size)]
-    basis, _ = lax.optimization_barrier((basis, mapped))
     basis_y = lax.ppermute(basis, "tp", beside)
 
     stat = shape((two_rows, width))
@@ -291,7 +272,9 @@
     )(arrived, mine, stats)
     own_dir = lax.all_to_all(dirs, PLANE, 0, 0, tiled=True).reshape(rank, width)
 
-    gram = local(gram_body, shape((rank, rank)), 4 * basis.size * rank)(basis, basis_y)
+    gram = local(gram_body, shape((rank, rank)), 4 * basis.size * rank)(
+        basis.reshape(-1, quarter), basis_y.reshape(-1, quarter)
+    )
     gram_y = lax.ppermute(gram, "tp", across)
     new_moments = local(placed_body, tuple(shape(a.shape) for a in moments))(
         own_new, other_core(back)

time: 119 us -> 114 us (0.958)
  blocking collectives: 45.6 us -> 33.5 us
  Pallas kernels: 13.1 us -> 7.45 us
  waiting for transfers between devices: 30.1 us -> 34.9 us
  starting transfers between devices: 26.4 us -> 30.3 us
  local copies, waits for them, and re-layouts: 0.17 us -> 4.04 us
    all_to_all x1, blocking collectives: 27.9 us -> 16.6 us  [spread(): lax.all_to_all(jnp.broadcast_to(shard[None], (peers, *shard.shape)), axes...]
    pallas_call x2 -> x0, Pallas kernels: 8.39 us -> none  [mapped_kernel(): pl.pallas_call(functools.partial(mapped_body, start, fresh), out_shape=(o...]
    ppermute x0 -> x3, waiting for transfers between devices: none -> 5.6 us  [step(): lax.ppermute(near, 'x', [((i + away) % x_size, i) for i in range(x_size)])]
    slice x0 -> x1, local copies, waits for them, and re-layouts: none -> 3.96 us  [step(): x_first, x_last = (inputs[:tok], inputs[tok:])]
    ppermute x0 -> x3, starting transfers between devices: none -> 3.6 us  [step(): lax.ppermute(near, 'x', [((i + away) % x_size, i) for i in range(x_size)])]
    pallas_call x8 -> x10, Pallas kernels: 4.72 us -> 7.45 us  [call(): pl.pallas_call(body, out_shape=outs, in_specs=[VMEM] * len(arrays), out_s...]
    ppermute x5, waiting for transfers between devices: 3.16 us -> 1.63 us  [other_core(): return lax.ppermute(a, 'c', SWAP)]
  transfers between devices with their start and end apart: 17 -> 20, of which waited for: 10 -> 13; matrix products, arithmetic and copies ran while one was open for 0% -> 4% of each run, Pallas kernels for 3% -> 3%
where the time goes in v4:
time: 114 us; the launch traced here: 113 us
  waiting for transfers between devices  34.9 us (31%)
  blocking collectives  33.5 us (29%)
  starting transfers between devices  30.3 us (27%)
  Pallas kernels  7.45 us (7%)
  local copies, waits for them, and re-layouts  4.04 us (4%)
  other arithmetic  1.64 us (1%)
    all_to_all x1, blocking collectives, step(): own_dir = lax.all_to_all(dirs, PLANE, 0, 0, tiled=True).reshape(rank, width)  17 us
    all_to_all x1, blocking collectives, spread(): lax.all_to_all(jnp.broadcast_to(shard[None], (peers, *shard.shape)), axes...  16.6 us
    all_to_all x1, waiting for transfers between devices, step(): lax.all_to_all(pair.reshape(planes, -1, width), PLANE, 0, 0, tiled=True)  12.7 us
    ppermute x5, starting transfers between devices, other_core(): return lax.ppermute(a, 'c', SWAP)  10.8 us
    ppermute x1, waiting for transfers between devices, step(): gram_y = lax.ppermute(gram, 'tp', across)  8.96 us
    pallas_call x10, Pallas kernels, call(): pl.pallas_call(body, out_shape=outs, in_specs=[VMEM] * len(arrays), out_s...  7.45 us
    ppermute x3, waiting for transfers between devices, step(): lax.ppermute(near, 'x', [((i + away) % x_size, i) for i in range(x_size)])  5.6 us
    slice x1, local copies, waits for them, and re-layouts, step(): x_first, x_last = (inputs[:tok], inputs[tok:])  3.96 us
  transfers between devices with their start and end apart: 20, of which 13 were waited for; matrix products, arithmetic and copies ran while one was open for 4% of the time, Pallas kernels for 3%

profile of v4, /device:TPU:1, one launch (start us, length us, event | category | flops | bytes accessed | tf_op | source)
XLA Modules:
  0.0 112.8 jit_solution(5053885617865900711)
XLA Ops:
  1.4 16.6 %all_to_all.15 = bf16[8,64,128]{2,1,0:T(8,128)(2,1)S(1)} all-to-all(bf16[8,64,128]{2,1,0:T(8,128)(2,1)S(1)} %broadcast_in_dim.2), channel_id=1, replica_groups=mesh['z'=8,'x'=4,'c'=2,'tp'=4] {'z'}, dimensions={0} | all-to-all | bytes 262144 | tf_op jit(solution)/shard_map/all_to_all | solution.py:22
  18.0 2.5 %collective-permute-start = (bf16[8,64,128]{2,1,0:T(8,128)(2,1)S(1)}, bf16[8,64,128]{2,1,0:T(8,128)(2,1)S(1)}, u32[]{:S(2)}, u32[]{:S(2)}) collective-permute-start(bf16[8,64,128]{2,1,0:T(8,128)(2,1)S(1)} %all_to_all.15), channel_id=1, source_target_pairs={{8,0},{16,8},{24,16},{0,24},{9,1},{17,9},{25,17},{1,25},{10,2},{18... | collective-permute-start | bytes 393224 | tf_op jit(solution)/shard_map/ppermute | solution.py:234
  21.6 1.8 %collective-permute-done = bf16[8,64,128]{2,1,0:T(8,128)(2,1)S(1)} collective-permute-done((bf16[8,64,128]{2,1,0:T(8,128)(2,1)S(1)}, bf16[8,64,128]{2,1,0:T(8,128)(2,1)S(1)}, u32[]{:S(2)}, u32[]{:S(2)}) %collective-permute-start) | collective-permute-done | bytes 131104 | tf_op jit(solution)/shard_map/ppermute | solution.py:234
  23.4 2.5 %collective-permute-done.1 = bf16[8,64,128]{2,1,0:T(8,128)(2,1)S(1)} collective-permute-done((bf16[8,64,128]{2,1,0:T(8,128)(2,1)S(1)}, bf16[8,64,128]{2,1,0:T(8,128)(2,1)S(1)}, u32[]{:S(2)}, u32[]{:S(2)}) %collective-permute-start.1) | collective-permute-done | bytes 131104 | tf_op jit(solution)/shard_map/ppermute | solution.py:234
  25.9 1.3 %collective-permute-done.2 = bf16[8,64,128]{2,1,0:T(8,128)(2,1)S(1)} collective-permute-done((bf16[8,64,128]{2,1,0:T(8,128)(2,1)S(1)}, bf16[8,64,128]{2,1,0:T(8,128)(2,1)S(1)}, u32[]{:S(2)}, u32[]{:S(2)}) %collective-permute-start.2) | collective-permute-done | bytes 131104 | tf_op jit(solution)/shard_map/ppermute | solution.py:234
  27.2 3.8 %collective-permute-start.3 = (bf16[4,8,64,128]{3,2,1,0:T(8,128)(2,1)S(1)}, bf16[4,8,64,128]{3,2,1,0:T(8,128)(2,1)S(1)}, u32[]{:S(2)}, u32[]{:S(2)}) collective-permute-start(bf16[4,8,64,128]{3,2,1,0:T(8,128)(2,1)S(1)} %pad_maximum_fusion.refs_1_), channel_id=1, source_target_pairs={{0,4},{4,0},{1,5},{5,1},{2,6},{6,2},{3,7},{7,3},{8,12},{12,8},{9,1... | collective-permute-start | bytes 1572872 | tf_op jit(solution)/shard_map/ppermute | solution.py:28
  31.1 4.0 %fusion.2 = (bf16[512,4096]{1,0:T(8,128)(2,1)S(1)}, bf16[512,4096]{1,0:T(8,128)(2,1)S(1)}) fusion(bf16[1024,4096]{1,0:T(8,128)(2,1)} %param.11), kind=kLoop, calls=%fused_computation.6 | loop fusion | bytes 16777216 | tf_op jit(solution)/shard_map/slice | solution.py:237
  35.1 1.4 %shard_map.170 = (bf16[128,512]{1,0:T(8,128)(2,1)S(1)}, bf16[8,4,2,64,128]{4,3,2,1,0:T(8,128)(2,1)S(1)}) custom-call(bf16[512,4096]{1,0:T(8,128)(2,1)S(1)} %get-tuple-element.57.refs_0_, bf16[4,8,64,128]{3,2,1,0:T(8,128)(2,1)S(1)} %pad_maximum_fusion.refs_1_, bf16[4,8,64,128]{3,2,1,0:T(8,128)(2,1)S(1)} %collective-permute-done.3.refs_2_), custom_call_target="tpu_custom_call" | custom-call | flops 1073741824 | bytes 1048576 | tf_op jit(solution)/shard_map/pallas_call | solution.py:37
  36.5 1.3 %shard_map.171.refs_1_ = bf16[128,512]{1,0:T(8,128)(2,1)S(1)} custom-call(bf16[512,4096]{1,0:T(8,128)(2,1)S(1)} %get-tuple-element.56.refs_0_, bf16[8,4,2,64,128]{4,3,2,1,0:T(8,128)(2,1)S(1)} %get-tuple-element.33.refs_1_), custom_call_target="tpu_custom_call" | custom-call | flops 1073741824 | bytes 1048576 | tf_op jit(solution)/shard_map/pallas_call | solution.py:37
  37.8 2.8 %collective-permute-start.5 = (bf16[128,512]{1,0:T(8,128)(2,1)S(1)}, bf16[128,512]{1,0:T(8,128)(2,1)S(1)}, u32[]{:S(2)}, u32[]{:S(2)}) collective-permute-start(bf16[128,512]{1,0:T(8,128)(2,1)S(1)} %shard_map.171.refs_1_), channel_id=1, source_target_pairs={{0,3},{1,0},{2,1},{3,2},{4,7},{5,4},{6,5},{7,6},{8,11},{9,8},{10,9... | collective-permute-start | bytes 393224 | tf_op jit(solution)/shard_map/ppermute | solution.py:246
  40.6 2.7 %collective-permute-start.4 = (bf16[128,512]{1,0:T(8,128)(2,1)S(1)}, bf16[128,512]{1,0:T(8,128)(2,1)S(1)}, u32[]{:S(2)}, u32[]{:S(2)}) collective-permute-start(bf16[128,512]{1,0:T(8,128)(2,1)S(1)} %get-tuple-element.32.refs_0_), channel_id=1, source_target_pairs={{0,3},{1,0},{2,1},{3,2},{4,7},{5,4},{6,5},{7,6},{8,11},{9,8},{10,9... | collective-permute-start | bytes 393224 | tf_op jit(solution)/shard_map/ppermute | solution.py:244
  43.4 3.4 %collective-permute-start.8 = (bf16[128,512]{1,0:T(8,128)(2,1)S(1)}, bf16[128,512]{1,0:T(8,128)(2,1)S(1)}, u32[]{:S(2)}, u32[]{:S(2)}) collective-permute-start(bf16[128,512]{1,0:T(8,128)(2,1)S(1)} %collective-permute-done.5.refs_3_), channel_id=1, source_target_pairs={{0,3},{1,0},{2,1},{3,2},{4,7},{5,4},{6,5},{7,6},{8,11},{9,8},{10,9... | collective-permute-start | bytes 393224 | tf_op jit(solution)/shard_map/ppermute | solution.py:248
  46.9 2.5 %collective-permute-done.9.refs_7_ = bf16[128,512]{1,0:T(8,128)(2,1)S(1)} collective-permute-done((bf16[128,512]{1,0:T(8,128)(2,1)S(1)}, bf16[128,512]{1,0:T(8,128)(2,1)S(1)}, u32[]{:S(2)}, u32[]{:S(2)}) %collective-permute-start.9) | collective-permute-done | bytes 131104 | tf_op jit(solution)/shard_map/ppermute | solution.py:245
  49.4 2.5 %collective-permute-done.7.refs_4_ = bf16[128,512]{1,0:T(8,128)(2,1)S(1)} collective-permute-done((bf16[128,512]{1,0:T(8,128)(2,1)S(1)}, bf16[128,512]{1,0:T(8,128)(2,1)S(1)}, u32[]{:S(2)}, u32[]{:S(2)}) %collective-permute-start.7) | collective-permute-done | bytes 131104 | tf_op jit(solution)/shard_map/ppermute | solution.py:247
  52.6 2.9 %collective-permute-start.10 = (bf16[256,768]{1,0:T(8,128)(2,1)S(1)}, bf16[256,768]{1,0:T(8,128)(2,1)S(1)}, u32[]{:S(2)}, u32[]{:S(2)}) collective-permute-start(bf16[256,768]{1,0:T(8,128)(2,1)S(1)} %get-tuple-element.35), channel_id=1, source_target_pairs={{0,4},{4,0},{1,5},{5,1},{2,6},{6,2},{3,7},{7,3},{8,12},{12,8},{9,1... | collective-permute-start | bytes 1179656 | tf_op jit(solution)/shard_map/ppermute | solution.py:28
  57.7 3.9 %all-to-all-start.1 = ((bf16[32,8,768]{2,1,0:T(8,128)(2,1)}), bf16[32,8,768]{2,1,0:T(8,128)(2,1)S(1)}, u32[]{:S(2)}, u32[]{:S(2)}) async-start(bf16[32,8,768]{2,1,0:T(8,128)(2,1)} %fusion), calls=%async_computation.1 | async-start | bytes 786432 | tf_op jit(solution)/shard_map/all_to_all | solution.py:269
  63.3 12.7 %all-to-all-done.1.arrived = bf16[32,8,768]{2,1,0:T(8,128)(2,1)S(1)} async-done(((bf16[32,8,768]{2,1,0:T(8,128)(2,1)}), bf16[32,8,768]{2,1,0:T(8,128)(2,1)S(1)}, u32[]{:S(2)}, u32[]{:S(2)}) %all-to-all-start.1) | async-done | bytes 393248 | tf_op jit(solution)/shard_map/all_to_all | solution.py:269
  76.1 17.0 %all_to_all.16 = bf16[32,8,768]{2,1,0:T(8,128)(2,1)S(1)} all-to-all(bf16[32,8,768]{2,1,0:T(8,128)(2,1)S(1)} %get-tuple-element.38), channel_id=1, replica_groups=mesh['z'=8,'x'=4,'c'=2,'tp'=4] {'z','x'}, dimensions={0} | all-to-all | bytes 786432 | tf_op jit(solution)/shard_map/all_to_all | solution.py:273
  93.0 3.5 %collective-permute-start.12 = (bf16[256,768]{1,0:T(8,128)(2,1)S(1)}, bf16[256,768]{1,0:T(8,128)(2,1)S(1)}, u32[]{:S(2)}, u32[]{:S(2)}) collective-permute-start(bf16[256,768]{1,0:T(8,128)(2,1)S(1)} %bitcast.11), channel_id=1, source_target_pairs={{0,4},{4,0},{1,5},{5,1},{2,6},{6,2},{3,7},{7,3},{8,12},{12,8},{9,1... | collective-permute-start | bytes 1179656 | tf_op jit(solution)/shard_map/ppermute | solution.py:28
  97.6 9.0 %collective-permute-done.14.gram_y = f32[256,256]{1,0:T(8,128)S(1)} collective-permute-done((f32[256,256]{1,0:T(8,128)S(1)}, f32[256,256]{1,0:T(8,128)S(1)}, u32[]{:S(2)}, u32[]{:S(2)}) %collective-permute-start.14) | collective-permute-done | bytes 262176 | tf_op jit(solution)/shard_map/ppermute | solution.py:278
  106.5 1.1 shard_map.177
  107.7 1.5 %collective-permute-start.16 = (f32[1,128]{1,0:T(1,128)S(1)}, f32[1,128]{1,0:T(1,128)S(1)}, u32[]{:S(2)}, u32[]{:S(2)}) collective-permute-start(f32[1,128]{1,0:T(1,128)S(1)} %get-tuple-element.41.s0), channel_id=1, source_target_pairs={{0,2},{1,3},{2,0},{3,1},{4,6},{5,7},{6,4},{7,5},{8,10},{9,11},{10,... | collective-permute-start | bytes 1544 | tf_op jit(solution)/shard_map/ppermute | solution.py:289
  109.1 1.2 %collective-permute-start.17 = (f32[1,128]{1,0:T(1,128)S(1)}, f32[1,128]{1,0:T(1,128)S(1)}, u32[]{:S(2)}, u32[]{:S(2)}) collective-permute-start(f32[1,128]{1,0:T(1,128)S(1)} %get-tuple-element.41.s0), channel_id=1, source_target_pairs={{0,3},{1,0},{2,1},{3,2},{4,7},{5,4},{6,5},{7,6},{8,11},{9,8},{10,9... | collective-permute-start | bytes 1544 | tf_op jit(solution)/shard_map/ppermute | solution.py:289
  111.9 0.9 shard_map.178
  (53 shorter events, 9.3 us)
Async XLA Ops:
  18.0 5.4 %collective-permute-start = (bf16[8,64,128]{2,1,0:T(8,128)(2,1)S(1)}, bf16[8,64,128]{2,1,0:T(8,128)(2,1)S(1)}, u32[]{:S(2)}, u32[]{:S(2)}) collective-permute-start(bf16[8,64,128]{2,1,0:T(8,128)(2,1)S(1)} %all_to_all.15), channel_id=1, source_target_pairs={{8,0},{16,8},{24,16},{0,24},{9,1},{17,9},{25,17},{1,25},{10,2},{18... | collective-permute-start | bytes 393224 | tf_op jit(solution)/shard_map/ppermute | solution.py:234
  20.4 5.4 %collective-permute-start.1 = (bf16[8,64,128]{2,1,0:T(8,128)(2,1)S(1)}, bf16[8,64,128]{2,1,0:T(8,128)(2,1)S(1)}, u32[]{:S(2)}, u32[]{:S(2)}) collective-permute-start(bf16[8,64,128]{2,1,0:T(8,128)(2,1)S(1)} %all_to_all.15), channel_id=1, source_target_pairs={{16,0},{24,8},{0,16},{8,24},{17,1},{25,9},{1,17},{9,25},{18,2},{26... | collective-permute-start | bytes 393224 | tf_op jit(solution)/shard_map/ppermute | solution.py:234
  21.0 6.2 %collective-permute-start.2 = (bf16[8,64,128]{2,1,0:T(8,128)(2,1)S(1)}, bf16[8,64,128]{2,1,0:T(8,128)(2,1)S(1)}, u32[]{:S(2)}, u32[]{:S(2)}) collective-permute-start(bf16[8,64,128]{2,1,0:T(8,128)(2,1)S(1)} %all_to_all.15), channel_id=1, source_target_pairs={{24,0},{0,8},{8,16},{16,24},{25,1},{1,9},{9,17},{17,25},{26,2},{2,... | collective-permute-start | bytes 393224 | tf_op jit(solution)/shard_map/ppermute | solution.py:234
  27.2 7.8 %collective-permute-start.3 = (bf16[4,8,64,128]{3,2,1,0:T(8,128)(2,1)S(1)}, bf16[4,8,64,128]{3,2,1,0:T(8,128)(2,1)S(1)}, u32[]{:S(2)}, u32[]{:S(2)}) collective-permute-start(bf16[4,8,64,128]{3,2,1,0:T(8,128)(2,1)S(1)} %pad_maximum_fusion.refs_1_), channel_id=1, source_target_pairs={{0,4},{4,0},{1,5},{5,1},{2,6},{6,2},{3,7},{7,3},{8,12},{12,8},{9,1... | collective-permute-start | bytes 1572872 | tf_op jit(solution)/shard_map/ppermute | solution.py:28
  35.0 16.9 %copy-start = (bf16[1024,1024]{1,0:T(8,128)(2,1)S(1)}, bf16[1024,1024]{1,0:T(8,128)(2,1)}, u32[]{:S(2)}) copy-start(bf16[1024,1024]{1,0:T(8,128)(2,1)} %v_ref.1) | copy-start | bytes 6291460
  35.0 16.8 %copy-start.1 = (bf16[1024,512]{1,0:T(8,128)(2,1)S(1)}, bf16[1024,512]{1,0:T(8,128)(2,1)}, u32[]{:S(2)}) copy-start(bf16[1024,512]{1,0:T(8,128)(2,1)} %k_ref.1) | copy-start | bytes 3145732
  37.8 5.6 %collective-permute-start.5 = (bf16[128,512]{1,0:T(8,128)(2,1)S(1)}, bf16[128,512]{1,0:T(8,128)(2,1)S(1)}, u32[]{:S(2)}, u32[]{:S(2)}) collective-permute-start(bf16[128,512]{1,0:T(8,128)(2,1)S(1)} %shard_map.171.refs_1_), channel_id=1, source_target_pairs={{0,3},{1,0},{2,1},{3,2},{4,7},{5,4},{6,5},{7,6},{8,11},{9,8},{10,9... | collective-permute-start | bytes 393224 | tf_op jit(solution)/shard_map/ppermute | solution.py:246
  40.6 6.2 %collective-permute-start.6 = (bf16[128,512]{1,0:T(8,128)(2,1)S(1)}, bf16[128,512]{1,0:T(8,128)(2,1)S(1)}, u32[]{:S(2)}, u32[]{:S(2)}) collective-permute-start(bf16[128,512]{1,0:T(8,128)(2,1)S(1)} %get-tuple-element.32.refs_0_), channel_id=1, source_target_pairs={{0,1},{1,2},{2,3},{3,0},{4,5},{5,6},{6,7},{7,4},{8,9},{9,10},{10,1... | collective-permute-start | bytes 393224 | tf_op jit(solution)/shard_map/ppermute | solution.py:243
  40.6 8.8 %collective-permute-start.9 = (bf16[128,512]{1,0:T(8,128)(2,1)S(1)}, bf16[128,512]{1,0:T(8,128)(2,1)S(1)}, u32[]{:S(2)}, u32[]{:S(2)}) collective-permute-start(bf16[128,512]{1,0:T(8,128)(2,1)S(1)} %shard_map.171.refs_1_), channel_id=1, source_target_pairs={{0,1},{1,2},{2,3},{3,0},{4,5},{5,6},{6,7},{7,4},{8,9},{9,10},{10,1... | collective-permute-start | bytes 393224 | tf_op jit(solution)/shard_map/ppermute | solution.py:245
  40.6 8.7 %collective-permute-start.4 = (bf16[128,512]{1,0:T(8,128)(2,1)S(1)}, bf16[128,512]{1,0:T(8,128)(2,1)S(1)}, u32[]{:S(2)}, u32[]{:S(2)}) collective-permute-start(bf16[128,512]{1,0:T(8,128)(2,1)S(1)} %get-tuple-element.32.refs_0_), channel_id=1, source_target_pairs={{0,3},{1,0},{2,1},{3,2},{4,7},{5,4},{6,5},{7,6},{8,11},{9,8},{10,9... | collective-permute-start | bytes 393224 | tf_op jit(solution)/shard_map/ppermute | solution.py:244
  43.4 5.9 %collective-permute-start.8 = (bf16[128,512]{1,0:T(8,128)(2,1)S(1)}, bf16[128,512]{1,0:T(8,128)(2,1)S(1)}, u32[]{:S(2)}, u32[]{:S(2)}) collective-permute-start(bf16[128,512]{1,0:T(8,128)(2,1)S(1)} %collective-permute-done.5.refs_3_), channel_id=1, source_target_pairs={{0,3},{1,0},{2,1},{3,2},{4,7},{5,4},{6,5},{7,6},{8,11},{9,8},{10,9... | collective-permute-start | bytes 393224 | tf_op jit(solution)/shard_map/ppermute | solution.py:248
  46.9 5.0 %collective-permute-start.7 = (bf16[128,512]{1,0:T(8,128)(2,1)S(1)}, bf16[128,512]{1,0:T(8,128)(2,1)S(1)}, u32[]{:S(2)}, u32[]{:S(2)}) collective-permute-start(bf16[128,512]{1,0:T(8,128)(2,1)S(1)} %collective-permute-done.6.refs_6_), channel_id=1, source_target_pairs={{0,1},{1,2},{2,3},{3,0},{4,5},{5,6},{6,7},{7,4},{8,9},{9,10},{10,1... | collective-permute-start | bytes 393224 | tf_op jit(solution)/shard_map/ppermute | solution.py:247
  52.5 9.3 %copy-start.2 = (f32[64,1024]{1,0:T(8,128)S(1)}, f32[64,1024]{1,0:T(8,128)}, u32[]{:S(2)}) copy-start(f32[64,1024]{1,0:T(8,128)} %refs_3_.1) | copy-start | bytes 786436
  52.5 9.3 %copy-start.3 = (bf16[64,256]{1,0:T(8,128)(2,1)S(1)}, bf16[64,256]{1,0:T(8,128)(2,1)}, u32[]{:S(2)}) copy-start(bf16[64,256]{1,0:T(8,128)(2,1)} %refs_0_.1) | copy-start | bytes 98308
  52.6 4.2 %collective-permute-start.10 = (bf16[256,768]{1,0:T(8,128)(2,1)S(1)}, bf16[256,768]{1,0:T(8,128)(2,1)S(1)}, u32[]{:S(2)}, u32[]{:S(2)}) collective-permute-start(bf16[256,768]{1,0:T(8,128)(2,1)S(1)} %get-tuple-element.35), channel_id=1, source_target_pairs={{0,4},{4,0},{1,5},{5,1},{2,6},{6,2},{3,7},{7,3},{8,12},{12,8},{9,1... | collective-permute-start | bytes 1179656 | tf_op jit(solution)/shard_map/ppermute | solution.py:28
  57.7 18.3 %all-to-all-start.1 = ((bf16[32,8,768]{2,1,0:T(8,128)(2,1)}), bf16[32,8,768]{2,1,0:T(8,128)(2,1)S(1)}, u32[]{:S(2)}, u32[]{:S(2)}) async-start(bf16[32,8,768]{2,1,0:T(8,128)(2,1)} %fusion), calls=%async_computation.1 | async-start | bytes 786432 | tf_op jit(solution)/shard_map/all_to_all | solution.py:269
  61.6 35.0 %collective-permute-start.13 = (bf16[8,4,2,64,128]{4,3,2,1,0:T(8,128)(2,1)S(1)}, bf16[8,4,2,64,128]{4,3,2,1,0:T(8,128)(2,1)S(1)}, u32[]{:S(2)}, u32[]{:S(2)}) collective-permute-start(bf16[8,4,2,64,128]{4,3,2,1,0:T(8,128)(2,1)S(1)} %get-tuple-element.33.refs_1_), channel_id=1, source_target_pairs={{0,1},{1,0},{2,3},{3,2},{4,5},{5,4},{6,7},{7,6},{8,9},{9,8},{10,11... | collective-permute-start | bytes 3145736 | tf_op jit(solution)/shard_map/ppermute | solution.py:261
  62.0 1.3 %collective-permute-start.11 = (f32[8,768]{1,0:T(8,128)S(1)}, f32[8,768]{1,0:T(8,128)S(1)}, u32[]{:S(2)}, u32[]{:S(2)}) collective-permute-start(f32[8,768]{1,0:T(8,128)S(1)} %get-tuple-element.37), channel_id=1, source_target_pairs={{0,4},{4,0},{1,5},{5,1},{2,6},{6,2},{3,7},{7,3},{8,12},{12,8},{9,1... | collective-permute-start | bytes 73736 | tf_op jit(solution)/shard_map/ppermute | solution.py:28
  93.0 13.5 %collective-permute-start.12 = (bf16[256,768]{1,0:T(8,128)(2,1)S(1)}, bf16[256,768]{1,0:T(8,128)(2,1)S(1)}, u32[]{:S(2)}, u32[]{:S(2)}) collective-permute-start(bf16[256,768]{1,0:T(8,128)(2,1)S(1)} %bitcast.11), channel_id=1, source_target_pairs={{0,4},{4,0},{1,5},{5,1},{2,6},{6,2},{3,7},{7,3},{8,12},{12,8},{9,1... | collective-permute-start | bytes 1179656 | tf_op jit(solution)/shard_map/ppermute | solution.py:28
  97.4 9.2 %collective-permute-start.14 = (f32[256,256]{1,0:T(8,128)S(1)}, f32[256,256]{1,0:T(8,128)S(1)}, u32[]{:S(2)}, u32[]{:S(2)}) collective-permute-start(f32[256,256]{1,0:T(8,128)S(1)} %shard_map.176.gram), channel_id=1, source_target_pairs={{0,3},{1,2},{2,1},{3,0},{4,7},{5,6},{6,5},{7,4},{8,11},{9,10},{10,... | collective-permute-start | bytes 786440 | tf_op jit(solution)/shard_map/ppermute | solution.py:278
  97.5 12.9 %collective-permute-start.18 = (f32[8,768]{1,0:T(8,128)S(1)}, f32[8,768]{1,0:T(8,128)S(1)}, u32[]{:S(2)}, u32[]{:S(2)}) collective-permute-start(f32[8,768]{1,0:T(8,128)S(1)} %get-tuple-element.51), channel_id=1, source_target_pairs={{0,4},{4,0},{1,5},{5,1},{2,6},{6,2},{3,7},{7,3},{8,12},{12,8},{9,1... | collective-permute-start | bytes 73736 | tf_op jit(solution)/shard_map/ppermute | solution.py:28
  107.6 3.7 %collective-permute-start.15 = (f32[1,128]{1,0:T(1,128)S(1)}, f32[1,128]{1,0:T(1,128)S(1)}, u32[]{:S(2)}, u32[]{:S(2)}) collective-permute-start(f32[1,128]{1,0:T(1,128)S(1)} %get-tuple-element.41.s0), channel_id=1, source_target_pairs={{0,1},{1,2},{2,3},{3,0},{4,5},{5,6},{6,7},{7,4},{8,9},{9,10},{10,1... | collective-permute-start | bytes 1544 | tf_op jit(solution)/shard_map/ppermute | solution.py:289
  107.7 4.0 %collective-permute-start.16 = (f32[1,128]{1,0:T(1,128)S(1)}, f32[1,128]{1,0:T(1,128)S(1)}, u32[]{:S(2)}, u32[]{:S(2)}) collective-permute-start(f32[1,128]{1,0:T(1,128)S(1)} %get-tuple-element.41.s0), channel_id=1, source_target_pairs={{0,2},{1,3},{2,0},{3,1},{4,6},{5,7},{6,4},{7,5},{8,10},{9,11},{10,... | collective-permute-start | bytes 1544 | tf_op jit(solution)/shard_map/ppermute | solution.py:289
  109.1 2.7 %collective-permute-start.17 = (f32[1,128]{1,0:T(1,128)S(1)}, f32[1,128]{1,0:T(1,128)S(1)}, u32[]{:S(2)}, u32[]{:S(2)}) collective-permute-start(f32[1,128]{1,0:T(1,128)S(1)} %get-tuple-element.41.s0), channel_id=1, source_target_pairs={{0,3},{1,0},{2,1},{3,2},{4,7},{5,4},{6,5},{7,6},{8,11},{9,8},{10,9... | collective-permute-start | bytes 1544 | tf_op jit(solution)/shard_map/ppermute | solution.py:289
  (6 other events, 55.9 us)

commit v5 on v4

--- a/solution.py
+++ b/solution.py
@@ -13,6 +13,7 @@
 PLANE = ("z", "x")
 SWAP = [(0, 1), (1, 0)]
 BF = jnp.bfloat16
+FIRST = 512
 F32 = jnp.float32
 VMEM = pl.BlockSpec(memory_space=pltpu.VMEM)
 
@@ -159,45 +160,40 @@
     )
 
 
-def update_body(own, other, kb, vb, gram, gram_y, key_up, value_up, sums):
-    c, t = lax.axis_index("c"), lax.axis_index("tp")
-    kw, vw = key_up.shape[1] // 2, value_up.shape[1] // 2
-    is_key = t < 2
+def update_body(d, kb, vb, key_up, value_up):
+    kw = key_up.shape[1]
+    key_up[...] = jnp.dot(kb[...], d[:, :kw], preferred_element_type=F32)
+    value_up[...] = jnp.dot(vb[...], d[:, kw:], preferred_element_type=F32)
+
+
+def square_body(d, gram, gram_y, *refs):
+    before, sums = refs[:-1], refs[-1]
+    kw = d.shape[1] // 3
+    is_key = lax.axis_index("tp") < 2
     key_gram = jnp.where(is_key, gram[...], gram_y[...])
     value_gram = jnp.where(is_key, gram_y[...], gram[...])
-
-    def pieces(g):
-        a = g.astype(BF)
-        r = g - a.astype(F32)
-        b = r.astype(BF)
-        return a, b, (r - b.astype(F32)).astype(BF)
-
-    def square(ps, d):
-        gd = sum(jnp.dot(p, d, preferred_element_type=F32) for p in ps)
-        return jnp.sum(gd * d.astype(F32), axis=0, keepdims=True)
-
-    kp, vp = pieces(key_gram), pieces(value_gram)
-    ksq = jnp.zeros((1, kw), F32)
-    vsq = jnp.zeros((1, vw), F32)
-    for src, side in ((own, c), (other, 1 - c)):
-        dk, dv = src[:, :kw], src[:, kw:]
-        ks, vs = (pl.ds(pl.multiple_of(side * w, 128), w) for w in (kw, vw))
-        key_up[:, ks] = jnp.dot(kb[...], dk, preferred_element_type=F32)
-        value_up[:, vs] = jnp.dot(vb[...], dv, preferred_element_type=F32)
-        ksq += square(kp, dk)
-        vsq += square(vp, dv)
     lane = lax.broadcasted_iota(jnp.int32, sums.shape, 1)
-    sums[...] = jnp.where(lane == 0, jnp.sum(ksq), jnp.where(lane == 1, jnp.sum(vsq), 0.0))
-
-
-def finish_body(counts, s0, s1, s2, s3, ku, vu, kw, vw, kn, vn, kc, vc):
+    total = sum((ref[...] for ref in before), jnp.zeros(sums.shape, F32))
+    for at, g, cols in ((0, key_gram, d[:, :kw]), (1, value_gram, d[:, kw:])):
+        dd = lax.dot_general(
+            cols, cols, (((1,), (1,)), ((), ())), preferred_element_type=F32
+        )
+        total += jnp.where(lane == at, jnp.sum(g * dd), 0.0)
+    sums[...] = total
+
+
+def finish_body(counts, s0, s1, s2, s3, ku, ku_far, vu, vu_far, kw, vw, kn, vn, kc, vc):
+    c = lax.axis_index("c")
     total = (s0[...] + s1[...]) + (s2[...] + s3[...])
-    for lane, u, w, n, b in ((0, ku, kw, kn, kc), (1, vu, vw, vn, vc)):
+    for lane, ups, w, n, b in ((0, (ku, ku_far), kw, kn, kc), (1, (vu, vu_far), vw, vn, vc)):
         mean = total[:, lane : lane + 1] / counts[lane]
         factor = jnp.minimum(1.0, 0.5 * lax.rsqrt(mean + 1e-06))
-        new = w[...] - 0.25 * factor * u[...]
-        n[...] = new
-        b[...] = new.astype(BF)
+        for u, side in zip(ups, (c, 1 - c)):
+            width = u.shape[1]
+            at = pl.ds(pl.multiple_of(side * width, 128), width)
+            new = w[:, at] - 0.25 * factor * u[...]
+            n[:, at] = new
+            b[:, at] = new.astype(BF)
 
 
 def step(
@@ -224,7 +220,7 @@
 
     both = jnp.concatenate([key_basis, value_basis], axis=1)
     quarter = both.shape[1] // tp_size
-    tok = inputs.shape[0] // 2
+    tok = FIRST
     shard = lax.dynamic_slice_in_dim(both, t * quarter, quarter, axis=1)
     near = spread(shard, "z")
     x_size = lax.axis_size("x")
@@ -280,15 +276,20 @@
         own_new, other_core(back)
     )
 
-    key_up, value_up, sums = local(
-        update_body,
-        (shape(key_weight.shape), shape(value_weight.shape), shape((1, 128))),
-        8 * rank * rank * width,
-    )(own_dir, other_core(own_dir), key_rows, value_rows, gram, gram_y)
-    sums = [sums] + [
-        lax.ppermute(sums, "tp", [(i, (i + k) % tp_size) for i in range(tp_size)])
-        for k in range(1, tp_size)
-    ]
+    far_dir = other_core(own_dir)
+    sums = ()
+    for d in (own_dir, far_dir):
+        sums = local(square_body, shape((1, 128)), 4 * rank * rank * width)(d, gram, gram_y, *sums)
+        sums = (sums,)
+    (sums,) = sums
+    parts = [sums]
+    for away in range(1, tp_size):
+        parts.append(lax.ppermute(sums, "tp", [(i, (i + away) % tp_size) for i in range(tp_size)]))
+    sums = parts
+    ups = tuple(shape((a.shape[0], a.shape[1] // 2)) for a in (key_weight, value_weight))
+    key_up, value_up = zip(
+        *(local(update_body, ups)(d, key_rows, value_rows) for d in (own_dir, far_dir))
+    )
     counts = (float(key_weight.size * devices), float(value_weight.size * devices))
     key_new, value_new, key_copy, value_copy = local(
         functools.partial(finish_body, counts),
@@ -298,7 +299,7 @@
             shape(key_weight.shape, BF),
             shape(value_weight.shape, BF),
         ),
-    )(*sums, key_up, value_up, key_old, value_old)
+    )(*sums, *key_up, *value_up, key_old, value_old)
     key_mean_new, key_var_new, value_mean_new, value_var_new = new_moments
     return (
         key_new,

time: 114 us -> 114 us (level)
    pallas_call x10 -> x13, Pallas kernels: 7.45 us -> 7.73 us  [call(): pl.pallas_call(body, out_shape=outs, in_specs=[VMEM] * len(arrays), out_s...]
  transfers between devices with their start and end apart: 20 -> 20, of which waited for: 13 -> 12; matrix products, arithmetic and copies ran while one was open for 4% -> 4% of each run, Pallas kernels for 3% -> 3%
where the time goes in v5:
time: 114 us; the launch traced here: 113 us
  waiting for transfers between devices  34.5 us (30%)
  blocking collectives  33.5 us (29%)
  starting transfers between devices  30.3 us (27%)
  Pallas kernels  7.73 us (7%)
  local copies, waits for them, and re-layouts  4.04 us (4%)
  other arithmetic  1.63 us (1%)
    all_to_all x1, blocking collectives, step(): own_dir = lax.all_to_all(dirs, PLANE, 0, 0, tiled=True).reshape(rank, width)  17 us
    all_to_all x1, blocking collectives, spread(): lax.all_to_all(jnp.broadcast_to(shard[None], (peers, *shard.shape)), axes...  16.6 us
    all_to_all x1, waiting for transfers between devices, step(): lax.all_to_all(pair.reshape(planes, -1, width), PLANE, 0, 0, tiled=True)  12.7 us
    ppermute x5, starting transfers between devices, other_core(): return lax.ppermute(a, 'c', SWAP)  10.8 us
    ppermute x1, waiting for transfers between devices, step(): gram_y = lax.ppermute(gram, 'tp', across)  8.96 us
    pallas_call x13, Pallas kernels, call(): pl.pallas_call(body, out_shape=outs, in_specs=[VMEM] * len(arrays), out_s...  7.73 us
    ppermute x3, waiting for transfers between devices, step(): lax.ppermute(near, 'x', [((i + away) % x_size, i) for i in range(x_size)])  5.6 us
    slice x1, local copies, waits for them, and re-layouts, step(): x_first, x_last = (inputs[:tok], inputs[tok:])  3.96 us
  transfers between devices with their start and end apart: 20, of which 12 were waited for; matrix products, arithmetic and copies ran while one was open for 4% of the time, Pallas kernels for 3%

profile of v5, /device:TPU:1, one launch (start us, length us, event | category | flops | bytes accessed | tf_op | source)
XLA Modules:
  0.0 112.7 jit_solution(15732456661010324037)
XLA Ops:
  1.4 16.6 %all_to_all.15 = bf16[8,64,128]{2,1,0:T(8,128)(2,1)S(1)} all-to-all(bf16[8,64,128]{2,1,0:T(8,128)(2,1)S(1)} %broadcast_in_dim.2), channel_id=1, replica_groups=mesh['z'=8,'x'=4,'c'=2,'tp'=4] {'z'}, dimensions={0} | all-to-all | bytes 262144 | tf_op jit(solution)/shard_map/all_to_all | solution.py:23
  18.0 2.5 %collective-permute-start = (bf16[8,64,128]{2,1,0:T(8,128)(2,1)S(1)}, bf16[8,64,128]{2,1,0:T(8,128)(2,1)S(1)}, u32[]{:S(2)}, u32[]{:S(2)}) collective-permute-start(bf16[8,64,128]{2,1,0:T(8,128)(2,1)S(1)} %all_to_all.15), channel_id=1, source_target_pairs={{8,0},{16,8},{24,16},{0,24},{9,1},{17,9},{25,17},{1,25},{10,2},{18... | collective-permute-start | bytes 393224 | tf_op jit(solution)/shard_map/ppermute | solution.py:230
  21.6 1.8 %collective-permute-done = bf16[8,64,128]{2,1,0:T(8,128)(2,1)S(1)} collective-permute-done((bf16[8,64,128]{2,1,0:T(8,128)(2,1)S(1)}, bf16[8,64,128]{2,1,0:T(8,128)(2,1)S(1)}, u32[]{:S(2)}, u32[]{:S(2)}) %collective-permute-start) | collective-permute-done | bytes 131104 | tf_op jit(solution)/shard_map/ppermute | solution.py:230
  23.4 2.5 %collective-permute-done.1 = bf16[8,64,128]{2,1,0:T(8,128)(2,1)S(1)} collective-permute-done((bf16[8,64,128]{2,1,0:T(8,128)(2,1)S(1)}, bf16[8,64,128]{2,1,0:T(8,128)(2,1)S(1)}, u32[]{:S(2)}, u32[]{:S(2)}) %collective-permute-start.1) | collective-permute-done | bytes 131104 | tf_op jit(solution)/shard_map/ppermute | solution.py:230
  25.9 1.3 %collective-permute-done.2 = bf16[8,64,128]{2,1,0:T(8,128)(2,1)S(1)} collective-permute-done((bf16[8,64,128]{2,1,0:T(8,128)(2,1)S(1)}, bf16[8,64,128]{2,1,0:T(8,128)(2,1)S(1)}, u32[]{:S(2)}, u32[]{:S(2)}) %collective-permute-start.2) | collective-permute-done | bytes 131104 | tf_op jit(solution)/shard_map/ppermute | solution.py:230
  27.2 3.8 %collective-permute-start.3 = (bf16[4,8,64,128]{3,2,1,0:T(8,128)(2,1)S(1)}, bf16[4,8,64,128]{3,2,1,0:T(8,128)(2,1)S(1)}, u32[]{:S(2)}, u32[]{:S(2)}) collective-permute-start(bf16[4,8,64,128]{3,2,1,0:T(8,128)(2,1)S(1)} %pad_maximum_fusion.refs_1_), channel_id=1, source_target_pairs={{0,4},{4,0},{1,5},{5,1},{2,6},{6,2},{3,7},{7,3},{8,12},{12,8},{9,1... | collective-permute-start | bytes 1572872 | tf_op jit(solution)/shard_map/ppermute | solution.py:29
  31.1 4.0 %fusion.2 = (bf16[512,4096]{1,0:T(8,128)(2,1)S(1)}, bf16[512,4096]{1,0:T(8,128)(2,1)S(1)}) fusion(bf16[1024,4096]{1,0:T(8,128)(2,1)} %param.11), kind=kLoop, calls=%fused_computation.6 | loop fusion | bytes 16777216 | tf_op jit(solution)/shard_map/slice | solution.py:233
  35.1 1.4 %shard_map.170 = (bf16[128,512]{1,0:T(8,128)(2,1)S(1)}, bf16[8,4,2,64,128]{4,3,2,1,0:T(8,128)(2,1)S(1)}) custom-call(bf16[512,4096]{1,0:T(8,128)(2,1)S(1)} %get-tuple-element.59.refs_0_, bf16[4,8,64,128]{3,2,1,0:T(8,128)(2,1)S(1)} %pad_maximum_fusion.refs_1_, bf16[4,8,64,128]{3,2,1,0:T(8,128)(2,1)S(1)} %collective-permute-done.3.refs_2_), custom_call_target="tpu_custom_call" | custom-call | flops 1073741824 | bytes 1048576 | tf_op jit(solution)/shard_map/pallas_call | solution.py:38
  36.5 1.3 %shard_map.171.refs_1_ = bf16[128,512]{1,0:T(8,128)(2,1)S(1)} custom-call(bf16[512,4096]{1,0:T(8,128)(2,1)S(1)} %get-tuple-element.58.refs_0_, bf16[8,4,2,64,128]{4,3,2,1,0:T(8,128)(2,1)S(1)} %get-tuple-element.34.refs_1_), custom_call_target="tpu_custom_call" | custom-call | flops 1073741824 | bytes 1048576 | tf_op jit(solution)/shard_map/pallas_call | solution.py:38
  37.8 2.8 %collective-permute-start.5 = (bf16[128,512]{1,0:T(8,128)(2,1)S(1)}, bf16[128,512]{1,0:T(8,128)(2,1)S(1)}, u32[]{:S(2)}, u32[]{:S(2)}) collective-permute-start(bf16[128,512]{1,0:T(8,128)(2,1)S(1)} %shard_map.171.refs_1_), channel_id=1, source_target_pairs={{0,3},{1,0},{2,1},{3,2},{4,7},{5,4},{6,5},{7,6},{8,11},{9,8},{10,9... | collective-permute-start | bytes 393224 | tf_op jit(solution)/shard_map/ppermute | solution.py:242
  40.6 2.7 %collective-permute-start.4 = (bf16[128,512]{1,0:T(8,128)(2,1)S(1)}, bf16[128,512]{1,0:T(8,128)(2,1)S(1)}, u32[]{:S(2)}, u32[]{:S(2)}) collective-permute-start(bf16[128,512]{1,0:T(8,128)(2,1)S(1)} %get-tuple-element.33.refs_0_), channel_id=1, source_target_pairs={{0,3},{1,0},{2,1},{3,2},{4,7},{5,4},{6,5},{7,6},{8,11},{9,8},{10,9... | collective-permute-start | bytes 393224 | tf_op jit(solution)/shard_map/ppermute | solution.py:240
  43.4 3.4 %collective-permute-start.8 = (bf16[128,512]{1,0:T(8,128)(2,1)S(1)}, bf16[128,512]{1,0:T(8,128)(2,1)S(1)}, u32[]{:S(2)}, u32[]{:S(2)}) collective-permute-start(bf16[128,512]{1,0:T(8,128)(2,1)S(1)} %collective-permute-done.5.refs_3_), channel_id=1, source_target_pairs={{0,3},{1,0},{2,1},{3,2},{4,7},{5,4},{6,5},{7,6},{8,11},{9,8},{10,9... | collective-permute-start | bytes 393224 | tf_op jit(solution)/shard_map/ppermute | solution.py:244
  46.9 2.5 %collective-permute-done.9.refs_7_ = bf16[128,512]{1,0:T(8,128)(2,1)S(1)} collective-permute-done((bf16[128,512]{1,0:T(8,128)(2,1)S(1)}, bf16[128,512]{1,0:T(8,128)(2,1)S(1)}, u32[]{:S(2)}, u32[]{:S(2)}) %collective-permute-start.9) | collective-permute-done | bytes 131104 | tf_op jit(solution)/shard_map/ppermute | solution.py:241
  49.4 2.5 %collective-permute-done.7.refs_4_ = bf16[128,512]{1,0:T(8,128)(2,1)S(1)} collective-permute-done((bf16[128,512]{1,0:T(8,128)(2,1)S(1)}, bf16[128,512]{1,0:T(8,128)(2,1)S(1)}, u32[]{:S(2)}, u32[]{:S(2)}) %collective-permute-start.7) | collective-permute-done | bytes 131104 | tf_op jit(solution)/shard_map/ppermute | solution.py:243
  52.6 2.9 %collective-permute-start.10 = (bf16[256,768]{1,0:T(8,128)(2,1)S(1)}, bf16[256,768]{1,0:T(8,128)(2,1)S(1)}, u32[]{:S(2)}, u32[]{:S(2)}) collective-permute-start(bf16[256,768]{1,0:T(8,128)(2,1)S(1)} %get-tuple-element.36), channel_id=1, source_target_pairs={{0,4},{4,0},{1,5},{5,1},{2,6},{6,2},{3,7},{7,3},{8,12},{12,8},{9,1... | collective-permute-start | bytes 1179656 | tf_op jit(solution)/shard_map/ppermute | solution.py:29
  57.7 3.9 %all-to-all-start.1 = ((bf16[32,8,768]{2,1,0:T(8,128)(2,1)}), bf16[32,8,768]{2,1,0:T(8,128)(2,1)S(1)}, u32[]{:S(2)}, u32[]{:S(2)}) async-start(bf16[32,8,768]{2,1,0:T(8,128)(2,1)} %fusion), calls=%async_computation.1 | async-start | bytes 786432 | tf_op jit(solution)/shard_map/all_to_all | solution.py:265
  62.4 0.8 collective-permute-done.11.theirs
  63.3 12.7 %all-to-all-done.1.arrived = bf16[32,8,768]{2,1,0:T(8,128)(2,1)S(1)} async-done(((bf16[32,8,768]{2,1,0:T(8,128)(2,1)}), bf16[32,8,768]{2,1,0:T(8,128)(2,1)S(1)}, u32[]{:S(2)}, u32[]{:S(2)}) %all-to-all-start.1) | async-done | bytes 393248 | tf_op jit(solution)/shard_map/all_to_all | solution.py:265
  76.1 17.0 %all_to_all.16 = bf16[32,8,768]{2,1,0:T(8,128)(2,1)S(1)} all-to-all(bf16[32,8,768]{2,1,0:T(8,128)(2,1)S(1)} %get-tuple-element.39), channel_id=1, replica_groups=mesh['z'=8,'x'=4,'c'=2,'tp'=4] {'z','x'}, dimensions={0} | all-to-all | bytes 786432 | tf_op jit(solution)/shard_map/all_to_all | solution.py:269
  93.0 3.5 %collective-permute-start.12 = (bf16[256,768]{1,0:T(8,128)(2,1)S(1)}, bf16[256,768]{1,0:T(8,128)(2,1)S(1)}, u32[]{:S(2)}, u32[]{:S(2)}) collective-permute-start(bf16[256,768]{1,0:T(8,128)(2,1)S(1)} %bitcast.10), channel_id=1, source_target_pairs={{0,4},{4,0},{1,5},{5,1},{2,6},{6,2},{3,7},{7,3},{8,12},{12,8},{9,1... | collective-permute-start | bytes 1179656 | tf_op jit(solution)/shard_map/ppermute | solution.py:29
  97.6 9.0 %collective-permute-done.14.gram_y = f32[256,256]{1,0:T(8,128)S(1)} collective-permute-done((f32[256,256]{1,0:T(8,128)S(1)}, f32[256,256]{1,0:T(8,128)S(1)}, u32[]{:S(2)}, u32[]{:S(2)}) %collective-permute-start.14) | collective-permute-done | bytes 262176 | tf_op jit(solution)/shard_map/ppermute | solution.py:274
  107.6 1.5 %collective-permute-start.16 = (f32[1,128]{1,0:T(1,128)S(1)}, f32[1,128]{1,0:T(1,128)S(1)}, u32[]{:S(2)}, u32[]{:S(2)}) collective-permute-start(f32[1,128]{1,0:T(1,128)S(1)} %shard_map.178.s0), channel_id=1, source_target_pairs={{0,2},{1,3},{2,0},{3,1},{4,6},{5,7},{6,4},{7,5},{8,10},{9,11},{10,... | collective-permute-start | bytes 1544 | tf_op jit(solution)/shard_map/ppermute | solution.py:287
  109.0 1.2 %collective-permute-start.17 = (f32[1,128]{1,0:T(1,128)S(1)}, f32[1,128]{1,0:T(1,128)S(1)}, u32[]{:S(2)}, u32[]{:S(2)}) collective-permute-start(f32[1,128]{1,0:T(1,128)S(1)} %shard_map.178.s0), channel_id=1, source_target_pairs={{0,3},{1,0},{2,1},{3,2},{4,7},{5,4},{6,5},{7,6},{8,11},{9,8},{10,9... | collective-permute-start | bytes 1544 | tf_op jit(solution)/shard_map/ppermute | solution.py:287
  111.8 0.9 shard_map.181
  (56 shorter events, 9.4 us)
Async XLA Ops:
  18.0 5.4 %collective-permute-start = (bf16[8,64,128]{2,1,0:T(8,128)(2,1)S(1)}, bf16[8,64,128]{2,1,0:T(8,128)(2,1)S(1)}, u32[]{:S(2)}, u32[]{:S(2)}) collective-permute-start(bf16[8,64,128]{2,1,0:T(8,128)(2,1)S(1)} %all_to_all.15), channel_id=1, source_target_pairs={{8,0},{16,8},{24,16},{0,24},{9,1},{17,9},{25,17},{1,25},{10,2},{18... | collective-permute-start | bytes 393224 | tf_op jit(solution)/shard_map/ppermute | solution.py:230
  20.4 5.4 %collective-permute-start.1 = (bf16[8,64,128]{2,1,0:T(8,128)(2,1)S(1)}, bf16[8,64,128]{2,1,0:T(8,128)(2,1)S(1)}, u32[]{:S(2)}, u32[]{:S(2)}) collective-permute-start(bf16[8,64,128]{2,1,0:T(8,128)(2,1)S(1)} %all_to_all.15), channel_id=1, source_target_pairs={{16,0},{24,8},{0,16},{8,24},{17,1},{25,9},{1,17},{9,25},{18,2},{26... | collective-permute-start | bytes 393224 | tf_op jit(solution)/shard_map/ppermute | solution.py:230
  21.0 6.2 %collective-permute-start.2 = (bf16[8,64,128]{2,1,0:T(8,128)(2,1)S(1)}, bf16[8,64,128]{2,1,0:T(8,128)(2,1)S(1)}, u32[]{:S(2)}, u32[]{:S(2)}) collective-permute-start(bf16[8,64,128]{2,1,0:T(8,128)(2,1)S(1)} %all_to_all.15), channel_id=1, source_target_pairs={{24,0},{0,8},{8,16},{16,24},{25,1},{1,9},{9,17},{17,25},{26,2},{2,... | collective-permute-start | bytes 393224 | tf_op jit(solution)/shard_map/ppermute | solution.py:230
  27.2 7.8 %collective-permute-start.3 = (bf16[4,8,64,128]{3,2,1,0:T(8,128)(2,1)S(1)}, bf16[4,8,64,128]{3,2,1,0:T(8,128)(2,1)S(1)}, u32[]{:S(2)}, u32[]{:S(2)}) collective-permute-start(bf16[4,8,64,128]{3,2,1,0:T(8,128)(2,1)S(1)} %pad_maximum_fusion.refs_1_), channel_id=1, source_target_pairs={{0,4},{4,0},{1,5},{5,1},{2,6},{6,2},{3,7},{7,3},{8,12},{12,8},{9,1... | collective-permute-start | bytes 1572872 | tf_op jit(solution)/shard_map/ppermute | solution.py:29
  35.0 16.9 %copy-start = (bf16[1024,1024]{1,0:T(8,128)(2,1)S(1)}, bf16[1024,1024]{1,0:T(8,128)(2,1)}, u32[]{:S(2)}) copy-start(bf16[1024,1024]{1,0:T(8,128)(2,1)} %v_ref.1) | copy-start | bytes 6291460
  35.0 16.8 %copy-start.1 = (bf16[1024,512]{1,0:T(8,128)(2,1)S(1)}, bf16[1024,512]{1,0:T(8,128)(2,1)}, u32[]{:S(2)}) copy-start(bf16[1024,512]{1,0:T(8,128)(2,1)} %k_ref.1) | copy-start | bytes 3145732
  37.8 5.6 %collective-permute-start.5 = (bf16[128,512]{1,0:T(8,128)(2,1)S(1)}, bf16[128,512]{1,0:T(8,128)(2,1)S(1)}, u32[]{:S(2)}, u32[]{:S(2)}) collective-permute-start(bf16[128,512]{1,0:T(8,128)(2,1)S(1)} %shard_map.171.refs_1_), channel_id=1, source_target_pairs={{0,3},{1,0},{2,1},{3,2},{4,7},{5,4},{6,5},{7,6},{8,11},{9,8},{10,9... | collective-permute-start | bytes 393224 | tf_op jit(solution)/shard_map/ppermute | solution.py:242
  40.6 6.2 %collective-permute-start.6 = (bf16[128,512]{1,0:T(8,128)(2,1)S(1)}, bf16[128,512]{1,0:T(8,128)(2,1)S(1)}, u32[]{:S(2)}, u32[]{:S(2)}) collective-permute-start(bf16[128,512]{1,0:T(8,128)(2,1)S(1)} %get-tuple-element.33.refs_0_), channel_id=1, source_target_pairs={{0,1},{1,2},{2,3},{3,0},{4,5},{5,6},{6,7},{7,4},{8,9},{9,10},{10,1... | collective-permute-start | bytes 393224 | tf_op jit(solution)/shard_map/ppermute | solution.py:239
  40.6 8.8 %collective-permute-start.9 = (bf16[128,512]{1,0:T(8,128)(2,1)S(1)}, bf16[128,512]{1,0:T(8,128)(2,1)S(1)}, u32[]{:S(2)}, u32[]{:S(2)}) collective-permute-start(bf16[128,512]{1,0:T(8,128)(2,1)S(1)} %shard_map.171.refs_1_), channel_id=1, source_target_pairs={{0,1},{1,2},{2,3},{3,0},{4,5},{5,6},{6,7},{7,4},{8,9},{9,10},{10,1... | collective-permute-start | bytes 393224 | tf_op jit(solution)/shard_map/ppermute | solution.py:241
  40.6 8.7 %collective-permute-start.4 = (bf16[128,512]{1,0:T(8,128)(2,1)S(1)}, bf16[128,512]{1,0:T(8,128)(2,1)S(1)}, u32[]{:S(2)}, u32[]{:S(2)}) collective-permute-start(bf16[128,512]{1,0:T(8,128)(2,1)S(1)} %get-tuple-element.33.refs_0_), channel_id=1, source_target_pairs={{0,3},{1,0},{2,1},{3,2},{4,7},{5,4},{6,5},{7,6},{8,11},{9,8},{10,9... | collective-permute-start | bytes 393224 | tf_op jit(solution)/shard_map/ppermute | solution.py:240
  43.4 5.9 %collective-permute-start.8 = (bf16[128,512]{1,0:T(8,128)(2,1)S(1)}, bf16[128,512]{1,0:T(8,128)(2,1)S(1)}, u32[]{:S(2)}, u32[]{:S(2)}) collective-permute-start(bf16[128,512]{1,0:T(8,128)(2,1)S(1)} %collective-permute-done.5.refs_3_), channel_id=1, source_target_pairs={{0,3},{1,0},{2,1},{3,2},{4,7},{5,4},{6,5},{7,6},{8,11},{9,8},{10,9... | collective-permute-start | bytes 393224 | tf_op jit(solution)/shard_map/ppermute | solution.py:244
  46.9 5.0 %collective-permute-start.7 = (bf16[128,512]{1,0:T(8,128)(2,1)S(1)}, bf16[128,512]{1,0:T(8,128)(2,1)S(1)}, u32[]{:S(2)}, u32[]{:S(2)}) collective-permute-start(bf16[128,512]{1,0:T(8,128)(2,1)S(1)} %collective-permute-done.6.refs_6_), channel_id=1, source_target_pairs={{0,1},{1,2},{2,3},{3,0},{4,5},{5,6},{6,7},{7,4},{8,9},{9,10},{10,1... | collective-permute-start | bytes 393224 | tf_op jit(solution)/shard_map/ppermute | solution.py:243
  52.5 9.3 %copy-start.2 = (f32[64,1024]{1,0:T(8,128)S(1)}, f32[64,1024]{1,0:T(8,128)}, u32[]{:S(2)}) copy-start(f32[64,1024]{1,0:T(8,128)} %refs_3_.1) | copy-start | bytes 786436
  52.5 9.3 %copy-start.3 = (bf16[64,256]{1,0:T(8,128)(2,1)S(1)}, bf16[64,256]{1,0:T(8,128)(2,1)}, u32[]{:S(2)}) copy-start(bf16[64,256]{1,0:T(8,128)(2,1)} %refs_0_.1) | copy-start | bytes 98308
  52.6 4.2 %collective-permute-start.10 = (bf16[256,768]{1,0:T(8,128)(2,1)S(1)}, bf16[256,768]{1,0:T(8,128)(2,1)S(1)}, u32[]{:S(2)}, u32[]{:S(2)}) collective-permute-start(bf16[256,768]{1,0:T(8,128)(2,1)S(1)} %get-tuple-element.36), channel_id=1, source_target_pairs={{0,4},{4,0},{1,5},{5,1},{2,6},{6,2},{3,7},{7,3},{8,12},{12,8},{9,1... | collective-permute-start | bytes 1179656 | tf_op jit(solution)/shard_map/ppermute | solution.py:29
  57.7 18.3 %all-to-all-start.1 = ((bf16[32,8,768]{2,1,0:T(8,128)(2,1)}), bf16[32,8,768]{2,1,0:T(8,128)(2,1)S(1)}, u32[]{:S(2)}, u32[]{:S(2)}) async-start(bf16[32,8,768]{2,1,0:T(8,128)(2,1)} %fusion), calls=%async_computation.1 | async-start | bytes 786432 | tf_op jit(solution)/shard_map/all_to_all | solution.py:265
  61.6 35.0 %collective-permute-start.13 = (bf16[8,4,2,64,128]{4,3,2,1,0:T(8,128)(2,1)S(1)}, bf16[8,4,2,64,128]{4,3,2,1,0:T(8,128)(2,1)S(1)}, u32[]{:S(2)}, u32[]{:S(2)}) collective-permute-start(bf16[8,4,2,64,128]{4,3,2,1,0:T(8,128)(2,1)S(1)} %get-tuple-element.34.refs_1_), channel_id=1, source_target_pairs={{0,1},{1,0},{2,3},{3,2},{4,5},{5,4},{6,7},{7,6},{8,9},{9,8},{10,11... | collective-permute-start | bytes 3145736 | tf_op jit(solution)/shard_map/ppermute | solution.py:257
  62.0 1.3 %collective-permute-start.11 = (f32[8,768]{1,0:T(8,128)S(1)}, f32[8,768]{1,0:T(8,128)S(1)}, u32[]{:S(2)}, u32[]{:S(2)}) collective-permute-start(f32[8,768]{1,0:T(8,128)S(1)} %get-tuple-element.38), channel_id=1, source_target_pairs={{0,4},{4,0},{1,5},{5,1},{2,6},{6,2},{3,7},{7,3},{8,12},{12,8},{9,1... | collective-permute-start | bytes 73736 | tf_op jit(solution)/shard_map/ppermute | solution.py:29
  93.0 14.0 %collective-permute-start.12 = (bf16[256,768]{1,0:T(8,128)(2,1)S(1)}, bf16[256,768]{1,0:T(8,128)(2,1)S(1)}, u32[]{:S(2)}, u32[]{:S(2)}) collective-permute-start(bf16[256,768]{1,0:T(8,128)(2,1)S(1)} %bitcast.10), channel_id=1, source_target_pairs={{0,4},{4,0},{1,5},{5,1},{2,6},{6,2},{3,7},{7,3},{8,12},{12,8},{9,1... | collective-permute-start | bytes 1179656 | tf_op jit(solution)/shard_map/ppermute | solution.py:29
  97.4 9.2 %collective-permute-start.14 = (f32[256,256]{1,0:T(8,128)S(1)}, f32[256,256]{1,0:T(8,128)S(1)}, u32[]{:S(2)}, u32[]{:S(2)}) collective-permute-start(f32[256,256]{1,0:T(8,128)S(1)} %shard_map.176.gram), channel_id=1, source_target_pairs={{0,3},{1,2},{2,1},{3,0},{4,7},{5,6},{6,5},{7,4},{8,11},{9,10},{10,... | collective-permute-start | bytes 786440 | tf_op jit(solution)/shard_map/ppermute | solution.py:274
  97.5 12.8 %collective-permute-start.18 = (f32[8,768]{1,0:T(8,128)S(1)}, f32[8,768]{1,0:T(8,128)S(1)}, u32[]{:S(2)}, u32[]{:S(2)}) collective-permute-start(f32[8,768]{1,0:T(8,128)S(1)} %get-tuple-element.53), channel_id=1, source_target_pairs={{0,4},{4,0},{1,5},{5,1},{2,6},{6,2},{3,7},{7,3},{8,12},{12,8},{9,1... | collective-permute-start | bytes 73736 | tf_op jit(solution)/shard_map/ppermute | solution.py:29
  107.5 3.8 %collective-permute-start.15 = (f32[1,128]{1,0:T(1,128)S(1)}, f32[1,128]{1,0:T(1,128)S(1)}, u32[]{:S(2)}, u32[]{:S(2)}) collective-permute-start(f32[1,128]{1,0:T(1,128)S(1)} %shard_map.178.s0), channel_id=1, source_target_pairs={{0,1},{1,2},{2,3},{3,0},{4,5},{5,6},{6,7},{7,4},{8,9},{9,10},{10,1... | collective-permute-start | bytes 1544 | tf_op jit(solution)/shard_map/ppermute | solution.py:287
  107.6 4.0 %collective-permute-start.16 = (f32[1,128]{1,0:T(1,128)S(1)}, f32[1,128]{1,0:T(1,128)S(1)}, u32[]{:S(2)}, u32[]{:S(2)}) collective-permute-start(f32[1,128]{1,0:T(1,128)S(1)} %shard_map.178.s0), channel_id=1, source_target_pairs={{0,2},{1,3},{2,0},{3,1},{4,6},{5,7},{6,4},{7,5},{8,10},{9,11},{10,... | collective-permute-start | bytes 1544 | tf_op jit(solution)/shard_map/ppermute | solution.py:287
  109.0 2.7 %collective-permute-start.17 = (f32[1,128]{1,0:T(1,128)S(1)}, f32[1,128]{1,0:T(1,128)S(1)}, u32[]{:S(2)}, u32[]{:S(2)}) collective-permute-start(f32[1,128]{1,0:T(1,128)S(1)} %shard_map.178.s0), channel_id=1, source_target_pairs={{0,3},{1,0},{2,1},{3,2},{4,7},{5,4},{6,5},{7,6},{8,11},{9,8},{10,9... | collective-permute-start | bytes 1544 | tf_op jit(solution)/shard_map/ppermute | solution.py:287
  (6 other events, 55.8 us)

commit v6 on v5

--- a/solution.py
+++ b/solution.py
@@ -47,6 +47,38 @@
         )(*arrays)
 
     return call
+
+
+STRIP = 128
+
+
+def staged_body(x_ref, *refs):
+    outs, sems = refs[:-1], refs[-1]
+    copies, at = [], 0
+    for out in outs:
+        for row in range(0, out.shape[0], STRIP):
+            src = x_ref.at[pl.ds(at, STRIP)]
+            copies.append(
+                pltpu.make_async_copy(src, out.at[pl.ds(row, STRIP)], sems.at[len(copies)])
+            )
+            at += STRIP
+    for copy in copies:
+        copy.start()
+    for copy in copies:
+        copy.wait()
+
+
+def staged(x, cuts):
+    return pl.pallas_call(
+        staged_body,
+        out_shape=tuple(shape((rows, x.shape[1]), x.dtype) for rows in cuts),
+        in_specs=[pl.BlockSpec(memory_space=pltpu.HBM)],
+        out_specs=(VMEM,) * len(cuts),
+        scratch_shapes=[pltpu.SemaphoreType.DMA((x.shape[0] // STRIP,))],
+        name="staged",
+        compiler_params=pltpu.CompilerParams(vmem_limit_bytes=44 << 20),
+        cost_estimate=pl.CostEstimate(flops=1 << 22, bytes_accessed=2 * x.size, transcendentals=0),
+    )(x)
 
 
 def mapped_body(fresh, *refs):
@@ -230,7 +262,7 @@
             lax.ppermute(near, "x", [((i + away) % x_size, i) for i in range(x_size)])
         )
     own = jnp.stack(own)
-    x_first, x_last = inputs[:tok], inputs[tok:]
+    x_first, x_last = staged(inputs, (tok, inputs.shape[0] - tok))
     first, basis = mapped_kernel(x_first, own, other_core(own))
     last = mapped_kernel(x_last, basis)
 

time: 114 us -> 114 us (level)
  local copies, waits for them, and re-layouts: 4.04 us -> 0.08 us
  Pallas kernels: 7.73 us -> 11.2 us
    slice x1 -> x0, local copies, waits for them, and re-layouts: 3.96 us -> none  [step(): x_first, x_last = (inputs[:tok], inputs[tok:])]
    pallas_call x0 -> x1, Pallas kernels: none -> 3.47 us  [staged(): pl.pallas_call(staged_body, out_shape=tuple((shape((rows, x.shape[1]), x....]
  transfers between devices with their start and end apart: 20 -> 20, of which waited for: 12 -> 12; matrix products, arithmetic and copies ran while one was open for 4% -> 0% of each run, Pallas kernels for 3% -> 6%
where the time goes in v6:
time: 114 us; the launch traced here: 112 us
  waiting for transfers between devices  34.5 us (30%)
  blocking collectives  33.5 us (29%)
  starting transfers between devices  30.3 us (27%)
  Pallas kernels  11.2 us (10%)
  other arithmetic  1.63 us (1%)
    all_to_all x1, blocking collectives, step(): own_dir = lax.all_to_all(dirs, PLANE, 0, 0, tiled=True).reshape(rank, width)  17 us
    all_to_all x1, blocking collectives, spread(): lax.all_to_all(jnp.broadcast_to(shard[None], (peers, *shard.shape)), axes...  16.6 us
    all_to_all x1, waiting for transfers between devices, step(): lax.all_to_all(pair.reshape(planes, -1, width), PLANE, 0, 0, tiled=True)  12.7 us
    ppermute x5, starting transfers between devices, other_core(): return lax.ppermute(a, 'c', SWAP)  11 us
    ppermute x1, waiting for transfers between devices, step(): gram_y = lax.ppermute(gram, 'tp', across)  8.96 us
    pallas_call x13, Pallas kernels, call(): pl.pallas_call(body, out_shape=outs, in_specs=[VMEM] * len(arrays), out_s...  7.7 us
    ppermute x3, waiting for transfers between devices, step(): lax.ppermute(near, 'x', [((i + away) % x_size, i) for i in range(x_size)])  5.6 us
    all_to_all x1, starting transfers between devices, step(): lax.all_to_all(pair.reshape(planes, -1, width), PLANE, 0, 0, tiled=True)  3.88 us
  transfers between devices with their start and end apart: 20, of which 12 were waited for; matrix products, arithmetic and copies ran while one was open for 0% of the time, Pallas kernels for 6%

profile of v6, /device:TPU:1, one launch (start us, length us, event | category | flops | bytes accessed | tf_op | source)
XLA Modules:
  0.0 112.2 jit_solution(10791012522456984060)
XLA Ops:
  1.4 16.6 %all_to_all.15 = bf16[8,64,128]{2,1,0:T(8,128)(2,1)S(1)} all-to-all(bf16[8,64,128]{2,1,0:T(8,128)(2,1)S(1)} %broadcast_in_dim.2), channel_id=1, replica_groups=mesh['z'=8,'x'=4,'c'=2,'tp'=4] {'z'}, dimensions={0} | all-to-all | bytes 262144 | tf_op jit(solution)/shard_map/all_to_all | solution.py:23
  18.0 2.5 %collective-permute-start = (bf16[8,64,128]{2,1,0:T(8,128)(2,1)S(1)}, bf16[8,64,128]{2,1,0:T(8,128)(2,1)S(1)}, u32[]{:S(2)}, u32[]{:S(2)}) collective-permute-start(bf16[8,64,128]{2,1,0:T(8,128)(2,1)S(1)} %all_to_all.15), channel_id=1, source_target_pairs={{8,0},{16,8},{24,16},{0,24},{9,1},{17,9},{25,17},{1,25},{10,2},{18... | collective-permute-start | bytes 393224 | tf_op jit(solution)/shard_map/ppermute | solution.py:262
  21.6 1.8 %collective-permute-done = bf16[8,64,128]{2,1,0:T(8,128)(2,1)S(1)} collective-permute-done((bf16[8,64,128]{2,1,0:T(8,128)(2,1)S(1)}, bf16[8,64,128]{2,1,0:T(8,128)(2,1)S(1)}, u32[]{:S(2)}, u32[]{:S(2)}) %collective-permute-start) | collective-permute-done | bytes 131104 | tf_op jit(solution)/shard_map/ppermute | solution.py:262
  23.4 2.5 %collective-permute-done.1 = bf16[8,64,128]{2,1,0:T(8,128)(2,1)S(1)} collective-permute-done((bf16[8,64,128]{2,1,0:T(8,128)(2,1)S(1)}, bf16[8,64,128]{2,1,0:T(8,128)(2,1)S(1)}, u32[]{:S(2)}, u32[]{:S(2)}) %collective-permute-start.1) | collective-permute-done | bytes 131104 | tf_op jit(solution)/shard_map/ppermute | solution.py:262
  25.9 1.3 %collective-permute-done.2 = bf16[8,64,128]{2,1,0:T(8,128)(2,1)S(1)} collective-permute-done((bf16[8,64,128]{2,1,0:T(8,128)(2,1)S(1)}, bf16[8,64,128]{2,1,0:T(8,128)(2,1)S(1)}, u32[]{:S(2)}, u32[]{:S(2)}) %collective-permute-start.2) | collective-permute-done | bytes 131104 | tf_op jit(solution)/shard_map/ppermute | solution.py:262
  27.2 3.8 %collective-permute-start.3 = (bf16[4,8,64,128]{3,2,1,0:T(8,128)(2,1)S(1)}, bf16[4,8,64,128]{3,2,1,0:T(8,128)(2,1)S(1)}, u32[]{:S(2)}, u32[]{:S(2)}) collective-permute-start(bf16[4,8,64,128]{3,2,1,0:T(8,128)(2,1)S(1)} %pad_maximum_fusion.refs_1_), channel_id=1, source_target_pairs={{0,4},{4,0},{1,5},{5,1},{2,6},{6,2},{3,7},{7,3},{8,12},{12,8},{9,1... | collective-permute-start | bytes 1572872 | tf_op jit(solution)/shard_map/ppermute | solution.py:29
  31.1 3.5 %staged.1 = (bf16[512,4096]{1,0:T(8,128)(2,1)S(1)}, bf16[512,4096]{1,0:T(8,128)(2,1)S(1)}) custom-call(bf16[1024,4096]{1,0:T(8,128)(2,1)} %x_ref.1), custom_call_target="tpu_custom_call" | custom-call | flops 4194304 | bytes 8388608 | tf_op jit(solution)/shard_map/staged/pallas_call | solution.py:72
  34.6 1.4 %shard_map.170 = (bf16[128,512]{1,0:T(8,128)(2,1)S(1)}, bf16[8,4,2,64,128]{4,3,2,1,0:T(8,128)(2,1)S(1)}) custom-call(bf16[512,4096]{1,0:T(8,128)(2,1)S(1)} %get-tuple-element.35.refs_0_, bf16[4,8,64,128]{3,2,1,0:T(8,128)(2,1)S(1)} %pad_maximum_fusion.refs_1_, bf16[4,8,64,128]{3,2,1,0:T(8,128)(2,1)S(1)} %collective-permute-done.3.refs_2_), custom_call_target="tpu_custom_call" | custom-call | flops 1073741824 | bytes 1048576 | tf_op jit(solution)/shard_map/pallas_call | solution.py:38
  36.0 1.3 %shard_map.171.refs_1_ = bf16[128,512]{1,0:T(8,128)(2,1)S(1)} custom-call(bf16[512,4096]{1,0:T(8,128)(2,1)S(1)} %get-tuple-element.37.refs_0_, bf16[8,4,2,64,128]{4,3,2,1,0:T(8,128)(2,1)S(1)} %get-tuple-element.38.refs_1_), custom_call_target="tpu_custom_call" | custom-call | flops 1073741824 | bytes 1048576 | tf_op jit(solution)/shard_map/pallas_call | solution.py:38
  37.3 2.8 %collective-permute-start.5 = (bf16[128,512]{1,0:T(8,128)(2,1)S(1)}, bf16[128,512]{1,0:T(8,128)(2,1)S(1)}, u32[]{:S(2)}, u32[]{:S(2)}) collective-permute-start(bf16[128,512]{1,0:T(8,128)(2,1)S(1)} %shard_map.171.refs_1_), channel_id=1, source_target_pairs={{0,3},{1,0},{2,1},{3,2},{4,7},{5,4},{6,5},{7,6},{8,11},{9,8},{10,9... | collective-permute-start | bytes 393224 | tf_op jit(solution)/shard_map/ppermute | solution.py:274
  40.1 2.7 %collective-permute-start.4 = (bf16[128,512]{1,0:T(8,128)(2,1)S(1)}, bf16[128,512]{1,0:T(8,128)(2,1)S(1)}, u32[]{:S(2)}, u32[]{:S(2)}) collective-permute-start(bf16[128,512]{1,0:T(8,128)(2,1)S(1)} %get-tuple-element.36.refs_0_), channel_id=1, source_target_pairs={{0,3},{1,0},{2,1},{3,2},{4,7},{5,4},{6,5},{7,6},{8,11},{9,8},{10,9... | collective-permute-start | bytes 393224 | tf_op jit(solution)/shard_map/ppermute | solution.py:272
  42.9 3.4 %collective-permute-start.8 = (bf16[128,512]{1,0:T(8,128)(2,1)S(1)}, bf16[128,512]{1,0:T(8,128)(2,1)S(1)}, u32[]{:S(2)}, u32[]{:S(2)}) collective-permute-start(bf16[128,512]{1,0:T(8,128)(2,1)S(1)} %collective-permute-done.5.refs_3_), channel_id=1, source_target_pairs={{0,3},{1,0},{2,1},{3,2},{4,7},{5,4},{6,5},{7,6},{8,11},{9,8},{10,9... | collective-permute-start | bytes 393224 | tf_op jit(solution)/shard_map/ppermute | solution.py:276
  46.4 2.5 %collective-permute-done.9.refs_7_ = bf16[128,512]{1,0:T(8,128)(2,1)S(1)} collective-permute-done((bf16[128,512]{1,0:T(8,128)(2,1)S(1)}, bf16[128,512]{1,0:T(8,128)(2,1)S(1)}, u32[]{:S(2)}, u32[]{:S(2)}) %collective-permute-start.9) | collective-permute-done | bytes 131104 | tf_op jit(solution)/shard_map/ppermute | solution.py:273
  48.9 2.5 %collective-permute-done.7.refs_4_ = bf16[128,512]{1,0:T(8,128)(2,1)S(1)} collective-permute-done((bf16[128,512]{1,0:T(8,128)(2,1)S(1)}, bf16[128,512]{1,0:T(8,128)(2,1)S(1)}, u32[]{:S(2)}, u32[]{:S(2)}) %collective-permute-start.7) | collective-permute-done | bytes 131104 | tf_op jit(solution)/shard_map/ppermute | solution.py:275
  52.1 2.9 %collective-permute-start.10 = (bf16[256,768]{1,0:T(8,128)(2,1)S(1)}, bf16[256,768]{1,0:T(8,128)(2,1)S(1)}, u32[]{:S(2)}, u32[]{:S(2)}) collective-permute-start(bf16[256,768]{1,0:T(8,128)(2,1)S(1)} %get-tuple-element.40), channel_id=1, source_target_pairs={{0,4},{4,0},{1,5},{5,1},{2,6},{6,2},{3,7},{7,3},{8,12},{12,8},{9,1... | collective-permute-start | bytes 1179656 | tf_op jit(solution)/shard_map/ppermute | solution.py:29
  57.2 3.9 %all-to-all-start.1 = ((bf16[32,8,768]{2,1,0:T(8,128)(2,1)}), bf16[32,8,768]{2,1,0:T(8,128)(2,1)S(1)}, u32[]{:S(2)}, u32[]{:S(2)}) async-start(bf16[32,8,768]{2,1,0:T(8,128)(2,1)} %fusion), calls=%async_computation.1 | async-start | bytes 786432 | tf_op jit(solution)/shard_map/all_to_all | solution.py:297
  61.9 0.8 collective-permute-done.11.theirs
  62.8 12.7 %all-to-all-done.1.arrived = bf16[32,8,768]{2,1,0:T(8,128)(2,1)S(1)} async-done(((bf16[32,8,768]{2,1,0:T(8,128)(2,1)}), bf16[32,8,768]{2,1,0:T(8,128)(2,1)S(1)}, u32[]{:S(2)}, u32[]{:S(2)}) %all-to-all-start.1) | async-done | bytes 393248 | tf_op jit(solution)/shard_map/all_to_all | solution.py:297
  75.6 17.0 %all_to_all.16 = bf16[32,8,768]{2,1,0:T(8,128)(2,1)S(1)} all-to-all(bf16[32,8,768]{2,1,0:T(8,128)(2,1)S(1)} %get-tuple-element.43), channel_id=1, replica_groups=mesh['z'=8,'x'=4,'c'=2,'tp'=4] {'z','x'}, dimensions={0} | all-to-all | bytes 786432 | tf_op jit(solution)/shard_map/all_to_all | solution.py:301
  92.5 3.5 %collective-permute-start.12 = (bf16[256,768]{1,0:T(8,128)(2,1)S(1)}, bf16[256,768]{1,0:T(8,128)(2,1)S(1)}, u32[]{:S(2)}, u32[]{:S(2)}) collective-permute-start(bf16[256,768]{1,0:T(8,128)(2,1)S(1)} %bitcast.10), channel_id=1, source_target_pairs={{0,4},{4,0},{1,5},{5,1},{2,6},{6,2},{3,7},{7,3},{8,12},{12,8},{9,1... | collective-permute-start | bytes 1179656 | tf_op jit(solution)/shard_map/ppermute | solution.py:29
  97.1 9.0 %collective-permute-done.14.gram_y = f32[256,256]{1,0:T(8,128)S(1)} collective-permute-done((f32[256,256]{1,0:T(8,128)S(1)}, f32[256,256]{1,0:T(8,128)S(1)}, u32[]{:S(2)}, u32[]{:S(2)}) %collective-permute-start.14) | collective-permute-done | bytes 262176 | tf_op jit(solution)/shard_map/ppermute | solution.py:306
  107.0 1.5 %collective-permute-start.16 = (f32[1,128]{1,0:T(1,128)S(1)}, f32[1,128]{1,0:T(1,128)S(1)}, u32[]{:S(2)}, u32[]{:S(2)}) collective-permute-start(f32[1,128]{1,0:T(1,128)S(1)} %shard_map.178.s0), channel_id=1, source_target_pairs={{0,2},{1,3},{2,0},{3,1},{4,6},{5,7},{6,4},{7,5},{8,10},{9,11},{10,... | collective-permute-start | bytes 1544 | tf_op jit(solution)/shard_map/ppermute | solution.py:319
  108.5 1.2 %collective-permute-start.17 = (f32[1,128]{1,0:T(1,128)S(1)}, f32[1,128]{1,0:T(1,128)S(1)}, u32[]{:S(2)}, u32[]{:S(2)}) collective-permute-start(f32[1,128]{1,0:T(1,128)S(1)} %shard_map.178.s0), channel_id=1, source_target_pairs={{0,3},{1,0},{2,1},{3,2},{4,7},{5,4},{6,5},{7,6},{8,11},{9,8},{10,9... | collective-permute-start | bytes 1544 | tf_op jit(solution)/shard_map/ppermute | solution.py:319
  111.2 0.9 shard_map.181
  (56 shorter events, 9.3 us)
Async XLA Ops:
  18.0 5.4 %collective-permute-start = (bf16[8,64,128]{2,1,0:T(8,128)(2,1)S(1)}, bf16[8,64,128]{2,1,0:T(8,128)(2,1)S(1)}, u32[]{:S(2)}, u32[]{:S(2)}) collective-permute-start(bf16[8,64,128]{2,1,0:T(8,128)(2,1)S(1)} %all_to_all.15), channel_id=1, source_target_pairs={{8,0},{16,8},{24,16},{0,24},{9,1},{17,9},{25,17},{1,25},{10,2},{18... | collective-permute-start | bytes 393224 | tf_op jit(solution)/shard_map/ppermute | solution.py:262
  20.4 5.4 %collective-permute-start.1 = (bf16[8,64,128]{2,1,0:T(8,128)(2,1)S(1)}, bf16[8,64,128]{2,1,0:T(8,128)(2,1)S(1)}, u32[]{:S(2)}, u32[]{:S(2)}) collective-permute-start(bf16[8,64,128]{2,1,0:T(8,128)(2,1)S(1)} %all_to_all.15), channel_id=1, source_target_pairs={{16,0},{24,8},{0,16},{8,24},{17,1},{25,9},{1,17},{9,25},{18,2},{26... | collective-permute-start | bytes 393224 | tf_op jit(solution)/shard_map/ppermute | solution.py:262
  21.0 6.2 %collective-permute-start.2 = (bf16[8,64,128]{2,1,0:T(8,128)(2,1)S(1)}, bf16[8,64,128]{2,1,0:T(8,128)(2,1)S(1)}, u32[]{:S(2)}, u32[]{:S(2)}) collective-permute-start(bf16[8,64,128]{2,1,0:T(8,128)(2,1)S(1)} %all_to_all.15), channel_id=1, source_target_pairs={{24,0},{0,8},{8,16},{16,24},{25,1},{1,9},{9,17},{17,25},{26,2},{2,... | collective-permute-start | bytes 393224 | tf_op jit(solution)/shard_map/ppermute | solution.py:262
  27.2 7.3 %collective-permute-start.3 = (bf16[4,8,64,128]{3,2,1,0:T(8,128)(2,1)S(1)}, bf16[4,8,64,128]{3,2,1,0:T(8,128)(2,1)S(1)}, u32[]{:S(2)}, u32[]{:S(2)}) collective-permute-start(bf16[4,8,64,128]{3,2,1,0:T(8,128)(2,1)S(1)} %pad_maximum_fusion.refs_1_), channel_id=1, source_target_pairs={{0,4},{4,0},{1,5},{5,1},{2,6},{6,2},{3,7},{7,3},{8,12},{12,8},{9,1... | collective-permute-start | bytes 1572872 | tf_op jit(solution)/shard_map/ppermute | solution.py:29
  34.5 16.8 %copy-start = (bf16[1024,1024]{1,0:T(8,128)(2,1)S(1)}, bf16[1024,1024]{1,0:T(8,128)(2,1)}, u32[]{:S(2)}) copy-start(bf16[1024,1024]{1,0:T(8,128)(2,1)} %v_ref.1) | copy-start | bytes 6291460
  34.6 16.8 %copy-start.1 = (bf16[1024,512]{1,0:T(8,128)(2,1)S(1)}, bf16[1024,512]{1,0:T(8,128)(2,1)}, u32[]{:S(2)}) copy-start(bf16[1024,512]{1,0:T(8,128)(2,1)} %k_ref.1) | copy-start | bytes 3145732
  37.3 5.6 %collective-permute-start.5 = (bf16[128,512]{1,0:T(8,128)(2,1)S(1)}, bf16[128,512]{1,0:T(8,128)(2,1)S(1)}, u32[]{:S(2)}, u32[]{:S(2)}) collective-permute-start(bf16[128,512]{1,0:T(8,128)(2,1)S(1)} %shard_map.171.refs_1_), channel_id=1, source_target_pairs={{0,3},{1,0},{2,1},{3,2},{4,7},{5,4},{6,5},{7,6},{8,11},{9,8},{10,9... | collective-permute-start | bytes 393224 | tf_op jit(solution)/shard_map/ppermute | solution.py:274
  40.1 6.2 %collective-permute-start.6 = (bf16[128,512]{1,0:T(8,128)(2,1)S(1)}, bf16[128,512]{1,0:T(8,128)(2,1)S(1)}, u32[]{:S(2)}, u32[]{:S(2)}) collective-permute-start(bf16[128,512]{1,0:T(8,128)(2,1)S(1)} %get-tuple-element.36.refs_0_), channel_id=1, source_target_pairs={{0,1},{1,2},{2,3},{3,0},{4,5},{5,6},{6,7},{7,4},{8,9},{9,10},{10,1... | collective-permute-start | bytes 393224 | tf_op jit(solution)/shard_map/ppermute | solution.py:271
  40.1 8.8 %collective-permute-start.9 = (bf16[128,512]{1,0:T(8,128)(2,1)S(1)}, bf16[128,512]{1,0:T(8,128)(2,1)S(1)}, u32[]{:S(2)}, u32[]{:S(2)}) collective-permute-start(bf16[128,512]{1,0:T(8,128)(2,1)S(1)} %shard_map.171.refs_1_), channel_id=1, source_target_pairs={{0,1},{1,2},{2,3},{3,0},{4,5},{5,6},{6,7},{7,4},{8,9},{9,10},{10,1... | collective-permute-start | bytes 393224 | tf_op jit(solution)/shard_map/ppermute | solution.py:273
  40.1 8.8 %collective-permute-start.4 = (bf16[128,512]{1,0:T(8,128)(2,1)S(1)}, bf16[128,512]{1,0:T(8,128)(2,1)S(1)}, u32[]{:S(2)}, u32[]{:S(2)}) collective-permute-start(bf16[128,512]{1,0:T(8,128)(2,1)S(1)} %get-tuple-element.36.refs_0_), channel_id=1, source_target_pairs={{0,3},{1,0},{2,1},{3,2},{4,7},{5,4},{6,5},{7,6},{8,11},{9,8},{10,9... | collective-permute-start | bytes 393224 | tf_op jit(solution)/shard_map/ppermute | solution.py:272
  42.9 5.9 %collective-permute-start.8 = (bf16[128,512]{1,0:T(8,128)(2,1)S(1)}, bf16[128,512]{1,0:T(8,128)(2,1)S(1)}, u32[]{:S(2)}, u32[]{:S(2)}) collective-permute-start(bf16[128,512]{1,0:T(8,128)(2,1)S(1)} %collective-permute-done.5.refs_3_), channel_id=1, source_target_pairs={{0,3},{1,0},{2,1},{3,2},{4,7},{5,4},{6,5},{7,6},{8,11},{9,8},{10,9... | collective-permute-start | bytes 393224 | tf_op jit(solution)/shard_map/ppermute | solution.py:276
  46.4 5.0 %collective-permute-start.7 = (bf16[128,512]{1,0:T(8,128)(2,1)S(1)}, bf16[128,512]{1,0:T(8,128)(2,1)S(1)}, u32[]{:S(2)}, u32[]{:S(2)}) collective-permute-start(bf16[128,512]{1,0:T(8,128)(2,1)S(1)} %collective-permute-done.6.refs_6_), channel_id=1, source_target_pairs={{0,1},{1,2},{2,3},{3,0},{4,5},{5,6},{6,7},{7,4},{8,9},{9,10},{10,1... | collective-permute-start | bytes 393224 | tf_op jit(solution)/shard_map/ppermute | solution.py:275
  52.0 9.1 %copy-start.2 = (f32[64,1024]{1,0:T(8,128)S(1)}, f32[64,1024]{1,0:T(8,128)}, u32[]{:S(2)}) copy-start(f32[64,1024]{1,0:T(8,128)} %refs_3_.1) | copy-start | bytes 786436
  52.0 9.1 %copy-start.3 = (bf16[64,256]{1,0:T(8,128)(2,1)S(1)}, bf16[64,256]{1,0:T(8,128)(2,1)}, u32[]{:S(2)}) copy-start(bf16[64,256]{1,0:T(8,128)(2,1)} %refs_0_.1) | copy-start | bytes 98308
  52.1 4.2 %collective-permute-start.10 = (bf16[256,768]{1,0:T(8,128)(2,1)S(1)}, bf16[256,768]{1,0:T(8,128)(2,1)S(1)}, u32[]{:S(2)}, u32[]{:S(2)}) collective-permute-start(bf16[256,768]{1,0:T(8,128)(2,1)S(1)} %get-tuple-element.40), channel_id=1, source_target_pairs={{0,4},{4,0},{1,5},{5,1},{2,6},{6,2},{3,7},{7,3},{8,12},{12,8},{9,1... | collective-permute-start | bytes 1179656 | tf_op jit(solution)/shard_map/ppermute | solution.py:29
  57.2 18.3 %all-to-all-start.1 = ((bf16[32,8,768]{2,1,0:T(8,128)(2,1)}), bf16[32,8,768]{2,1,0:T(8,128)(2,1)S(1)}, u32[]{:S(2)}, u32[]{:S(2)}) async-start(bf16[32,8,768]{2,1,0:T(8,128)(2,1)} %fusion), calls=%async_computation.1 | async-start | bytes 786432 | tf_op jit(solution)/shard_map/all_to_all | solution.py:297
  61.0 35.0 %collective-permute-start.13 = (bf16[8,4,2,64,128]{4,3,2,1,0:T(8,128)(2,1)S(1)}, bf16[8,4,2,64,128]{4,3,2,1,0:T(8,128)(2,1)S(1)}, u32[]{:S(2)}, u32[]{:S(2)}) collective-permute-start(bf16[8,4,2,64,128]{4,3,2,1,0:T(8,128)(2,1)S(1)} %get-tuple-element.38.refs_1_), channel_id=1, source_target_pairs={{0,1},{1,0},{2,3},{3,2},{4,5},{5,4},{6,7},{7,6},{8,9},{9,8},{10,11... | collective-permute-start | bytes 3145736 | tf_op jit(solution)/shard_map/ppermute | solution.py:289
  61.3 1.5 %collective-permute-start.11 = (f32[8,768]{1,0:T(8,128)S(1)}, f32[8,768]{1,0:T(8,128)S(1)}, u32[]{:S(2)}, u32[]{:S(2)}) collective-permute-start(f32[8,768]{1,0:T(8,128)S(1)} %get-tuple-element.42), channel_id=1, source_target_pairs={{0,4},{4,0},{1,5},{5,1},{2,6},{6,2},{3,7},{7,3},{8,12},{12,8},{9,1... | collective-permute-start | bytes 73736 | tf_op jit(solution)/shard_map/ppermute | solution.py:29
  92.5 14.0 %collective-permute-start.12 = (bf16[256,768]{1,0:T(8,128)(2,1)S(1)}, bf16[256,768]{1,0:T(8,128)(2,1)S(1)}, u32[]{:S(2)}, u32[]{:S(2)}) collective-permute-start(bf16[256,768]{1,0:T(8,128)(2,1)S(1)} %bitcast.10), channel_id=1, source_target_pairs={{0,4},{4,0},{1,5},{5,1},{2,6},{6,2},{3,7},{7,3},{8,12},{12,8},{9,1... | collective-permute-start | bytes 1179656 | tf_op jit(solution)/shard_map/ppermute | solution.py:29
  96.9 9.2 %collective-permute-start.14 = (f32[256,256]{1,0:T(8,128)S(1)}, f32[256,256]{1,0:T(8,128)S(1)}, u32[]{:S(2)}, u32[]{:S(2)}) collective-permute-start(f32[256,256]{1,0:T(8,128)S(1)} %shard_map.176.gram), channel_id=1, source_target_pairs={{0,3},{1,2},{2,1},{3,0},{4,7},{5,6},{6,5},{7,4},{8,11},{9,10},{10,... | collective-permute-start | bytes 786440 | tf_op jit(solution)/shard_map/ppermute | solution.py:306
  97.0 12.7 %collective-permute-start.18 = (f32[8,768]{1,0:T(8,128)S(1)}, f32[8,768]{1,0:T(8,128)S(1)}, u32[]{:S(2)}, u32[]{:S(2)}) collective-permute-start(f32[8,768]{1,0:T(8,128)S(1)} %get-tuple-element.57), channel_id=1, source_target_pairs={{0,4},{4,0},{1,5},{5,1},{2,6},{6,2},{3,7},{7,3},{8,12},{12,8},{9,1... | collective-permute-start | bytes 73736 | tf_op jit(solution)/shard_map/ppermute | solution.py:29
  106.9 3.8 %collective-permute-start.15 = (f32[1,128]{1,0:T(1,128)S(1)}, f32[1,128]{1,0:T(1,128)S(1)}, u32[]{:S(2)}, u32[]{:S(2)}) collective-permute-start(f32[1,128]{1,0:T(1,128)S(1)} %shard_map.178.s0), channel_id=1, source_target_pairs={{0,1},{1,2},{2,3},{3,0},{4,5},{5,6},{6,7},{7,4},{8,9},{9,10},{10,1... | collective-permute-start | bytes 1544 | tf_op jit(solution)/shard_map/ppermute | solution.py:319
  107.0 4.0 %collective-permute-start.16 = (f32[1,128]{1,0:T(1,128)S(1)}, f32[1,128]{1,0:T(1,128)S(1)}, u32[]{:S(2)}, u32[]{:S(2)}) collective-permute-start(f32[1,128]{1,0:T(1,128)S(1)} %shard_map.178.s0), channel_id=1, source_target_pairs={{0,2},{1,3},{2,0},{3,1},{4,6},{5,7},{6,4},{7,5},{8,10},{9,11},{10,... | collective-permute-start | bytes 1544 | tf_op jit(solution)/shard_map/ppermute | solution.py:319
  108.5 2.7 %collective-permute-start.17 = (f32[1,128]{1,0:T(1,128)S(1)}, f32[1,128]{1,0:T(1,128)S(1)}, u32[]{:S(2)}, u32[]{:S(2)}) collective-permute-start(f32[1,128]{1,0:T(1,128)S(1)} %shard_map.178.s0), channel_id=1, source_target_pairs={{0,3},{1,0},{2,1},{3,2},{4,7},{5,4},{6,5},{7,6},{8,11},{9,8},{10,9... | collective-permute-start | bytes 1544 | tf_op jit(solution)/shard_map/ppermute | solution.py:319
  (6 other events, 54.7 us)
